TPU v7x, 128 devices: a whole 4x4x4 slice. The times are simulated.
128 devices in a mesh: sp: 16 (over z, x), tp: 8 (over y, core).
Axes of the slice: x: 4, y: 4, z: 4, core: 2. Of those that a mesh axis runs over, the one named last changes fastest.
Arguments:
- tokens: bfloat16 [4, 16384, 2048], P(None, 'sp'), may hold values from -6 to 6
- norm_gain: bfloat16 [2048], replicated, may hold values from 0.099609375 to 1.8984375
- conv_value_weight: bfloat16 [2048, 1024], P('sp', 'tp'), may hold values from -0.125 to 0.125
- conv_gate_weight: bfloat16 [2048, 1024], P('sp', 'tp'), may hold values from -0.125 to 0.125
- query_weight: bfloat16 [2048, 1024], P('sp', 'tp'), may hold values from -40 to 40
- key_weight: bfloat16 [2048, 512], P('sp', 'tp'), may hold values from -1 to 1
- value_weight: bfloat16 [2048, 512], P('sp', 'tp'), may hold values from -0.125 to 0.125
- conv_taps: bfloat16 [31, 1024], P(None, 'tp'), may hold values from -1 to 1
- conv_gain: bfloat16 [1024], P('tp'), may hold values from 0.099609375 to 1.8984375
- sink_logit: float32 [16], P('tp'), may hold values from 1 to 6
- out_conv_weight: bfloat16 [1024, 2048], P('tp', 'sp'), may hold values from -0.125 to 0.125
- out_attn_weight: bfloat16 [1024, 2048], P('tp', 'sp'), may hold values from -0.125 to 0.125
Outputs:
- mixed: bfloat16 [4, 16384, 2048], P(None, ('sp', 'tp'))
- log_total: float32 [4, 16, 16384], P(None, 'tp', 'sp')
All inputs are finite; a program needn't handle non-finite values.
Results may differ from a plain program's by a relative error of at most 0.015.
Values may be sent and summed in bfloat16 or wider, within the bound.
No kernel may reach another device: no remote copies, remote signals or barrier semaphores. Data moves between devices by JAX's collectives and lax.ppermute only.
A program may use at most 128 MiB of HBM per device.

v0:
```python
import functools

import jax
import jax.numpy as jnp
from jax import lax
from jax.experimental import pallas as pl
from jax.experimental.pallas import tpu as pltpu
from jax.sharding import PartitionSpec as P

HEAD_DIM = 64
WINDOW = 128
EPSILON = 1e-06
ROPE_BASE = 10000.0
MASK_VALUE = -1e30
LANES = 128
EDGE = 16
Q_BLOCK = 256
BF16 = jnp.bfloat16
F32 = jnp.float32


def params(*semantics, mb=48):
    return pltpu.CompilerParams(
        dimension_semantics=semantics, vmem_limit_bytes=mb * 1024 * 1024
    )


def norm_kernel(x_ref, gain_ref, out_ref):
    x = x_ref[...].astype(F32)
    mean = jnp.mean(x, axis=-1, keepdims=True)
    centred = x - mean
    variance = jnp.mean(centred * centred, axis=-1, keepdims=True)
    scaled = centred * lax.rsqrt(variance + EPSILON)
    out_ref[...] = (scaled * gain_ref[...].astype(F32)).astype(BF16)


def norm_tokens(x, gain, block=256):
    rows, width = x.shape
    return pl.pallas_call(
        norm_kernel,
        grid=(rows // block,),
        in_specs=[
            pl.BlockSpec((block, width), lambda i: (i, 0)),
            pl.BlockSpec((1, width), lambda i: (0, 0)),
        ],
        out_specs=pl.BlockSpec((block, width), lambda i: (i, 0)),
        out_shape=jax.ShapeDtypeStruct((rows, width), BF16),
        compiler_params=params("arbitrary"),
        cost_estimate=pl.CostEstimate(
            flops=40 * rows * width, transcendentals=rows, bytes_accessed=4 * rows * width
        ),
        name="norm_tokens",
    )(x, gain.reshape(1, width))


def project_kernel(x_ref, w_ref, cos_ref, sin_ref, gated_ref, q_ref, kv_ref):
    pieces, rows, cols = w_ref.shape
    raw = jnp.dot(
        x_ref[...], w_ref[...].reshape(pieces * rows, cols), preferred_element_type=F32
    )
    value, gate = raw[:, :LANES], raw[:, LANES : 2 * LANES]
    gated_ref[...] = (value * jax.nn.sigmoid(gate)).astype(BF16)
    lane = lax.broadcasted_iota(jnp.int32, value.shape, 1)
    low = (lane % HEAD_DIM) < HEAD_DIM // 2
    half = HEAD_DIM // 2
    for part, ref, scale in ((2, q_ref, HEAD_DIM**-0.5), (3, kv_ref, None)):
        x = raw[:, part * LANES : (part + 1) * LANES]
        partner = jnp.where(low, pltpu.roll(x, LANES - half, 1), pltpu.roll(x, half, 1))
        at = slice((part - 2) * LANES, (part - 1) * LANES)
        turned = x * cos_ref[:, at] + partner * sin_ref[:, at]
        if scale is not None:
            turned = turned * scale
        ref[...] = turned.astype(BF16)


def project(normed, weight, cosine, sine, block=512):
    rows, width = normed.shape
    per_seq = cosine.shape[0] // block
    out = pl.BlockSpec((block, LANES), lambda i: (i, 0))
    return pl.pallas_call(
        project_kernel,
        grid=(rows // block,),
        in_specs=[
            pl.BlockSpec((block, width), lambda i: (i, 0)),
            pl.BlockSpec(weight.shape, lambda i: (0, 0, 0)),
            pl.BlockSpec((block, 2 * LANES), lambda i: (i % per_seq, 0)),
            pl.BlockSpec((block, 2 * LANES), lambda i: (i % per_seq, 0)),
        ],
        out_specs=[out, out, out],
        out_shape=[jax.ShapeDtypeStruct((rows, LANES), BF16)] * 3,
        compiler_params=params("arbitrary"),
        cost_estimate=pl.CostEstimate(
            flops=2 * rows * width * weight.shape[2],
            transcendentals=0,
            bytes_accessed=2 * rows * width,
        ),
        name="project",
    )(normed, weight, cosine, sine)


def conv_kernel(before_ref, x_ref, after_ref, taps_ref, out_ref, buf_ref, *, chunk):
    length = x_ref.shape[1]
    buf_ref[0:EDGE, :] = before_ref[0].astype(F32)
    buf_ref[EDGE : EDGE + length, :] = x_ref[0].astype(F32)
    buf_ref[EDGE + length : 2 * EDGE + length, :] = after_ref[0].astype(F32)
    tap_count = taps_ref.shape[0]
    shift = EDGE - tap_count // 2
    dests, _, share, _ = out_ref.shape

    def one(dest, _):
        for part in range(share // chunk):
            total = jnp.zeros((chunk, LANES), F32)
            for tap in range(tap_count):
                at = dest * share + (part * chunk + shift + tap)
                total = total + buf_ref[pl.ds(at, chunk), :] * taps_ref[tap : tap + 1, :]
            out_ref[dest, 0, pl.ds(part * chunk, chunk), :] = total.astype(BF16)
        return 0

    lax.fori_loop(0, dests, one, 0)


def conv(before, gated, after, taps, dests, chunk=64):
    seqs, length, _ = gated.shape
    edge = pl.BlockSpec((1, EDGE, LANES), lambda s: (s, 0, 0))
    return pl.pallas_call(
        functools.partial(conv_kernel, chunk=chunk),
        grid=(seqs,),
        in_specs=[
            edge,
            pl.BlockSpec((1, length, LANES), lambda s: (s, 0, 0)),
            edge,
            pl.BlockSpec(taps.shape, lambda s: (0, 0)),
        ],
        out_specs=pl.BlockSpec((dests, 1, length // dests, LANES), lambda s: (0, s, 0, 0)),
        out_shape=jax.ShapeDtypeStruct((dests, seqs, length // dests, LANES), BF16),
        scratch_shapes=[pltpu.VMEM((length + 2 * EDGE, LANES), F32)],
        compiler_params=params("arbitrary"),
        cost_estimate=pl.CostEstimate(
            flops=60 * 31 * seqs * length * LANES,
            transcendentals=0,
            bytes_accessed=4 * seqs * length * LANES,
        ),
        name="conv",
    )(before, gated, after, taps)


def attend_kernel(
    place_ref, sink_ref, q_ref, before_ref, kv_ref, after_ref, out_ref, log_ref, pad_ref, bias_ref
):
    length = kv_ref.shape[1]
    seq, block = pl.program_id(0), pl.program_id(1)
    blocks = length // Q_BLOCK
    span = Q_BLOCK + 2 * WINDOW

    @pl.when((seq == 0) & (block == 0))
    def _():
        query = lax.broadcasted_iota(jnp.int32, (Q_BLOCK, span), 0)
        key = lax.broadcasted_iota(jnp.int32, (Q_BLOCK, span), 1)
        band = (key >= query) & (key <= query + 2 * WINDOW)
        first = jnp.where(place_ref[0] == 0, WINDOW, 0)
        last = jnp.where(place_ref[0] == place_ref[1] - 1, Q_BLOCK + WINDOW, span)
        zero, out = jnp.zeros(band.shape, F32), jnp.full(band.shape, MASK_VALUE, F32)
        bias_ref[0] = jnp.where(band, zero, out)
        bias_ref[1] = jnp.where(band & (key >= first), zero, out)
        bias_ref[2] = jnp.where(band & (key < last), zero, out)

    @pl.when(block == 0)
    def _():
        pad_ref[0:WINDOW, :] = before_ref[0]
        pad_ref[WINDOW : WINDOW + length, :] = kv_ref[0]
        pad_ref[WINDOW + length : 2 * WINDOW + length, :] = after_ref[0]

    keys = pad_ref[pl.ds(pl.multiple_of(block * Q_BLOCK, Q_BLOCK), span), :]
    bias = bias_ref[jnp.where(block == 0, 1, jnp.where(block == blocks - 1, 2, 0))]
    query = q_ref[0].astype(F32)
    lane = lax.broadcasted_iota(jnp.int32, (Q_BLOCK, LANES), 1)
    low = lane < HEAD_DIM
    sub = lax.broadcasted_iota(jnp.int32, (LANES, LANES), 0)
    diagonal = sub == lax.broadcasted_iota(jnp.int32, (LANES, LANES), 1)
    results = []
    for head in range(2):
        turned = query if head == 0 else pltpu.roll(query, HEAD_DIM, 1)
        own = jnp.where(low, turned, 0.0).astype(BF16)
        scores = lax.dot_general(
            own, keys, (((1,), (1,)), ((), ())), preferred_element_type=F32
        )
        scores = scores + bias
        sink = sink_ref[head]
        top = jnp.maximum(jnp.max(scores, axis=-1, keepdims=True), sink)
        weights = jnp.exp(scores - top)
        total = jnp.sum(weights, axis=-1, keepdims=True) + jnp.exp(sink - top)
        mixed = jnp.dot(weights.astype(BF16), keys, preferred_element_type=F32)
        results.append(mixed / total)
        log_total = jnp.broadcast_to(top + jnp.log(total), (Q_BLOCK, LANES))
        for part in range(Q_BLOCK // LANES):
            rows = log_total[part * LANES : (part + 1) * LANES]
            log_ref[0, head : head + 1, part * LANES : (part + 1) * LANES] = jnp.sum(
                jnp.where(diagonal, rows, 0.0), axis=0, keepdims=True
            )
    both = jnp.where(low, pltpu.roll(results[0], HEAD_DIM, 1), results[1]).astype(BF16)
    share = out_ref.shape[2]
    out_ref[...] = both.reshape(Q_BLOCK // share, 1, share, LANES)


def attend(place, sink, query, before, kv, after, dests):
    seqs, length, _ = kv.shape
    share = length // dests
    span = Q_BLOCK + 2 * WINDOW
    edge = pl.BlockSpec((1, WINDOW, LANES), lambda s, b: (s, 0, 0))
    smem = pl.BlockSpec(memory_space=pltpu.SMEM)
    return pl.pallas_call(
        attend_kernel,
        grid=(seqs, length // Q_BLOCK),
        in_specs=[
            smem,
            smem,
            pl.BlockSpec((1, Q_BLOCK, LANES), lambda s, b: (s, b, 0)),
            edge,
            pl.BlockSpec((1, length, LANES), lambda s, b: (s, 0, 0)),
            edge,
        ],
        out_specs=[
            pl.BlockSpec((Q_BLOCK // share, 1, share, LANES), lambda s, b: (b, s, 0, 0)),
            pl.BlockSpec((1, 2, Q_BLOCK), lambda s, b: (s, 0, b)),
        ],
        out_shape=[
            jax.ShapeDtypeStruct((dests, seqs, share, LANES), BF16),
            jax.ShapeDtypeStruct((seqs, 2, length), F32),
        ],
        scratch_shapes=[
            pltpu.VMEM((length + 2 * WINDOW, LANES), BF16),
            pltpu.VMEM((3, Q_BLOCK, span), F32),
        ],
        compiler_params=params("arbitrary", "arbitrary"),
        cost_estimate=pl.CostEstimate(
            flops=40 * seqs * length * span * LANES // 8,
            transcendentals=0,
            bytes_accessed=6 * seqs * length * LANES,
        ),
        name="attend",
    )(place, sink, query, before, kv, after)


def mix_kernel(conv_ref, attn_ref, gain_ref, w_ref, out_ref, act_ref):
    sources = conv_ref.shape[0]
    half = sources * LANES

    @pl.when(pl.program_id(0) == 0)
    def _():
        x = jnp.concatenate([conv_ref[s] for s in range(sources)], axis=-1).astype(F32)
        mean = jnp.mean(x, axis=-1, keepdims=True)
        centred = x - mean
        variance = jnp.mean(centred * centred, axis=-1, keepdims=True)
        v = centred * lax.rsqrt(variance + EPSILON) * gain_ref[...].astype(F32)
        act_ref[:, :half] = (v / (1.0 + jnp.exp(-v))).astype(BF16)
        for s in range(sources):
            act_ref[:, half + s * LANES : half + (s + 1) * LANES] = attn_ref[s]

    cols = w_ref.shape[0]
    conv_w = jnp.concatenate([w_ref[c, :, :LANES].reshape(half, LANES) for c in range(cols)], -1)
    attn_w = jnp.concatenate(
        [w_ref[c, :, LANES : 2 * LANES].reshape(half, LANES) for c in range(cols)], -1
    )
    total = jnp.dot(act_ref[:, :half], conv_w, preferred_element_type=F32)
    total = total + jnp.dot(act_ref[:, half:], attn_w, preferred_element_type=F32)
    out_ref[...] = total.astype(BF16)


def mix(conv_tok, attn_tok, gain, weight, cols=2):
    sources, rows, _ = conv_tok.shape
    groups, _, height, _ = weight.shape
    whole = pl.BlockSpec((sources, rows, LANES), lambda n: (0, 0, 0))
    return pl.pallas_call(
        mix_kernel,
        grid=(groups // cols,),
        in_specs=[
            whole,
            whole,
            pl.BlockSpec(gain.shape, lambda n: (0, 0)),
            pl.BlockSpec((cols, sources, height, LANES), lambda n: (n, 0, 0, 0)),
        ],
        out_specs=pl.BlockSpec((rows, cols * LANES), lambda n: (0, n)),
        out_shape=jax.ShapeDtypeStruct((rows, groups * LANES), BF16),
        scratch_shapes=[pltpu.VMEM((rows, 2 * sources * LANES), BF16)],
        compiler_params=params("arbitrary"),
        cost_estimate=pl.CostEstimate(
            flops=4 * rows * sources * LANES * groups * LANES,
            transcendentals=0,
            bytes_accessed=2 * weight.size,
        ),
        name="mix",
    )(conv_tok, attn_tok, gain, weight)


def turn_tables(tok_count):
    half = HEAD_DIM // 2
    offset = lax.axis_index("sp") * tok_count
    positions = (offset + jnp.arange(tok_count, dtype=jnp.int32)).astype(F32)
    inverse = ROPE_BASE ** (-jnp.arange(half, dtype=F32) / half)
    angles = positions[:, None] * inverse[None, :]
    c, s = jnp.cos(angles), jnp.sin(angles)
    one, zero = jnp.ones_like(c), jnp.zeros_like(s)
    cosine = jnp.concatenate([c, c, c, c, c, c, one, one], axis=-1)
    sine = jnp.concatenate([-s, s, -s, s, -s, s, zero, zero], axis=-1)
    return cosine, sine


def on_device(
    tokens,
    norm_gain,
    conv_value_weight,
    conv_gate_weight,
    query_weight,
    key_weight,
    value_weight,
    conv_taps,
    conv_gain,
    sink_logit,
    out_conv_weight,
    out_attn_weight,
):
    seqs, length, width = tokens.shape
    sp, tp = lax.axis_size("sp"), lax.axis_size("tp")
    place = jnp.stack([lax.axis_index("sp"), jnp.int32(sp)]).astype(jnp.int32)

    gain_rows = jnp.broadcast_to(conv_gain[None], (EDGE, LANES))
    out_piece = jnp.concatenate([out_conv_weight, out_attn_weight, gain_rows], axis=0)
    out_weight = lax.all_gather(out_piece, ("sp", "tp"), axis=0, tiled=True)
    out_weight = out_weight.reshape(sp, tp, out_piece.shape[0], LANES)

    in_piece = jnp.concatenate(
        [conv_value_weight, conv_gate_weight, query_weight, key_weight, value_weight], axis=1
    )
    in_weight = lax.all_to_all(
        jnp.broadcast_to(in_piece[None], (sp, *in_piece.shape)), "sp", 0, 0, tiled=True
    )
    normed = norm_tokens(tokens.reshape(seqs * length, width), norm_gain)
    cosine, sine = turn_tables(length)
    gated, query, kv = (
        a.reshape(seqs, length, LANES) for a in project(normed, in_weight, cosine, sine)
    )

    up = [(i, i + 1) for i in range(sp - 1)]
    down = [(i + 1, i) for i in range(sp - 1)]
    low = jnp.concatenate([kv[:, :WINDOW], gated[:, :EDGE]], axis=1)
    high = jnp.concatenate([kv[:, -WINDOW:], gated[:, -EDGE:]], axis=1)
    before = lax.ppermute(high, "sp", up)
    after = lax.ppermute(low, "sp", down)

    filtered = conv(
        before[:, WINDOW:], gated, after[:, WINDOW:], conv_taps.astype(F32), tp
    )
    conv_tok = lax.all_to_all(filtered, "tp", 0, 0, tiled=True)
    attn, log_total = attend(
        place, sink_logit, query, before[:, :WINDOW], kv, after[:, :WINDOW], tp
    )
    attn_tok = lax.all_to_all(attn, "tp", 0, 0, tiled=True)

    gain = out_weight[0, :, 2 * LANES].reshape(1, tp * LANES)
    rows = seqs * length // tp
    mixed = mix(
        conv_tok.reshape(tp, rows, LANES), attn_tok.reshape(tp, rows, LANES), gain, out_weight
    )
    return mixed.reshape(seqs, length // tp, width), log_total


def solution(mesh):
    placed = (
        P(None, "sp", None),
        P(),
        P("sp", "tp"),
        P("sp", "tp"),
        P("sp", "tp"),
        P("sp", "tp"),
        P("sp", "tp"),
        P(None, "tp"),
        P("tp"),
        P("tp"),
        P("tp", "sp"),
        P("tp", "sp"),
    )
    return jax.shard_map(
        on_device,
        mesh=mesh,
        in_specs=placed,
        out_specs=(P(None, ("sp", "tp"), None), P(None, "tp", "sp")),
        check_vma=False,
    )
```

profile of v0, /device:TPU:32, one launch (start us, length us, event | category | flops | bytes accessed | tf_op | source)
XLA Modules:
  0.0 156.9 jit_solution(9100520671002556928)
XLA Ops:
  7.9 1.4 pad_maximum_fusion.2
  9.3 0.8 copy.16
  10.1 0.8 copy.17
  10.9 0.9 concatenate.24
  11.8 1.5 broadcast_in_dim.4
  13.4 7.9 %all-to-all-start = ((bf16[16,128,512]{2,1,0:T(8,128)(2,1)}), bf16[16,128,512]{2,1,0:T(8,128)(2,1)}, u32[]{:S(2)}, u32[]{:S(2)}) async-start(bf16[16,128,512]{2,1,0:T(8,128)(2,1)} %broadcast_in_dim.4), calls=%async_computation | async-start | bytes 4194304 | tf_op jit(solution)/shard_map/all_to_all | solution.py:334
  21.3 0.7 reshape.45.gain_ref
  22.0 1.9 %multiply_sine_fusion = (f32[1024,32]{1,0:T(8,128)S(1)}, f32[1024,32]{1,0:T(8,128)S(1)}, f32[1024,32]{1,0:T(8,128)S(1)}) fusion(f32[1024]{0:T(1024)S(1)} %add_convert_fusion, f32[32]{0:T(128)S(1)} %multiply_power_fusion), kind=kLoop, calls=%fused_computation | loop fusion | flops 65536 | bytes 397440 | tf_op jit(solution)/shard_map/sin | solution.py:301
  23.9 3.3 %concatenate.26.cos_ref = f32[1024,256]{1,0:T(8,128)S(1)} concatenate(f32[1024,32]{1,0:T(8,128)S(1)} %get-tuple-element.18, f32[1024,32]{1,0:T(8,128)S(1)} %get-tuple-element.18, f32[1024,32]{1,0:T(8,128)S(1)} %get-tuple-element.18, f32[1024,32]{1,0:T(8,128)S(1)} %get-tuple-element.18, f32[1024,32]{1,0:T(8,128)S(1)} %get-tuple-element.18, f32[1024,32]{1,0:T(8,128)S(1)} %get-tuple-element.18, ...), dimensions={1} | concatenate | bytes 2097152 | tf_op jit(solution)/shard_map/concatenate | solution.py:303
  27.2 0.8 concatenate.27
  28.0 4.2 %concatenate.28.sin_ref = f32[1024,256]{1,0:T(8,128)S(1)} concatenate(f32[1024,32]{1,0:T(8,128)S(1)} %get-tuple-element.17, f32[1024,32]{1,0:T(8,128)S(1)} %get-tuple-element.16, f32[1024,32]{1,0:T(8,128)S(1)} %get-tuple-element.17, f32[1024,32]{1,0:T(8,128)S(1)} %get-tuple-element.16, f32[1024,32]{1,0:T(8,128)S(1)} %get-tuple-element.17, f32[1024,32]{1,0:T(8,128)S(1)} %get-tuple-element.16, ...), dimensions={1} | concatenate | bytes 2097152 | tf_op jit(solution)/shard_map/concatenate | solution.py:304
  32.2 20.1 %norm_tokens.1.x_ref = bf16[4096,2048]{1,0:T(8,128)(2,1)} custom-call(bf16[4096,2048]{1,0:T(8,128)(2,1)} %bitcast.18, bf16[1,2048]{1,0:T(2,128)(2,1)S(1)} %reshape.45.gain_ref), custom_call_target="tpu_custom_call" | custom-call | flops 335544320 | bytes 33554432 | tf_op jit(solution)/shard_map/norm_tokens/pallas_call | solution.py:39
  52.5 14.6 %project.1 = (bf16[4096,128]{1,0:T(8,128)(2,1)S(1)}, bf16[4096,128]{1,0:T(8,128)(2,1)S(1)}, bf16[4096,128]{1,0:T(8,128)(2,1)S(1)}) custom-call(bf16[4096,2048]{1,0:T(8,128)(2,1)} %norm_tokens.1.x_ref, bf16[16,128,512]{2,1,0:T(8,128)(2,1)} %all-to-all-done.w_ref, f32[1024,256]{1,0:T(8,128)S(1)} %concatenate.26.cos_ref, f32[1024,256]{1,0:T(8,128)S(1)} %concatenate.28.sin_ref), custom_call_target="tpu_custom_call" | custom-call | flops 8589934592 | bytes 16777216 | tf_op jit(solution)/shard_map/project/pallas_call | solution.py:80
  67.2 4.4 %collective-permute-start.1 = (bf16[4,144,128]{2,1,0:T(8,128)(2,1)S(1)}, bf16[4,144,128]{2,1,0:T(8,128)(2,1)S(1)}, u32[]{:S(2)}, u32[]{:S(2)}) collective-permute-start(bf16[4,144,128]{2,1,0:T(8,128)(2,1)S(1)} %pad_maximum_fusion.1), channel_id=1, source_target_pairs={{8,0},{16,8},{24,16},{32,24},{40,32},{48,40},{56,48},{64,56},{72,6... | collective-permute-start | bytes 442376 | tf_op jit(solution)/shard_map/ppermute | solution.py:348
  71.6 1.9 %collective-permute-start = (bf16[4,144,128]{2,1,0:T(8,128)(2,1)S(1)}, bf16[4,144,128]{2,1,0:T(8,128)(2,1)S(1)}, u32[]{:S(2)}, u32[]{:S(2)}) collective-permute-start(bf16[4,144,128]{2,1,0:T(8,128)(2,1)S(1)} %pad_maximum_fusion), channel_id=1, source_target_pairs={{0,8},{8,16},{16,24},{24,32},{32,40},{40,48},{48,56},{56,64},{64,7... | collective-permute-start | bytes 442376 | tf_op jit(solution)/shard_map/ppermute | solution.py:347
  74.2 8.5 %collective-permute-done = bf16[4,144,128]{2,1,0:T(8,128)(2,1)S(1)} collective-permute-done((bf16[4,144,128]{2,1,0:T(8,128)(2,1)S(1)}, bf16[4,144,128]{2,1,0:T(8,128)(2,1)S(1)}, u32[]{:S(2)}, u32[]{:S(2)}) %collective-permute-start) | collective-permute-done | bytes 147488 | tf_op jit(solution)/shard_map/ppermute | solution.py:347
  82.8 15.5 %attend.1 = (bf16[8,4,128,128]{3,2,1,0:T(8,128)(2,1)}, f32[4,2,1024]{2,1,0:T(2,128)}) custom-call(s32[2]{0:T(128)S(1)} %pad_add_fusion.place_ref, f32[2]{0:T(128)S(1)} %copy-done, bf16[4,1024,128]{2,1,0:T(8,128)(2,1)S(1)} %bitcast.17, bf16[4,128,128]{2,1,0:T(8,128)(2,1)S(1)} %slice.42.before_ref, bf16[4,1024,128]{2,1,0:T(8,128)(2,1)S(1)} %bitcast.14, ...), custom_call_target="tpu_custom_call" | custom-call | flops 1342177280 | bytes 3145728 | tf_op jit(solution)/shard_map/attend/pallas_call | solution.py:211
  98.3 5.1 %all-to-all-start.2 = ((bf16[8,4,128,128]{3,2,1,0:T(8,128)(2,1)}), bf16[8,4,128,128]{3,2,1,0:T(8,128)(2,1)S(1)}, u32[]{:S(2)}, u32[]{:S(2)}) async-start(bf16[8,4,128,128]{3,2,1,0:T(8,128)(2,1)} %get-tuple-element.10), calls=%async_computation.2 | async-start | bytes 2097152 | tf_op jit(solution)/shard_map/all_to_all | solution.py:357
  103.5 5.6 %conv.1 = bf16[8,4,128,128]{3,2,1,0:T(8,128)(2,1)} custom-call(bf16[4,16,128]{2,1,0:T(8,128)(2,1)S(1)} %slice.38.before_ref, bf16[4,1024,128]{2,1,0:T(8,128)(2,1)S(1)} %bitcast.16, bf16[4,16,128]{2,1,0:T(8,128)(2,1)S(1)} %slice.41.after_ref, f32[31,128]{1,0:T(8,128)S(1)} %convert_element_type.11.taps_ref), custom_call_target="tpu_custom_call" | custom-call | flops 975175680 | bytes 2097152 | tf_op jit(solution)/shard_map/conv/pallas_call | solution.py:125
  109.1 10.3 %all-to-all-done.2 = bf16[8,4,128,128]{3,2,1,0:T(8,128)(2,1)S(1)} async-done(((bf16[8,4,128,128]{3,2,1,0:T(8,128)(2,1)}), bf16[8,4,128,128]{3,2,1,0:T(8,128)(2,1)S(1)}, u32[]{:S(2)}, u32[]{:S(2)}) %all-to-all-start.2) | async-done | bytes 1048608 | tf_op jit(solution)/shard_map/all_to_all | solution.py:357
  119.4 3.6 %all-to-all-start.1 = ((bf16[8,4,128,128]{3,2,1,0:T(8,128)(2,1)}), bf16[8,4,128,128]{3,2,1,0:T(8,128)(2,1)S(1)}, u32[]{:S(2)}, u32[]{:S(2)}) async-start(bf16[8,4,128,128]{3,2,1,0:T(8,128)(2,1)} %conv.1), calls=%async_computation.1 | async-start | bytes 2097152 | tf_op jit(solution)/shard_map/all_to_all | solution.py:353
  123.0 0.7 slice_bitcast_fusion.gain_ref
  123.7 15.1 %all-to-all-done.1 = bf16[8,4,128,128]{3,2,1,0:T(8,128)(2,1)S(1)} async-done(((bf16[8,4,128,128]{3,2,1,0:T(8,128)(2,1)}), bf16[8,4,128,128]{3,2,1,0:T(8,128)(2,1)S(1)}, u32[]{:S(2)}, u32[]{:S(2)}) %all-to-all-start.1) | async-done | bytes 1048608 | tf_op jit(solution)/shard_map/all_to_all | solution.py:353
  138.8 11.2 %mix.1 = bf16[512,2048]{1,0:T(8,128)(2,1)} custom-call(bf16[8,512,128]{2,1,0:T(8,128)(2,1)S(1)} %bitcast.12, bf16[8,512,128]{2,1,0:T(8,128)(2,1)S(1)} %bitcast.11, bf16[1,1024]{1,0:T(2,128)(2,1)S(1)} %slice_bitcast_fusion.gain_ref, bf16[16,8,272,128]{3,2,1,0:T(8,128)(2,1)} %bitcast.20), custom_call_target="tpu_custom_call" | custom-call | flops 4294967296 | bytes 8912896 | tf_op jit(solution)/shard_map/mix/pallas_call | solution.py:273
  (23 shorter events, 1.8 us)
Async XLA Ops:
  7.2 115.8 %all-gather.2.cloned.1.call-start = ((), (), s32[]{:S(2)}) async-start(), calls=%async_computation.3 | async-start | bytes 8982528 | tf_op jit(solution)/shard_map/all_gather | solution.py:328
  13.4 39.2 %all-to-all-start = ((bf16[16,128,512]{2,1,0:T(8,128)(2,1)}), bf16[16,128,512]{2,1,0:T(8,128)(2,1)}, u32[]{:S(2)}, u32[]{:S(2)}) async-start(bf16[16,128,512]{2,1,0:T(8,128)(2,1)} %broadcast_in_dim.4), calls=%async_computation | async-start | bytes 4194304 | tf_op jit(solution)/shard_map/all_to_all | solution.py:334
  52.3 30.4 %copy-start = (f32[2]{0:T(128)S(1)}, f32[2]{0:T(128)}, u32[]{:S(2)}) copy-start(f32[2]{0:T(128)} %sink_ref.1) | copy-start | bytes 28
  52.3 51.1 %copy-start.1 = (bf16[31,128]{1,0:T(8,128)(2,1)S(1)}, bf16[31,128]{1,0:T(8,128)(2,1)}, u32[]{:S(2)}) copy-start(bf16[31,128]{1,0:T(8,128)(2,1)} %param.19) | copy-start | bytes 23812
  67.2 7.1 %collective-permute-start.1 = (bf16[4,144,128]{2,1,0:T(8,128)(2,1)S(1)}, bf16[4,144,128]{2,1,0:T(8,128)(2,1)S(1)}, u32[]{:S(2)}, u32[]{:S(2)}) collective-permute-start(bf16[4,144,128]{2,1,0:T(8,128)(2,1)S(1)} %pad_maximum_fusion.1), channel_id=1, source_target_pairs={{8,0},{16,8},{24,16},{32,24},{40,32},{48,40},{56,48},{64,56},{72,6... | collective-permute-start | bytes 442376 | tf_op jit(solution)/shard_map/ppermute | solution.py:348
  71.6 11.2 %collective-permute-start = (bf16[4,144,128]{2,1,0:T(8,128)(2,1)S(1)}, bf16[4,144,128]{2,1,0:T(8,128)(2,1)S(1)}, u32[]{:S(2)}, u32[]{:S(2)}) collective-permute-start(bf16[4,144,128]{2,1,0:T(8,128)(2,1)S(1)} %pad_maximum_fusion), channel_id=1, source_target_pairs={{0,8},{8,16},{16,24},{24,32},{32,40},{40,48},{48,56},{56,64},{64,7... | collective-permute-start | bytes 442376 | tf_op jit(solution)/shard_map/ppermute | solution.py:347
  98.3 21.1 %all-to-all-start.2 = ((bf16[8,4,128,128]{3,2,1,0:T(8,128)(2,1)}), bf16[8,4,128,128]{3,2,1,0:T(8,128)(2,1)S(1)}, u32[]{:S(2)}, u32[]{:S(2)}) async-start(bf16[8,4,128,128]{3,2,1,0:T(8,128)(2,1)} %get-tuple-element.10), calls=%async_computation.2 | async-start | bytes 2097152 | tf_op jit(solution)/shard_map/all_to_all | solution.py:357
  119.4 19.4 %all-to-all-start.1 = ((bf16[8,4,128,128]{3,2,1,0:T(8,128)(2,1)}), bf16[8,4,128,128]{3,2,1,0:T(8,128)(2,1)S(1)}, u32[]{:S(2)}, u32[]{:S(2)}) async-start(bf16[8,4,128,128]{3,2,1,0:T(8,128)(2,1)} %conv.1), calls=%async_computation.1 | async-start | bytes 2097152 | tf_op jit(solution)/shard_map/all_to_all | solution.py:353
Sparse Core Ops, SparseCore 0:
  10.9 84.9 all-gather.1
where the time goes:
time: 158 us; the launch traced here: 157 us
  Pallas kernels  67.1 us (42%)
  waiting for transfers between devices  34.7 us (22%)
  starting transfers between devices  22.9 us (14%)
  local copies, waits for them, and re-layouts  14.5 us (9%)
  between operations  14.2 us (9%)
  other arithmetic  3.41 us (2%)
    pallas_call x1, Pallas kernels, norm_tokens(): pl.pallas_call(norm_kernel, grid=(rows // block,), in_specs=[pl.BlockSpec...  20.1 us
    pallas_call x1, Pallas kernels, attend(): pl.pallas_call(attend_kernel, grid=(seqs, length // Q_BLOCK), in_specs=[s...  15.5 us
    all_to_all x1, waiting for transfers between devices, on_device(): conv_tok = lax.all_to_all(filtered, 'tp', 0, 0, tiled=True)  15.1 us
    pallas_call x1, Pallas kernels, project(): pl.pallas_call(project_kernel, grid=(rows // block,), in_specs=[pl.BlockS...  14.6 us
    pallas_call x1, Pallas kernels, mix(): pl.pallas_call(mix_kernel, grid=(groups // cols,), in_specs=[whole, whole...  11.2 us
    all_to_all x1, waiting for transfers between devices, on_device(): attn_tok = lax.all_to_all(attn, 'tp', 0, 0, tiled=True)  10.3 us
    ppermute x1, waiting for transfers between devices, on_device(): before = lax.ppermute(high, 'sp', up)  8.51 us
    all_to_all x1, starting transfers between devices, on_device(): lax.all_to_all(jnp.broadcast_to(in_piece[None], (sp, *in_piece.shape)), '...  7.9 us
  transfers between devices with their start and end apart: 6, of which 5 were waited for; matrix products, arithmetic and copies ran while one was open for 10% of the time, Pallas kernels for 36%

commit v1 on v0

v1 whole, which is shorter than its diff:
```python
import functools

import jax
import jax.numpy as jnp
from jax import lax
from jax.experimental import pallas as pl
from jax.experimental.pallas import tpu as pltpu
from jax.sharding import PartitionSpec as P

HEAD_DIM = 64
WINDOW = 128
EPSILON = 1e-06
ROPE_BASE = 10000.0
MASK_VALUE = -1e30
LANES = 128
EDGE = 16
Q_BLOCK = 128
BF16 = jnp.bfloat16
F32 = jnp.float32


def in_hbm(value):
    return pltpu.with_memory_space_constraint(value, pltpu.HBM)


def params(*semantics, mb=48):
    return pltpu.CompilerParams(
        dimension_semantics=semantics, vmem_limit_bytes=mb * 1024 * 1024
    )


def norm_kernel(x_ref, gain_ref, out_ref):
    x = x_ref[...].astype(F32)
    mean = jnp.mean(x, axis=-1, keepdims=True)
    centred = x - mean
    variance = jnp.mean(centred * centred, axis=-1, keepdims=True)
    scaled = centred * lax.rsqrt(variance + EPSILON) * gain_ref[...].astype(F32)
    out_ref[...] = scaled.astype(BF16)


def norm_tokens(x, gain, block=512):
    rows, width = x.shape
    block = min(block, rows)
    return pl.pallas_call(
        norm_kernel,
        grid=(rows // block,),
        in_specs=[
            pl.BlockSpec((block, width), lambda i: (i, 0)),
            pl.BlockSpec((1, width), lambda i: (0, 0)),
        ],
        out_specs=pl.BlockSpec((block, width), lambda i: (i, 0)),
        out_shape=pltpu.HBM((rows, width), BF16),
        compiler_params=params("arbitrary", mb=28),
        cost_estimate=pl.CostEstimate(
            flops=40 * rows * width, transcendentals=rows, bytes_accessed=4 * rows * width
        ),
        name="norm_tokens",
    )(in_hbm(x), gain.reshape(1, width))


def project_kernel(
    x_ref, edge_ref, w_ref, taps_ref, cos_ref, sin_ref, out_ref, q_ref, kv_ref, buf_ref, *, sub, chunk
):
    step = pl.program_id(0)
    dests, _, share, _ = out_ref.shape
    length, seqs = dests * share, edge_ref.shape[0]
    half = HEAD_DIM // 2
    tap_count = taps_ref.shape[0]
    shift = EDGE - tap_count // 2
    slot, last = step % 2, (step + 1) % 2

    def gate(raw):
        return raw[:, :LANES] * jax.nn.sigmoid(raw[:, LANES : 2 * LANES])

    def filter_rows(first):
        for at in range(first, first + sub, chunk):
            total = jnp.zeros((chunk, LANES), F32)
            for tap in range(tap_count):
                rows = buf_ref[last, at + shift + tap : at + shift + tap + chunk, :]
                total = total + rows * taps_ref[tap : tap + 1, :]
            out_ref[at // share, 0, at % share : at % share + chunk, :] = total.astype(BF16)

    @pl.when(step < seqs)
    def _():
        weight = w_ref[...].reshape(-1, w_ref.shape[2])
        low = (lax.broadcasted_iota(jnp.int32, (sub, LANES), 1) % HEAD_DIM) < half
        ends = gate(
            jnp.dot(edge_ref[step], weight[:, : 2 * LANES], preferred_element_type=F32)
        ).astype(BF16).astype(F32)
        buf_ref[slot, 0:EDGE, :] = ends[:EDGE]
        buf_ref[slot, EDGE + length : 2 * EDGE + length, :] = ends[EDGE:]
        for first in range(0, length, sub):
            raw = jnp.dot(x_ref[first : first + sub, :], weight, preferred_element_type=F32)
            filter_rows(first)
            buf_ref[slot, EDGE + first : EDGE + first + sub, :] = (
                gate(raw).astype(BF16).astype(F32)
            )
            table = slice(first, first + sub)
            for part, ref, scale in ((2, q_ref, HEAD_DIM**-0.5), (3, kv_ref, None)):
                x = raw[:, part * LANES : (part + 1) * LANES]
                partner = jnp.where(low, pltpu.roll(x, LANES - half, 1), pltpu.roll(x, half, 1))
                at = slice((part - 2) * LANES, (part - 1) * LANES)
                turned = x * cos_ref[table, at] + partner * sin_ref[table, at]
                if scale is not None:
                    turned = turned * scale
                ref[0, table, :] = turned.astype(BF16)

    @pl.when(step == seqs)
    def _():
        for first in range(0, length, sub):
            filter_rows(first)


def project(normed, edges, weight, taps, cosine, sine, dests, sub=256, chunk=32):
    seqs = edges.shape[0]
    rows, width = normed.shape
    length = rows // seqs
    inside = pl.BlockSpec(memory_space=pltpu.VMEM)
    heads = pltpu.HBM((seqs, length, LANES), BF16)
    head_block = pl.BlockSpec((1, length, LANES), lambda s: (jnp.minimum(s, seqs - 1), 0, 0))
    return pl.pallas_call(
        functools.partial(project_kernel, sub=sub, chunk=chunk),
        grid=(seqs + 1,),
        in_specs=[pl.BlockSpec((length, width), lambda s: (jnp.minimum(s, seqs - 1), 0))]
        + [inside] * 5,
        out_specs=[
            pl.BlockSpec(
                (dests, 1, length // dests, LANES), lambda s: (0, jnp.maximum(s - 1, 0), 0, 0)
            ),
            head_block,
            head_block,
        ],
        out_shape=[
            jax.ShapeDtypeStruct((dests, seqs, length // dests, LANES), BF16), heads, heads
        ],
        scratch_shapes=[pltpu.VMEM((2, length + 2 * EDGE, LANES), F32)],
        compiler_params=params("arbitrary", mb=28),
        cost_estimate=pl.CostEstimate(
            flops=2 * rows * width * weight.shape[2],
            transcendentals=0,
            bytes_accessed=2 * rows * width,
        ),
        name="project",
    )(in_hbm(normed), edges, weight, taps, cosine, sine)


def attend_kernel(
    place_ref, sink_ref, q_ref, before_ref, kv_ref, after_ref, out_ref, log_ref,
    pad_ref, one_ref, bias_ref,
):
    length = kv_ref.shape[1]
    blocks = length // Q_BLOCK
    span = Q_BLOCK + 2 * WINDOW

    @pl.when(pl.program_id(0) == 0)
    def _():
        query = lax.broadcasted_iota(jnp.int32, (Q_BLOCK, span), 0)
        key = lax.broadcasted_iota(jnp.int32, (Q_BLOCK, span), 1)
        band = (key >= query) & (key <= query + 2 * WINDOW)
        first = jnp.where(place_ref[0] == 0, WINDOW, 0)
        last = jnp.where(place_ref[0] == place_ref[1] - 1, Q_BLOCK + WINDOW, span)
        zero, out = jnp.zeros(band.shape, F32), jnp.full(band.shape, MASK_VALUE, F32)
        bias_ref[0] = jnp.where(band, zero, out)
        bias_ref[1] = jnp.where(band & (key >= first), zero, out)
        bias_ref[2] = jnp.where(band & (key < last), zero, out)

    pad_ref[0:WINDOW, :] = before_ref[0]
    pad_ref[WINDOW : WINDOW + length, :] = kv_ref[0]
    pad_ref[WINDOW + length : 2 * WINDOW + length, :] = after_ref[0]
    padded = pad_ref[...]
    in_low = lax.broadcasted_iota(jnp.int32, padded.shape, 1) < HEAD_DIM
    one_ref[...] = jnp.where(in_low, jnp.ones_like(padded), padded)

    low = lax.broadcasted_iota(jnp.int32, (Q_BLOCK, LANES), 1) < HEAD_DIM
    low_both = lax.broadcasted_iota(jnp.int32, (2 * Q_BLOCK, LANES), 1) < HEAD_DIM
    diagonal = lax.broadcasted_iota(jnp.int32, (LANES, LANES), 0) == lax.broadcasted_iota(
        jnp.int32, (LANES, LANES), 1
    )
    is_first = lax.broadcasted_iota(jnp.int32, (2 * Q_BLOCK, 1), 0) < Q_BLOCK
    sink = jnp.where(is_first, sink_ref[0], sink_ref[1])

    def score(block):
        at = block * Q_BLOCK
        keys = pad_ref[at : at + span, :]
        bias = bias_ref[1 if block == 0 else 2 if block == blocks - 1 else 0]
        query = q_ref[0, at : at + Q_BLOCK, :]
        swapped = pltpu.roll(query.astype(F32), HEAD_DIM, 1).astype(BF16)
        own = jnp.concatenate([query, swapped], 0)
        own = jnp.where(low_both, own, jnp.zeros_like(own))
        scores = lax.dot_general(
            own, keys, (((1,), (1,)), ((), ())), preferred_element_type=F32
        )
        return scores + jnp.concatenate([bias, bias], 0)

    def weigh(block, scores):
        top = jnp.maximum(jnp.max(scores, axis=-1, keepdims=True), sink)
        return top, jnp.exp(scores - top).astype(BF16)

    def blend(block, top, weights):
        at = block * Q_BLOCK
        both = jnp.dot(weights, one_ref[at : at + span, :], preferred_element_type=F32)
        swapped = pltpu.roll(both, HEAD_DIM, 1)
        total = jnp.where(low_both, both, swapped) + jnp.exp(sink - top)
        log_total = top + jnp.log(total)
        for head in range(2):
            log_ref[0, head : head + 1, at : at + Q_BLOCK] = jnp.sum(
                jnp.where(diagonal, log_total[head * Q_BLOCK : (head + 1) * Q_BLOCK], 0.0),
                axis=0,
                keepdims=True,
            )
        first = swapped[:Q_BLOCK] / total[:Q_BLOCK]
        second = both[Q_BLOCK:] / total[Q_BLOCK:]
        out_ref[block, 0] = jnp.where(low, first, second).astype(BF16)

    ahead, behind = score(0), None
    for block in range(blocks):
        scores = ahead
        if block + 1 < blocks:
            ahead = score(block + 1)
        top, weights = weigh(block, scores)
        if behind is not None:
            blend(block - 1, *behind)
        behind = top, weights
    blend(blocks - 1, *behind)


def attend(place, sink, query, before, kv, after, dests):
    seqs, length, _ = kv.shape
    span = Q_BLOCK + 2 * WINDOW
    edge = pl.BlockSpec((1, WINDOW, LANES), lambda s: (s, 0, 0))
    whole = pl.BlockSpec((1, length, LANES), lambda s: (s, 0, 0))
    smem = pl.BlockSpec(memory_space=pltpu.SMEM)
    return pl.pallas_call(
        attend_kernel,
        grid=(seqs,),
        in_specs=[smem, smem, whole, edge, whole, edge],
        out_specs=[
            pl.BlockSpec((dests, 1, length // dests, LANES), lambda s: (0, s, 0, 0)),
            pl.BlockSpec((1, 2, length), lambda s: (s, 0, 0)),
        ],
        out_shape=[
            jax.ShapeDtypeStruct((dests, seqs, length // dests, LANES), BF16),
            jax.ShapeDtypeStruct((seqs, 2, length), F32),
        ],
        scratch_shapes=[
            pltpu.VMEM((length + 2 * WINDOW, LANES), BF16),
            pltpu.VMEM((length + 2 * WINDOW, LANES), BF16),
            pltpu.VMEM((3, Q_BLOCK, span), F32),
        ],
        compiler_params=params("arbitrary"),
        cost_estimate=pl.CostEstimate(
            flops=40 * seqs * length * span * LANES // 8,
            transcendentals=0,
            bytes_accessed=6 * seqs * length * LANES,
        ),
        name="attend",
    )(place, sink, in_hbm(query), before, in_hbm(kv), after)


def side_by_side(ref):
    return jnp.concatenate([ref[i] for i in range(ref.shape[0])], axis=-1)


def columns(ref):
    return jnp.concatenate([ref[c].reshape(-1, LANES) for c in range(ref.shape[0])], axis=-1)


def mix_conv_kernel(x_ref, gain_ref, w_ref, out_ref, act_ref):
    @pl.when(pl.program_id(0) == 0)
    def _():
        x = side_by_side(x_ref).astype(F32)
        gain = side_by_side(gain_ref)[0:1].astype(F32)
        mean = jnp.mean(x, axis=-1, keepdims=True)
        centred = x - mean
        variance = jnp.mean(centred * centred, axis=-1, keepdims=True)
        v = centred * lax.rsqrt(variance + EPSILON) * gain
        act_ref[...] = (v / (1.0 + jnp.exp(-v))).astype(BF16)

    out_ref[...] = jnp.dot(act_ref[...], columns(w_ref), preferred_element_type=F32)


def mix_attn_kernel(x_ref, part_ref, w_ref, out_ref):
    total = part_ref[...] + jnp.dot(
        side_by_side(x_ref), columns(w_ref), preferred_element_type=F32
    )
    out_ref[...] = total.astype(BF16)


def mix(kernel, x, extra, weight, which, out_dtype, cols, name, scratch=()):
    sources, rows, _ = x.shape
    groups = weight.shape[0]
    block = pl.BlockSpec((rows, cols * LANES), lambda n: (0, n))
    if which == 0:
        place = weight.shape[2] // EDGE - 1
        extra_spec = pl.BlockSpec((None, sources, EDGE, LANES), lambda n: (0, 0, place, 0))
    else:
        extra_spec = block
    return pl.pallas_call(
        kernel,
        grid=(groups // cols,),
        in_specs=[
            pl.BlockSpec(x.shape, lambda n: (0, 0, 0)),
            extra_spec,
            pl.BlockSpec((cols, sources, LANES, LANES), lambda n: (n, 0, which, 0)),
        ],
        out_specs=block,
        out_shape=pltpu.HBM((rows, groups * LANES), out_dtype),
        scratch_shapes=list(scratch),
        compiler_params=params("arbitrary", mb=32),
        cost_estimate=pl.CostEstimate(
            flops=2 * rows * sources * LANES * groups * LANES,
            transcendentals=0,
            bytes_accessed=weight.size,
        ),
        name=name,
    )(x, extra, weight)


def pack_kernel(
    value_ref, gate_ref, query_ref, key_ref, kv_ref, conv_ref, attn_ref, gain_ref, out_ref, in_ref
):
    out_ref[0:LANES, :] = conv_ref[...]
    out_ref[LANES : 2 * LANES, :] = attn_ref[...]
    out_ref[2 * LANES :, :] = jnp.broadcast_to(gain_ref[...].astype(F32), (EDGE, LANES)).astype(BF16)
    both = jnp.concatenate([key_ref[...], kv_ref[...]], 0).astype(F32).T.astype(BF16)
    piece = jnp.concatenate([value_ref[...], gate_ref[...], query_ref[...], both], axis=1)
    for copy in range(in_ref.shape[0]):
        in_ref[copy] = piece


def pack(value, gate, query, key, kv, conv, attn, gain, copies):
    rows = value.shape[0]
    cols = 3 * LANES + 2 * key.shape[1]
    return pl.pallas_call(
        pack_kernel,
        out_shape=[
            jax.ShapeDtypeStruct((2 * LANES + EDGE, LANES), BF16),
            jax.ShapeDtypeStruct((copies, rows, cols), BF16),
        ],
        compiler_params=pltpu.CompilerParams(vmem_limit_bytes=16 * 1024 * 1024),
        name="pack",
    )(value, gate, query, key.T, kv.T, conv, attn, gain.reshape(1, LANES))


def turn_tables(tok_count):
    half = HEAD_DIM // 2
    offset = lax.axis_index("sp") * tok_count
    positions = (offset + jnp.arange(tok_count, dtype=jnp.int32)).astype(F32)
    lane = jnp.arange(2 * LANES, dtype=jnp.int32)
    inverse = ROPE_BASE ** (-(lane % half).astype(F32) / half)
    angles = positions[:, None] * inverse[None, :]
    turns = (lane < LANES + HEAD_DIM)[None, :]
    sign = jnp.where(lane % HEAD_DIM < half, -1.0, 1.0).astype(F32)[None, :]
    return jnp.where(turns, jnp.cos(angles), 1.0), jnp.where(turns, jnp.sin(angles) * sign, 0.0)


def on_device(
    tokens,
    norm_gain,
    conv_value_weight,
    conv_gate_weight,
    query_weight,
    key_weight,
    value_weight,
    conv_taps,
    conv_gain,
    sink_logit,
    out_conv_weight,
    out_attn_weight,
):
    seqs, length, width = tokens.shape
    sp, tp = lax.axis_size("sp"), lax.axis_size("tp")
    place = jnp.stack([lax.axis_index("sp"), jnp.int32(sp)]).astype(jnp.int32)
    up = [(i, i + 1) for i in range(sp - 1)]
    down = [(i + 1, i) for i in range(sp - 1)]

    out_piece, in_piece = pack(
        conv_value_weight, conv_gate_weight, query_weight, key_weight, value_weight,
        out_conv_weight, out_attn_weight, conv_gain, sp,
    )
    out_weight = lax.all_gather(out_piece, ("sp", "tp"), axis=0, tiled=True)
    out_weight = out_weight.reshape(sp, tp, out_piece.shape[0], LANES)
    in_weight = lax.all_to_all(in_piece, "sp", 0, 0, tiled=True)

    before = lax.ppermute(tokens[:, -EDGE:], "sp", up)
    after = lax.ppermute(tokens[:, :EDGE], "sp", down)
    normed = norm_tokens(tokens.reshape(seqs * length, width), norm_gain)
    edges = norm_tokens(
        jnp.concatenate([before, after], axis=1).reshape(2 * seqs * EDGE, width), norm_gain
    ).reshape(seqs, 2 * EDGE, width)
    cosine, sine = turn_tables(length)
    filtered, query, kv = project(
        normed, edges, in_weight, conv_taps.astype(F32), cosine, sine, tp
    )

    before = lax.ppermute(kv[:, -WINDOW:], "sp", up)
    after = lax.ppermute(kv[:, :WINDOW], "sp", down)
    conv_tok = lax.all_to_all(filtered, "tp", 0, 0, tiled=True)
    attn, log_total = attend(place, sink_logit, query, before, kv, after, tp)
    attn_tok = lax.all_to_all(attn, "tp", 0, 0, tiled=True)

    rows = seqs * length // tp
    out_weight = in_hbm(out_weight)
    part = mix(
        mix_conv_kernel, conv_tok.reshape(tp, rows, LANES), out_weight, out_weight, 0, F32, 4,
        "mix_conv", [pltpu.VMEM((rows, tp * LANES), BF16)],
    )
    mixed = mix(
        mix_attn_kernel, attn_tok.reshape(tp, rows, LANES), in_hbm(part), out_weight, 1, BF16, 8, "mix_attn"
    )
    return mixed.reshape(seqs, length // tp, width), log_total


def solution(mesh):
    placed = (
        P(None, "sp", None),
        P(),
        P("sp", "tp"),
        P("sp", "tp"),
        P("sp", "tp"),
        P("sp", "tp"),
        P("sp", "tp"),
        P(None, "tp"),
        P("tp"),
        P("tp"),
        P("tp", "sp"),
        P("tp", "sp"),
    )
    return jax.shard_map(
        on_device,
        mesh=mesh,
        in_specs=placed,
        out_specs=(P(None, ("sp", "tp"), None), P(None, "tp", "sp")),
        check_vma=False,
    )
```

time: 158 us -> 146 us (0.924)
  the two profiles are of different devices: /device:TPU:32 before, /device:TPU:1 now
where the time goes in v1:
time: 146 us; the launch traced here: 144 us
  Pallas kernels  61.6 us (42%)
  starting transfers between devices  27.7 us (19%)
  waiting for transfers between devices  21 us (14%)
  between operations  14.1 us (10%)
  local copies, waits for them, and re-layouts  11.7 us (8%)
  other arithmetic  7.47 us (5%)
    pallas_call x2, Pallas kernels, norm_tokens(): pl.pallas_call(norm_kernel, grid=(rows // block,), in_specs=[pl.BlockSpec...  19.4 us
    pallas_call x1, Pallas kernels, project(): pl.pallas_call(functools.partial(project_kernel, sub=sub, chunk=chunk), g...  18.2 us
    pallas_call x2, Pallas kernels, mix(): pl.pallas_call(kernel, grid=(groups // cols,), in_specs=[pl.BlockSpec(x.s...  13 us
    pallas_call x1, Pallas kernels, attend(): pl.pallas_call(attend_kernel, grid=(seqs,), in_specs=[smem, smem, whole,...  9.46 us
    all_to_all x1, starting transfers between devices, on_device(): in_weight = lax.all_to_all(in_piece, 'sp', 0, 0, tiled=True)  8.43 us
    unnamed x22, local copies, waits for them, and re-layouts  8.14 us
    all_to_all x1, waiting for transfers between devices, on_device(): attn_tok = lax.all_to_all(attn, 'tp', 0, 0, tiled=True)  7.69 us
    all_to_all x1, starting transfers between devices, on_device(): conv_tok = lax.all_to_all(filtered, 'tp', 0, 0, tiled=True)  6.13 us
  transfers between devices with their start and end apart: 8, of which 6 were waited for; matrix products, arithmetic and copies ran while one was open for 8% of the time, Pallas kernels for 38%

profile of v1, /device:TPU:1, one launch (start us, length us, event | category | flops | bytes accessed | tf_op | source)
XLA Modules:
  0.0 143.6 jit_solution(14337359231004341782)
XLA Ops:
  13.1 1.5 %pack.1 = (bf16[272,128]{1,0:T(8,128)(2,1)}, bf16[16,128,512]{2,1,0:T(8,128)(2,1)}) custom-call(bf16[128,128]{1,0:T(8,128)(2,1)S(1)} %copy-done.2, bf16[128,128]{1,0:T(8,128)(2,1)S(1)} %copy-done.3, bf16[128,128]{1,0:T(8,128)(2,1)S(1)} %copy-done.4, bf16[64,128]{1,0:T(8,128)(2,1)S(1)} %bitcast.14, bf16[64,128]{1,0:T(8,128)(2,1)S(1)} %bitcast.15, ...), custom_call_target="tpu_custom_call" | custom-call | tf_op jit(solution)/shard_map/pack/pallas_call | solution.py:334
  14.7 8.4 %all-to-all-start = ((bf16[16,128,512]{2,1,0:T(8,128)(2,1)}), bf16[16,128,512]{2,1,0:T(8,128)(2,1)S(1)}, u32[]{:S(2)}, u32[]{:S(2)}) async-start(bf16[16,128,512]{2,1,0:T(8,128)(2,1)} %get-tuple-element.9), calls=%async_computation | async-start | bytes 4194304 | tf_op jit(solution)/shard_map/all_to_all | solution.py:383
  23.1 1.9 %fusion.7 = (bf16[4,16,2048]{2,1,0:T(8,128)(2,1)}, bf16[4,16,2048]{2,1,0:T(8,128)(2,1)}) fusion(bf16[4,1024,2048]{2,1,0:T(8,128)(2,1)} %param.12), kind=kLoop, calls=%fused_computation.16 | loop fusion | bytes 1048576 | tf_op jit(solution)/shard_map/slice | solution.py:385
  25.0 3.3 %collective-permute-start = (bf16[4,16,2048]{2,1,0:T(8,128)(2,1)}, bf16[4,16,2048]{2,1,0:T(8,128)(2,1)S(1)}, u32[]{:S(2)}, u32[]{:S(2)}) collective-permute-start(bf16[4,16,2048]{2,1,0:T(8,128)(2,1)} %get-tuple-element.16), channel_id=1, source_target_pairs={{0,8},{8,16},{16,24},{24,32},{32,40},{40,48},{48,56},{56,64},{64,7... | collective-permute-start | bytes 786440 | tf_op jit(solution)/shard_map/ppermute | solution.py:385
  28.3 1.3 collective-permute-start.1
  31.0 17.2 %norm_tokens.2.x_ref = bf16[4096,2048]{1,0:T(8,128)(2,1)} custom-call(bf16[4096,2048]{1,0:T(8,128)(2,1)} %bitcast.20, bf16[1,2048]{1,0:T(2,128)(2,1)S(1)} %reshape.66.gain_ref), custom_call_target="tpu_custom_call" | custom-call | flops 335544320 | bytes 33554432 | tf_op jit(solution)/shard_map/norm_tokens/pallas_call | solution.py:44
  48.2 4.8 %fusion.2 = (f32[1024,256]{1,0:T(8,128)S(1)}, f32[1024,256]{1,0:T(8,128)}) fusion(f32[256]{0:T(256)S(1)} %get-tuple-element.22, f32[256]{0:T(256)S(1)} %get-tuple-element.23, f32[1024]{0:T(1024)S(1)} %add_convert_fusion, pred[256]{0:T(512)(128)(4,1)S(1)} %iota_compare_fusion), kind=kLoop, calls=%fused_computation.4 | loop fusion | flops 1048576 | bytes 2103552 | tf_op jit(solution)/shard_map/jit(_where)/select_n | solution.py:354
  53.1 2.3 %collective-permute-done = bf16[4,16,2048]{2,1,0:T(8,128)(2,1)S(1)} collective-permute-done((bf16[4,16,2048]{2,1,0:T(8,128)(2,1)}, bf16[4,16,2048]{2,1,0:T(8,128)(2,1)S(1)}, u32[]{:S(2)}, u32[]{:S(2)}) %collective-permute-start) | collective-permute-done | bytes 262176 | tf_op jit(solution)/shard_map/ppermute | solution.py:385
  55.4 1.8 %collective-permute-done.1 = bf16[4,16,2048]{2,1,0:T(8,128)(2,1)} collective-permute-done((bf16[4,16,2048]{2,1,0:T(8,128)(2,1)}, bf16[4,16,2048]{2,1,0:T(8,128)(2,1)}, u32[]{:S(2)}, u32[]{:S(2)}) %collective-permute-start.1) | collective-permute-done | bytes 262176 | tf_op jit(solution)/shard_map/ppermute | solution.py:386
  57.1 1.8 %pad_maximum_fusion = bf16[4,32,2048]{2,1,0:T(8,128)(2,1)} fusion(bf16[4,16,2048]{2,1,0:T(8,128)(2,1)} %collective-permute-done.1, bf16[4,16,2048]{2,1,0:T(8,128)(2,1)S(1)} %collective-permute-done), kind=kLoop, calls=%fused_computation.5 | loop fusion | flops 1048576 | bytes 1048576 | tf_op jit(solution)/shard_map/concatenate | solution.py:389
  59.0 2.2 %norm_tokens.3 = bf16[128,2048]{1,0:T(8,128)(2,1)} custom-call(bf16[128,2048]{1,0:T(8,128)(2,1)} %bitcast.21, bf16[1,2048]{1,0:T(2,128)(2,1)S(1)} %reshape.66.gain_ref), custom_call_target="tpu_custom_call" | custom-call | flops 10485760 | bytes 1048576 | tf_op jit(solution)/shard_map/norm_tokens/pallas_call | solution.py:44
  61.2 1.2 copy-done
  62.4 1.0 copy-done.1
  63.5 18.2 %project.1 = (bf16[8,4,128,128]{3,2,1,0:T(8,128)(2,1)}, bf16[4,1024,128]{2,1,0:T(8,128)(2,1)}, bf16[4,1024,128]{2,1,0:T(8,128)(2,1)}) custom-call(bf16[4096,2048]{1,0:T(8,128)(2,1)} %norm_tokens.2.x_ref, bf16[4,32,2048]{2,1,0:T(8,128)(2,1)S(1)} %bitcast.13, bf16[16,128,512]{2,1,0:T(8,128)(2,1)S(1)} %all-to-all-done.w_ref, ...), custom_call_target="tpu_custom_call" | custom-call | flops 8589934592 | bytes 16777216 | tf_op jit(solution)/shard_map/project/pallas_call | solution.py:121
  81.6 6.1 %all-to-all-start.2 = ((bf16[8,4,128,128]{3,2,1,0:T(8,128)(2,1)}), bf16[8,4,128,128]{3,2,1,0:T(8,128)(2,1)S(1)}, u32[]{:S(2)}, u32[]{:S(2)}) async-start(bf16[8,4,128,128]{3,2,1,0:T(8,128)(2,1)} %get-tuple-element.13), calls=%async_computation.2 | async-start | bytes 2097152 | tf_op jit(solution)/shard_map/all_to_all | solution.py:398
  88.8 2.1 %collective-permute-start.2 = (bf16[4,128,128]{2,1,0:T(8,128)(2,1)S(1)}, bf16[4,128,128]{2,1,0:T(8,128)(2,1)S(1)}, u32[]{:S(2)}, u32[]{:S(2)}) collective-permute-start(bf16[4,128,128]{2,1,0:T(8,128)(2,1)S(1)} %get-tuple-element.19), channel_id=1, source_target_pairs={{0,8},{8,16},{16,24},{24,32},{32,40},{40,48},{48,56},{56,64},{64,7... | collective-permute-start | bytes 393224 | tf_op jit(solution)/shard_map/ppermute | solution.py:396
  90.9 1.3 collective-permute-start.3
  92.3 4.3 %collective-permute-done.2.before_ref = bf16[4,128,128]{2,1,0:T(8,128)(2,1)S(1)} collective-permute-done((bf16[4,128,128]{2,1,0:T(8,128)(2,1)S(1)}, bf16[4,128,128]{2,1,0:T(8,128)(2,1)S(1)}, u32[]{:S(2)}, u32[]{:S(2)}) %collective-permute-start.2) | collective-permute-done | bytes 131104 | tf_op jit(solution)/shard_map/ppermute | solution.py:396
  96.6 4.0 %collective-permute-done.3.after_ref = bf16[4,128,128]{2,1,0:T(8,128)(2,1)S(1)} collective-permute-done((bf16[4,128,128]{2,1,0:T(8,128)(2,1)S(1)}, bf16[4,128,128]{2,1,0:T(8,128)(2,1)S(1)}, u32[]{:S(2)}, u32[]{:S(2)}) %collective-permute-start.3) | collective-permute-done | bytes 131104 | tf_op jit(solution)/shard_map/ppermute | solution.py:397
  100.5 9.5 %attend.1 = (bf16[8,4,128,128]{3,2,1,0:T(8,128)(2,1)}, f32[4,2,1024]{2,1,0:T(2,128)}) custom-call(s32[2]{0:T(128)S(1)} %pad_add_fusion.place_ref, f32[2]{0:T(128)S(1)} %copy-done.10, bf16[4,1024,128]{2,1,0:T(8,128)(2,1)} %get-tuple-element.10.q_ref, bf16[4,128,128]{2,1,0:T(8,128)(2,1)S(1)} %collective-permute-done.2.before_ref, ...), custom_call_target="tpu_custom_call" | custom-call | flops 1006632960 | bytes 3145728 | tf_op jit(solution)/shard_map/attend/pallas_call | solution.py:233
  110.9 5.2 %all-to-all-start.1 = ((bf16[8,4,128,128]{3,2,1,0:T(8,128)(2,1)}), bf16[8,4,128,128]{3,2,1,0:T(8,128)(2,1)S(1)}, u32[]{:S(2)}, u32[]{:S(2)}) async-start(bf16[8,4,128,128]{3,2,1,0:T(8,128)(2,1)} %get-tuple-element.12), calls=%async_computation.1 | async-start | bytes 2097152 | tf_op jit(solution)/shard_map/all_to_all | solution.py:400
  116.1 7.3 %mix_conv.1.part_ref = f32[512,2048]{1,0:T(8,128)} custom-call(bf16[8,512,128]{2,1,0:T(8,128)(2,1)S(1)} %bitcast.11, bf16[16,8,272,128]{3,2,1,0:T(8,128)(2,1)} %bitcast.17, bf16[16,8,272,128]{3,2,1,0:T(8,128)(2,1)} %bitcast.18), custom_call_target="tpu_custom_call" | custom-call | flops 2147483648 | bytes 4456448 | tf_op jit(solution)/shard_map/mix_conv/pallas_call | solution.py:298
  123.3 7.7 %all-to-all-done.1 = bf16[8,4,128,128]{3,2,1,0:T(8,128)(2,1)S(1)} async-done(((bf16[8,4,128,128]{3,2,1,0:T(8,128)(2,1)}), bf16[8,4,128,128]{3,2,1,0:T(8,128)(2,1)S(1)}, u32[]{:S(2)}, u32[]{:S(2)}) %all-to-all-start.1) | async-done | bytes 1048608 | tf_op jit(solution)/shard_map/all_to_all | solution.py:400
  131.0 5.7 %mix_attn.1 = bf16[512,2048]{1,0:T(8,128)(2,1)} custom-call(bf16[8,512,128]{2,1,0:T(8,128)(2,1)S(1)} %bitcast.12, f32[512,2048]{1,0:T(8,128)} %mix_conv.1.part_ref, bf16[16,8,272,128]{3,2,1,0:T(8,128)(2,1)} %bitcast.19), custom_call_target="tpu_custom_call" | custom-call | flops 2147483648 | bytes 4456448 | tf_op jit(solution)/shard_map/mix_attn/pallas_call | solution.py:298
  (32 shorter events, 9.3 us)
Async XLA Ops:
  7.2 108.9 %all-gather.2.cloned.1.call-start = ((), (), s32[]{:S(2)}) async-start(), calls=%async_computation.3 | async-start | bytes 8982528 | tf_op jit(solution)/shard_map/all_gather | solution.py:381
  7.2 0.8 copy-start.2
  8.0 0.8 copy-start.3
  8.7 0.8 copy-start.4
  9.5 0.8 copy-start.5
  10.2 0.8 copy-start.6
  11.0 0.7 copy-start.7
  11.7 0.7 copy-start.8
  12.4 0.7 copy-start.9
  14.7 46.5 %all-to-all-start = ((bf16[16,128,512]{2,1,0:T(8,128)(2,1)}), bf16[16,128,512]{2,1,0:T(8,128)(2,1)S(1)}, u32[]{:S(2)}, u32[]{:S(2)}) async-start(bf16[16,128,512]{2,1,0:T(8,128)(2,1)} %get-tuple-element.9), calls=%async_computation | async-start | bytes 4194304 | tf_op jit(solution)/shard_map/all_to_all | solution.py:383
  25.0 30.4 %collective-permute-start = (bf16[4,16,2048]{2,1,0:T(8,128)(2,1)}, bf16[4,16,2048]{2,1,0:T(8,128)(2,1)S(1)}, u32[]{:S(2)}, u32[]{:S(2)}) collective-permute-start(bf16[4,16,2048]{2,1,0:T(8,128)(2,1)} %get-tuple-element.16), channel_id=1, source_target_pairs={{0,8},{8,16},{16,24},{24,32},{32,40},{40,48},{48,56},{56,64},{64,7... | collective-permute-start | bytes 786440 | tf_op jit(solution)/shard_map/ppermute | solution.py:385
  28.3 28.9 %collective-permute-start.1 = (bf16[4,16,2048]{2,1,0:T(8,128)(2,1)}, bf16[4,16,2048]{2,1,0:T(8,128)(2,1)}, u32[]{:S(2)}, u32[]{:S(2)}) collective-permute-start(bf16[4,16,2048]{2,1,0:T(8,128)(2,1)} %get-tuple-element.17), channel_id=1, source_target_pairs={{8,0},{16,8},{24,16},{32,24},{40,32},{48,40},{56,48},{64,56},{72,6... | collective-permute-start | bytes 786440 | tf_op jit(solution)/shard_map/ppermute | solution.py:386
  61.2 1.2 copy-start
  62.4 1.0 copy-start.1
  63.5 37.1 %copy-start.10 = (f32[2]{0:T(128)S(1)}, f32[2]{0:T(128)}, u32[]{:S(2)}) copy-start(f32[2]{0:T(128)} %sink_ref.1) | copy-start | bytes 28
  81.6 29.2 %all-to-all-start.2 = ((bf16[8,4,128,128]{3,2,1,0:T(8,128)(2,1)}), bf16[8,4,128,128]{3,2,1,0:T(8,128)(2,1)S(1)}, u32[]{:S(2)}, u32[]{:S(2)}) async-start(bf16[8,4,128,128]{3,2,1,0:T(8,128)(2,1)} %get-tuple-element.13), calls=%async_computation.2 | async-start | bytes 2097152 | tf_op jit(solution)/shard_map/all_to_all | solution.py:398
  88.8 7.8 %collective-permute-start.2 = (bf16[4,128,128]{2,1,0:T(8,128)(2,1)S(1)}, bf16[4,128,128]{2,1,0:T(8,128)(2,1)S(1)}, u32[]{:S(2)}, u32[]{:S(2)}) collective-permute-start(bf16[4,128,128]{2,1,0:T(8,128)(2,1)S(1)} %get-tuple-element.19), channel_id=1, source_target_pairs={{0,8},{8,16},{16,24},{24,32},{32,40},{40,48},{48,56},{56,64},{64,7... | collective-permute-start | bytes 393224 | tf_op jit(solution)/shard_map/ppermute | solution.py:396
  90.9 9.6 %collective-permute-start.3 = (bf16[4,128,128]{2,1,0:T(8,128)(2,1)S(1)}, bf16[4,128,128]{2,1,0:T(8,128)(2,1)S(1)}, u32[]{:S(2)}, u32[]{:S(2)}) collective-permute-start(bf16[4,128,128]{2,1,0:T(8,128)(2,1)S(1)} %get-tuple-element.18), channel_id=1, source_target_pairs={{8,0},{16,8},{24,16},{32,24},{40,32},{48,40},{56,48},{64,56},{72,6... | collective-permute-start | bytes 393224 | tf_op jit(solution)/shard_map/ppermute | solution.py:397
  110.9 20.1 %all-to-all-start.1 = ((bf16[8,4,128,128]{3,2,1,0:T(8,128)(2,1)}), bf16[8,4,128,128]{3,2,1,0:T(8,128)(2,1)S(1)}, u32[]{:S(2)}, u32[]{:S(2)}) async-start(bf16[8,4,128,128]{3,2,1,0:T(8,128)(2,1)} %get-tuple-element.12), calls=%async_computation.1 | async-start | bytes 2097152 | tf_op jit(solution)/shard_map/all_to_all | solution.py:400
Sparse Core Ops, SparseCore 0:
  14.8 95.8 all-gather.1

commit v2 on v1

--- a/solution.py
+++ b/solution.py
@@ -15,6 +15,7 @@
 LANES = 128
 EDGE = 16
 Q_BLOCK = 128
+SPAN = Q_BLOCK + 2 * WINDOW
 BF16 = jnp.bfloat16
 F32 = jnp.float32
 
@@ -29,13 +30,16 @@
     )
 
 
-def norm_kernel(x_ref, gain_ref, out_ref):
-    x = x_ref[...].astype(F32)
+def normalize(x, gain):
+    x = x.astype(F32)
     mean = jnp.mean(x, axis=-1, keepdims=True)
     centred = x - mean
     variance = jnp.mean(centred * centred, axis=-1, keepdims=True)
-    scaled = centred * lax.rsqrt(variance + EPSILON) * gain_ref[...].astype(F32)
-    out_ref[...] = scaled.astype(BF16)
+    return centred * lax.rsqrt(variance + EPSILON) * gain.astype(F32)
+
+
+def norm_kernel(x_ref, gain_ref, out_ref):
+    out_ref[...] = normalize(x_ref[...], gain_ref[...]).astype(BF16)
 
 
 def norm_tokens(x, gain, block=512):
@@ -59,15 +63,16 @@
 
 
 def project_kernel(
-    x_ref, edge_ref, w_ref, taps_ref, cos_ref, sin_ref, out_ref, q_ref, kv_ref, buf_ref, *, sub, chunk
+    x_ref, before_ref, after_ref, gain_ref, w_ref, taps_ref, cos_ref, sin_ref, out_ref, q_ref, kv_ref, buf_ref, *, sub, chunk
 ):
     step = pl.program_id(0)
     dests, _, share, _ = out_ref.shape
-    length, seqs = dests * share, edge_ref.shape[0]
+    length, seqs = dests * share, before_ref.shape[0]
     half = HEAD_DIM // 2
     tap_count = taps_ref.shape[0]
     shift = EDGE - tap_count // 2
     slot, last = step % 2, (step + 1) % 2
+    taps = taps_ref[...].astype(F32)
 
     def gate(raw):
         return raw[:, :LANES] * jax.nn.sigmoid(raw[:, LANES : 2 * LANES])
@@ -77,15 +82,18 @@
             total = jnp.zeros((chunk, LANES), F32)
             for tap in range(tap_count):
                 rows = buf_ref[last, at + shift + tap : at + shift + tap + chunk, :]
-                total = total + rows * taps_ref[tap : tap + 1, :]
+                total = total + rows * taps[tap : tap + 1, :]
             out_ref[at // share, 0, at % share : at % share + chunk, :] = total.astype(BF16)
 
     @pl.when(step < seqs)
     def _():
         weight = w_ref[...].reshape(-1, w_ref.shape[2])
-        low = (lax.broadcasted_iota(jnp.int32, (sub, LANES), 1) % HEAD_DIM) < half
+        lane = lax.broadcasted_iota(jnp.int32, (sub, LANES), 1)
+        low, keyed = (lane % HEAD_DIM) < half, lane < HEAD_DIM
+        edges = jnp.concatenate([before_ref[step], after_ref[step]], axis=0)
+        edges = normalize(edges, gain_ref[...]).astype(BF16)
         ends = gate(
-            jnp.dot(edge_ref[step], weight[:, : 2 * LANES], preferred_element_type=F32)
+            jnp.dot(edges, weight[:, : 2 * LANES], preferred_element_type=F32)
         ).astype(BF16).astype(F32)
         buf_ref[slot, 0:EDGE, :] = ends[:EDGE]
         buf_ref[slot, EDGE + length : 2 * EDGE + length, :] = ends[EDGE:]
@@ -99,8 +107,10 @@
             for part, ref, scale in ((2, q_ref, HEAD_DIM**-0.5), (3, kv_ref, None)):
                 x = raw[:, part * LANES : (part + 1) * LANES]
                 partner = jnp.where(low, pltpu.roll(x, LANES - half, 1), pltpu.roll(x, half, 1))
-                at = slice((part - 2) * LANES, (part - 1) * LANES)
-                turned = x * cos_ref[table, at] + partner * sin_ref[table, at]
+                cosine, sine = cos_ref[table, :], sin_ref[table, :]
+                if part == 3:
+                    cosine, sine = jnp.where(keyed, cosine, 1.0), jnp.where(keyed, sine, 0.0)
+                turned = x * cosine + partner * sine
                 if scale is not None:
                     turned = turned * scale
                 ref[0, table, :] = turned.astype(BF16)
@@ -111,8 +121,8 @@
             filter_rows(first)
 
 
-def project(normed, edges, weight, taps, cosine, sine, dests, sub=256, chunk=32):
-    seqs = edges.shape[0]
+def project(normed, before, after, gain, weight, taps, cosine, sine, dests, sub=256, chunk=32):
+    seqs = before.shape[0]
     rows, width = normed.shape
     length = rows // seqs
     inside = pl.BlockSpec(memory_space=pltpu.VMEM)
@@ -122,7 +132,7 @@
         functools.partial(project_kernel, sub=sub, chunk=chunk),
         grid=(seqs + 1,),
         in_specs=[pl.BlockSpec((length, width), lambda s: (jnp.minimum(s, seqs - 1), 0))]
-        + [inside] * 5,
+        + [inside] * 7,
         out_specs=[
             pl.BlockSpec(
                 (dests, 1, length // dests, LANES), lambda s: (0, jnp.maximum(s - 1, 0), 0, 0)
@@ -141,36 +151,17 @@
             bytes_accessed=2 * rows * width,
         ),
         name="project",
-    )(in_hbm(normed), edges, weight, taps, cosine, sine)
-
-
-def attend_kernel(
-    place_ref, sink_ref, q_ref, before_ref, kv_ref, after_ref, out_ref, log_ref,
-    pad_ref, one_ref, bias_ref,
-):
-    length = kv_ref.shape[1]
-    blocks = length // Q_BLOCK
-    span = Q_BLOCK + 2 * WINDOW
-
-    @pl.when(pl.program_id(0) == 0)
-    def _():
-        query = lax.broadcasted_iota(jnp.int32, (Q_BLOCK, span), 0)
-        key = lax.broadcasted_iota(jnp.int32, (Q_BLOCK, span), 1)
-        band = (key >= query) & (key <= query + 2 * WINDOW)
-        first = jnp.where(place_ref[0] == 0, WINDOW, 0)
-        last = jnp.where(place_ref[0] == place_ref[1] - 1, Q_BLOCK + WINDOW, span)
-        zero, out = jnp.zeros(band.shape, F32), jnp.full(band.shape, MASK_VALUE, F32)
-        bias_ref[0] = jnp.where(band, zero, out)
-        bias_ref[1] = jnp.where(band & (key >= first), zero, out)
-        bias_ref[2] = jnp.where(band & (key < last), zero, out)
-
-    pad_ref[0:WINDOW, :] = before_ref[0]
-    pad_ref[WINDOW : WINDOW + length, :] = kv_ref[0]
-    pad_ref[WINDOW + length : 2 * WINDOW + length, :] = after_ref[0]
-    padded = pad_ref[...]
-    in_low = lax.broadcasted_iota(jnp.int32, padded.shape, 1) < HEAD_DIM
-    one_ref[...] = jnp.where(in_low, jnp.ones_like(padded), padded)
-
+    )(in_hbm(normed), before, after, gain.reshape(1, width), weight, taps, cosine, sine)
+
+
+def band_bias(first, last):
+    query = lax.broadcasted_iota(jnp.int32, (Q_BLOCK, SPAN), 0)
+    key = lax.broadcasted_iota(jnp.int32, (Q_BLOCK, SPAN), 1)
+    allowed = (key >= query) & (key <= query + 2 * WINDOW) & (key >= first) & (key < last)
+    return jnp.where(allowed, 0.0, MASK_VALUE).astype(F32)
+
+
+def attend_blocks(sink_ref, jobs):
     low = lax.broadcasted_iota(jnp.int32, (Q_BLOCK, LANES), 1) < HEAD_DIM
     low_both = lax.broadcasted_iota(jnp.int32, (2 * Q_BLOCK, LANES), 1) < HEAD_DIM
     diagonal = lax.broadcasted_iota(jnp.int32, (LANES, LANES), 0) == lax.broadcasted_iota(
@@ -179,82 +170,205 @@
     is_first = lax.broadcasted_iota(jnp.int32, (2 * Q_BLOCK, 1), 0) < Q_BLOCK
     sink = jnp.where(is_first, sink_ref[0], sink_ref[1])
 
-    def score(block):
-        at = block * Q_BLOCK
-        keys = pad_ref[at : at + span, :]
-        bias = bias_ref[1 if block == 0 else 2 if block == blocks - 1 else 0]
-        query = q_ref[0, at : at + Q_BLOCK, :]
+    def score(job):
+        query, bias = job[0](), job[3]()
         swapped = pltpu.roll(query.astype(F32), HEAD_DIM, 1).astype(BF16)
         own = jnp.concatenate([query, swapped], 0)
         own = jnp.where(low_both, own, jnp.zeros_like(own))
         scores = lax.dot_general(
-            own, keys, (((1,), (1,)), ((), ())), preferred_element_type=F32
+            own, job[1](), (((1,), (1,)), ((), ())), preferred_element_type=F32
         )
         return scores + jnp.concatenate([bias, bias], 0)
 
-    def weigh(block, scores):
+    def weigh(scores):
         top = jnp.maximum(jnp.max(scores, axis=-1, keepdims=True), sink)
         return top, jnp.exp(scores - top).astype(BF16)
 
-    def blend(block, top, weights):
-        at = block * Q_BLOCK
-        both = jnp.dot(weights, one_ref[at : at + span, :], preferred_element_type=F32)
+    def blend(job, top, weights):
+        both = jnp.dot(weights, job[2](), preferred_element_type=F32)
         swapped = pltpu.roll(both, HEAD_DIM, 1)
         total = jnp.where(low_both, both, swapped) + jnp.exp(sink - top)
         log_total = top + jnp.log(total)
-        for head in range(2):
-            log_ref[0, head : head + 1, at : at + Q_BLOCK] = jnp.sum(
+        logs = [
+            jnp.sum(
                 jnp.where(diagonal, log_total[head * Q_BLOCK : (head + 1) * Q_BLOCK], 0.0),
                 axis=0,
                 keepdims=True,
             )
+            for head in range(2)
+        ]
         first = swapped[:Q_BLOCK] / total[:Q_BLOCK]
         second = both[Q_BLOCK:] / total[Q_BLOCK:]
-        out_ref[block, 0] = jnp.where(low, first, second).astype(BF16)
-
-    ahead, behind = score(0), None
-    for block in range(blocks):
+        job[4](jnp.where(low, first, second).astype(BF16), logs)
+
+    ahead, behind = score(jobs[0]), None
+    for at, job in enumerate(jobs):
         scores = ahead
-        if block + 1 < blocks:
-            ahead = score(block + 1)
-        top, weights = weigh(block, scores)
+        if at + 1 < len(jobs):
+            ahead = score(jobs[at + 1])
+        top, weights = weigh(scores)
         if behind is not None:
-            blend(block - 1, *behind)
+            blend(jobs[at - 1], *behind)
         behind = top, weights
-    blend(blocks - 1, *behind)
-
-
-def attend(place, sink, query, before, kv, after, dests):
+    blend(jobs[-1], *behind)
+
+
+def with_ones(keys):
+    in_low = lax.broadcasted_iota(jnp.int32, keys.shape, keys.ndim - 1) < HEAD_DIM
+    return jnp.where(in_low, jnp.ones_like(keys), keys)
+
+
+def inner_kernel(sink_ref, q_ref, kv_ref, out_ref, log_ref, one_ref, bias_ref):
+    length = kv_ref.shape[1]
+
+    @pl.when(pl.program_id(0) == 0)
+    def _():
+        bias_ref[...] = band_bias(0, SPAN)
+
+    one_ref[...] = with_ones(kv_ref[0])
+
+    def job(block):
+        at = block * Q_BLOCK
+        span = slice(at - WINDOW, at + Q_BLOCK + WINDOW)
+
+        def store(out, logs):
+            out_ref[block, 0] = out
+            for head in range(2):
+                log_ref[0, head : head + 1, at : at + Q_BLOCK] = logs[head]
+
+        return (
+            lambda: q_ref[0, at : at + Q_BLOCK, :],
+            lambda: kv_ref[0, span, :],
+            lambda: one_ref[span, :],
+            lambda: bias_ref[...],
+            store,
+        )
+
+    attend_blocks(sink_ref, [job(block) for block in range(1, length // Q_BLOCK - 1)])
+
+
+def attend_inner(sink, query, kv, dests):
     seqs, length, _ = kv.shape
-    span = Q_BLOCK + 2 * WINDOW
-    edge = pl.BlockSpec((1, WINDOW, LANES), lambda s: (s, 0, 0))
     whole = pl.BlockSpec((1, length, LANES), lambda s: (s, 0, 0))
-    smem = pl.BlockSpec(memory_space=pltpu.SMEM)
     return pl.pallas_call(
-        attend_kernel,
+        inner_kernel,
         grid=(seqs,),
-        in_specs=[smem, smem, whole, edge, whole, edge],
+        in_specs=[pl.BlockSpec(memory_space=pltpu.SMEM), whole, whole],
         out_specs=[
             pl.BlockSpec((dests, 1, length // dests, LANES), lambda s: (0, s, 0, 0)),
             pl.BlockSpec((1, 2, length), lambda s: (s, 0, 0)),
         ],
         out_shape=[
-            jax.ShapeDtypeStruct((dests, seqs, length // dests, LANES), BF16),
-            jax.ShapeDtypeStruct((seqs, 2, length), F32),
+            pltpu.HBM((dests, seqs, length // dests, LANES), BF16),
+            pltpu.HBM((seqs, 2, length), F32),
         ],
         scratch_shapes=[
-            pltpu.VMEM((length + 2 * WINDOW, LANES), BF16),
-            pltpu.VMEM((length + 2 * WINDOW, LANES), BF16),
-            pltpu.VMEM((3, Q_BLOCK, span), F32),
-        ],
-        compiler_params=params("arbitrary"),
+            pltpu.VMEM((length, LANES), BF16),
+            pltpu.VMEM((Q_BLOCK, SPAN), F32),
+        ],
+        compiler_params=params("arbitrary", mb=28),
         cost_estimate=pl.CostEstimate(
-            flops=40 * seqs * length * span * LANES // 8,
+            flops=40 * seqs * length * SPAN * LANES // 8,
             transcendentals=0,
             bytes_accessed=6 * seqs * length * LANES,
         ),
-        name="attend",
-    )(place, sink, in_hbm(query), before, in_hbm(kv), after)
+        name="attend_inner",
+    )(sink, in_hbm(query), in_hbm(kv))
+
+
+def edge_kernel(
+    place_ref, sink_ref, q_low_ref, q_high_ref, before_ref, kv_low_ref, kv_high_ref, after_ref,
+    _, __, out_ref, log_ref, pad_ref, one_ref, bias_ref, own_ref, own_log_ref, sems
+):
+    seqs = before_ref.shape[0]
+    blocks = out_ref.shape[0]
+    bias_ref[0] = band_bias(jnp.where(place_ref[0] == 0, WINDOW, 0), SPAN)
+    bias_ref[1] = band_bias(
+        0, jnp.where(place_ref[0] == place_ref[1] - 1, Q_BLOCK + WINDOW, SPAN)
+    )
+    pad_ref[0, :, :WINDOW] = before_ref[...]
+    pad_ref[0, :, WINDOW:] = kv_low_ref[...]
+    pad_ref[1, :, : SPAN - WINDOW] = kv_high_ref[...]
+    pad_ref[1, :, SPAN - WINDOW :] = after_ref[...]
+    one_ref[...] = with_ones(pad_ref[...])
+
+    def job(side, seq):
+        def store(out, logs):
+            own_ref[side, seq] = out
+            for head in range(2):
+                own_log_ref[side, seq, head : head + 1, :] = logs[head]
+
+        return (
+            lambda: (q_low_ref, q_high_ref)[side][seq],
+            lambda: pad_ref[side, seq],
+            lambda: one_ref[side, seq],
+            lambda: bias_ref[side],
+            store,
+        )
+
+    attend_blocks(sink_ref, [job(side, seq) for side in range(2) for seq in range(seqs)])
+    copies = []
+    for side, block in enumerate((0, blocks - 1)):
+        copies.append(
+            pltpu.make_async_copy(own_ref.at[side], out_ref.at[block], sems.at[side, 0])
+        )
+        copies.append(
+            pltpu.make_async_copy(
+                own_log_ref.at[side],
+                log_ref.at[:, :, pl.ds(block * Q_BLOCK, Q_BLOCK)],
+                sems.at[side, 1],
+            )
+        )
+    for copy in copies:
+        copy.start()
+    for copy in copies:
+        copy.wait()
+
+
+def attend_edge(place, sink, query, before, kv, after, out, log_total):
+    seqs, length, _ = kv.shape
+    ends = SPAN - WINDOW
+    smem = pl.BlockSpec(memory_space=pltpu.SMEM)
+    raw = pl.BlockSpec(memory_space=pl.ANY)
+
+    def rows(count, at):
+        return pl.BlockSpec((seqs, count, LANES), lambda i: (0, at, 0))
+
+    return pl.pallas_call(
+        edge_kernel,
+        grid=(1,),
+        in_specs=[
+            smem,
+            smem,
+            rows(Q_BLOCK, 0),
+            rows(Q_BLOCK, length // Q_BLOCK - 1),
+            rows(WINDOW, 0),
+            rows(ends, 0),
+            rows(ends, length // ends - 1),
+            rows(WINDOW, 0),
+            raw,
+            raw,
+        ],
+        out_specs=[raw, raw],
+        out_shape=[pltpu.HBM(out.shape, BF16), pltpu.HBM(log_total.shape, F32)],
+        input_output_aliases={8: 0, 9: 1},
+        scratch_shapes=[
+            pltpu.VMEM((2, seqs, SPAN, LANES), BF16),
+            pltpu.VMEM((2, seqs, SPAN, LANES), BF16),
+            pltpu.VMEM((2, Q_BLOCK, SPAN), F32),
+            pltpu.VMEM((2, seqs, Q_BLOCK, LANES), BF16),
+            pltpu.VMEM((2, seqs, 2, Q_BLOCK), F32),
+            pltpu.SemaphoreType.DMA((2, 2)),
+        ],
+        compiler_params=params("arbitrary", mb=28),
+        cost_estimate=pl.CostEstimate(
+            flops=10 * seqs * length * SPAN * LANES // 8,
+            transcendentals=0,
+            bytes_accessed=2 * seqs * length * LANES,
+        ),
+        name="attend_edge",
+    )(place, sink, in_hbm(query), in_hbm(query), before, in_hbm(kv), in_hbm(kv), after,
+      in_hbm(out), in_hbm(log_total))
 
 
 def side_by_side(ref):
@@ -268,12 +382,7 @@
 def mix_conv_kernel(x_ref, gain_ref, w_ref, out_ref, act_ref):
     @pl.when(pl.program_id(0) == 0)
     def _():
-        x = side_by_side(x_ref).astype(F32)
-        gain = side_by_side(gain_ref)[0:1].astype(F32)
-        mean = jnp.mean(x, axis=-1, keepdims=True)
-        centred = x - mean
-        variance = jnp.mean(centred * centred, axis=-1, keepdims=True)
-        v = centred * lax.rsqrt(variance + EPSILON) * gain
+        v = normalize(side_by_side(x_ref), side_by_side(gain_ref)[0:1])
         act_ref[...] = (v / (1.0 + jnp.exp(-v))).astype(BF16)
 
     out_ref[...] = jnp.dot(act_ref[...], columns(w_ref), preferred_element_type=F32)
@@ -331,27 +440,34 @@
 def pack(value, gate, query, key, kv, conv, attn, gain, copies):
     rows = value.shape[0]
     cols = 3 * LANES + 2 * key.shape[1]
+    operands = (value, gate, query, key.T, kv.T, conv, attn, gain.reshape(1, LANES))
+    shapes = ((2 * LANES + EDGE, LANES), (copies, rows, cols))
     return pl.pallas_call(
         pack_kernel,
+        grid=(1,),
+        in_specs=[pl.BlockSpec(a.shape, lambda i: (0, 0)) for a in operands],
+        out_specs=[
+            pl.BlockSpec(shapes[0], lambda i: (0, 0)),
+            pl.BlockSpec(shapes[1], lambda i: (0, 0, 0)),
+        ],
         out_shape=[
-            jax.ShapeDtypeStruct((2 * LANES + EDGE, LANES), BF16),
-            jax.ShapeDtypeStruct((copies, rows, cols), BF16),
+            jax.ShapeDtypeStruct(shapes[0], BF16),
+            jax.ShapeDtypeStruct(shapes[1], BF16),
         ],
         compiler_params=pltpu.CompilerParams(vmem_limit_bytes=16 * 1024 * 1024),
         name="pack",
-    )(value, gate, query, key.T, kv.T, conv, attn, gain.reshape(1, LANES))
+    )(*(in_hbm(a) for a in operands))
 
 
 def turn_tables(tok_count):
     half = HEAD_DIM // 2
     offset = lax.axis_index("sp") * tok_count
     positions = (offset + jnp.arange(tok_count, dtype=jnp.int32)).astype(F32)
-    lane = jnp.arange(2 * LANES, dtype=jnp.int32)
+    lane = jnp.arange(LANES, dtype=jnp.int32)
     inverse = ROPE_BASE ** (-(lane % half).astype(F32) / half)
     angles = positions[:, None] * inverse[None, :]
-    turns = (lane < LANES + HEAD_DIM)[None, :]
     sign = jnp.where(lane % HEAD_DIM < half, -1.0, 1.0).astype(F32)[None, :]
-    return jnp.where(turns, jnp.cos(angles), 1.0), jnp.where(turns, jnp.sin(angles) * sign, 0.0)
+    return jnp.cos(angles), jnp.sin(angles) * sign
 
 
 def on_device(
@@ -385,18 +501,18 @@
     before = lax.ppermute(tokens[:, -EDGE:], "sp", up)
     after = lax.ppermute(tokens[:, :EDGE], "sp", down)
     normed = norm_tokens(tokens.reshape(seqs * length, width), norm_gain)
-    edges = norm_tokens(
-        jnp.concatenate([before, after], axis=1).reshape(2 * seqs * EDGE, width), norm_gain
-    ).reshape(seqs, 2 * EDGE, width)
     cosine, sine = turn_tables(length)
     filtered, query, kv = project(
-        normed, edges, in_weight, conv_taps.astype(F32), cosine, sine, tp
+        normed, before, after, norm_gain, in_weight, conv_taps, cosine, sine, tp
     )
 
     before = lax.ppermute(kv[:, -WINDOW:], "sp", up)
     after = lax.ppermute(kv[:, :WINDOW], "sp", down)
     conv_tok = lax.all_to_all(filtered, "tp", 0, 0, tiled=True)
-    attn, log_total = attend(place, sink_logit, query, before, kv, after, tp)
+    attn, log_total = attend_inner(sink_logit, query, kv, tp)
+    attn, log_total = attend_edge(
+        place, sink_logit, query, before, kv, after, attn, log_total
+    )
     attn_tok = lax.all_to_all(attn, "tp", 0, 0, tiled=True)
 
     rows = seqs * length // tp

time: 146 us -> 133 us (0.911); the launches traced: 144 us -> 132 us
  local copies, waits for them, and re-layouts: 11.7 us -> 3.58 us
  other arithmetic: 7.47 us -> 1.99 us
    unnamed x22 -> x4, local copies, waits for them, and re-layouts: 8.14 us -> 0.01 us
    select_n x1 -> x0, other arithmetic: 4.85 us -> none  [turn_tables(): jnp.where(turns, jnp.sin(angles) * sign, 0.0)]
    all_to_all x1, waiting for transfers between devices: 0.91 us -> 5.34 us  [on_device(): conv_tok = lax.all_to_all(filtered, 'tp', 0, 0, tiled=True)]
    ppermute x1, waiting for transfers between devices: 4.3 us -> 0.01 us  [on_device(): before = lax.ppermute(kv[:, -WINDOW:], 'sp', up)]
    ppermute x1, waiting for transfers between devices: 2.32 us -> 5.92 us  [on_device(): before = lax.ppermute(tokens[:, -EDGE:], 'sp', up)]
    pallas_call x2 -> x3, Pallas kernels: 11 us -> 14 us  [the longest x1 7.72 us: attend_inner(): pl.pallas_call(inner_kernel, grid=(seqs,), in_specs=[pl.BlockSpec(memory_...]
    ppermute x1, waiting for transfers between devices: 3.96 us -> 1.04 us  [on_device(): after = lax.ppermute(kv[:, :WINDOW], 'sp', down)]
    pallas_call x2 -> x1, Pallas kernels: 19.4 us -> 17.2 us  [norm_tokens(): pl.pallas_call(norm_kernel, grid=(rows // block,), in_specs=[pl.BlockSpec...]
  transfers between devices with their start and end apart: 8 -> 8, of which waited for: 6 -> 6; matrix products, arithmetic and copies ran while one was open for 8% -> 4% of each run, Pallas kernels for 38% -> 41%
where the time goes in v2:
time: 133 us; the launch traced here: 132 us
  Pallas kernels  62.4 us (47%)
  starting transfers between devices  28.2 us (21%)
  waiting for transfers between devices  22 us (17%)
  between operations  14.1 us (11%)
  local copies, waits for them, and re-layouts  3.58 us (3%)
  other arithmetic  1.99 us (1%)
    pallas_call x1, Pallas kernels, project(): pl.pallas_call(functools.partial(project_kernel, sub=sub, chunk=chunk), g...  18.2 us
    pallas_call x1, Pallas kernels, norm_tokens(): pl.pallas_call(norm_kernel, grid=(rows // block,), in_specs=[pl.BlockSpec...  17.2 us
    pallas_call x2, Pallas kernels, mix(): pl.pallas_call(kernel, grid=(groups // cols,), in_specs=[pl.BlockSpec(x.s...  13 us
    all_to_all x1, starting transfers between devices, on_device(): in_weight = lax.all_to_all(in_piece, 'sp', 0, 0, tiled=True)  8.43 us
    pallas_call x1, Pallas kernels, attend_inner(): pl.pallas_call(inner_kernel, grid=(seqs,), in_specs=[pl.BlockSpec(memory_...  7.72 us
    all_to_all x1, waiting for transfers between devices, on_device(): attn_tok = lax.all_to_all(attn, 'tp', 0, 0, tiled=True)  7.47 us
    all_to_all x1, starting transfers between devices, on_device(): conv_tok = lax.all_to_all(filtered, 'tp', 0, 0, tiled=True)  6.08 us
    ppermute x1, waiting for transfers between devices, on_device(): before = lax.ppermute(tokens[:, -EDGE:], 'sp', up)  5.92 us
  transfers between devices with their start and end apart: 8, of which 6 were waited for; matrix products, arithmetic and copies ran while one was open for 4% of the time, Pallas kernels for 41%

profile of v2, /device:TPU:1, one launch (start us, length us, event | category | flops | bytes accessed | tf_op | source)
XLA Modules:
  0.0 132.3 jit_solution(2059580009035801282)
XLA Ops:
  7.2 2.4 %pack.1 = (bf16[272,128]{1,0:T(8,128)(2,1)}, bf16[16,128,512]{2,1,0:T(8,128)(2,1)}) custom-call(bf16[128,128]{1,0:T(8,128)(2,1)} %value_ref.1, bf16[128,128]{1,0:T(8,128)(2,1)} %gate_ref.1, bf16[128,128]{1,0:T(8,128)(2,1)} %query_ref.1, bf16[64,128]{1,0:T(8,128)(2,1)} %bitcast.16, bf16[64,128]{1,0:T(8,128)(2,1)} %bitcast.17, bf16[128,128]{1,0:T(8,128)(2,1)} %conv_ref.1, ...), custom_call_target="tpu_custom_call" | custom-call | tf_op jit(solution)/shard_map/pack/pallas_call | solution.py:445
  9.6 8.4 %all-to-all-start = ((bf16[16,128,512]{2,1,0:T(8,128)(2,1)}), bf16[16,128,512]{2,1,0:T(8,128)(2,1)S(1)}, u32[]{:S(2)}, u32[]{:S(2)}) async-start(bf16[16,128,512]{2,1,0:T(8,128)(2,1)} %get-tuple-element.11), calls=%async_computation | async-start | bytes 4194304 | tf_op jit(solution)/shard_map/all_to_all | solution.py:499
  18.1 1.9 %fusion.5 = (bf16[4,16,2048]{2,1,0:T(8,128)(2,1)}, bf16[4,16,2048]{2,1,0:T(8,128)(2,1)}) fusion(bf16[4,1024,2048]{2,1,0:T(8,128)(2,1)} %param.12), kind=kLoop, calls=%fused_computation.12 | loop fusion | bytes 1048576 | tf_op jit(solution)/shard_map/slice | solution.py:502
  19.9 3.3 %collective-permute-start = (bf16[4,16,2048]{2,1,0:T(8,128)(2,1)}, bf16[4,16,2048]{2,1,0:T(8,128)(2,1)S(1)}, u32[]{:S(2)}, u32[]{:S(2)}) collective-permute-start(bf16[4,16,2048]{2,1,0:T(8,128)(2,1)} %get-tuple-element.21), channel_id=1, source_target_pairs={{0,8},{8,16},{16,24},{24,32},{32,40},{40,48},{48,56},{56,64},{64,7... | collective-permute-start | bytes 786440 | tf_op jit(solution)/shard_map/ppermute | solution.py:501
  23.2 1.3 collective-permute-start.1
  24.5 0.7 reshape.56.gain_ref
  25.3 17.2 %norm_tokens.1.x_ref = bf16[4096,2048]{1,0:T(8,128)(2,1)} custom-call(bf16[4096,2048]{1,0:T(8,128)(2,1)} %bitcast.14, bf16[1,2048]{1,0:T(2,128)(2,1)S(1)} %reshape.56.gain_ref), custom_call_target="tpu_custom_call" | custom-call | flops 335544320 | bytes 33554432 | tf_op jit(solution)/shard_map/norm_tokens/pallas_call | solution.py:48
  42.5 1.9 %fusion = (f32[1024,128]{1,0:T(8,128)S(1)}, f32[1024,128]{1,0:T(8,128)S(1)}) fusion(f32[128]{0:T(128)S(1)} %get-tuple-element.26, f32[128]{0:T(128)S(1)} %get-tuple-element.27, f32[1024]{0:T(1024)S(1)} %add_convert_fusion), kind=kLoop, calls=%fused_computation.2 | loop fusion | flops 262144 | bytes 1053696 | tf_op jit(solution)/shard_map/mul | solution.py:470
  44.4 5.9 %collective-permute-done.before_ref = bf16[4,16,2048]{2,1,0:T(8,128)(2,1)S(1)} collective-permute-done((bf16[4,16,2048]{2,1,0:T(8,128)(2,1)}, bf16[4,16,2048]{2,1,0:T(8,128)(2,1)S(1)}, u32[]{:S(2)}, u32[]{:S(2)}) %collective-permute-start) | collective-permute-done | bytes 262176 | tf_op jit(solution)/shard_map/ppermute | solution.py:501
  50.3 1.9 %collective-permute-done.1.after_ref = bf16[4,16,2048]{2,1,0:T(8,128)(2,1)} collective-permute-done((bf16[4,16,2048]{2,1,0:T(8,128)(2,1)}, bf16[4,16,2048]{2,1,0:T(8,128)(2,1)}, u32[]{:S(2)}, u32[]{:S(2)}) %collective-permute-start.1) | collective-permute-done | bytes 262176 | tf_op jit(solution)/shard_map/ppermute | solution.py:502
  52.2 18.2 %project.1 = (bf16[8,4,128,128]{3,2,1,0:T(8,128)(2,1)}, bf16[4,1024,128]{2,1,0:T(8,128)(2,1)}, bf16[4,1024,128]{2,1,0:T(8,128)(2,1)}) custom-call(bf16[4096,2048]{1,0:T(8,128)(2,1)} %norm_tokens.1.x_ref, bf16[4,16,2048]{2,1,0:T(8,128)(2,1)S(1)} %collective-permute-done.before_ref, bf16[4,16,2048]{2,1,0:T(8,128)(2,1)} %collective-permute-done.1.after_ref, ...), custom_call_target="tpu_custom_call" | custom-call | flops 8589934592 | bytes 16777216 | tf_op jit(solution)/shard_map/project/pallas_call | solution.py:131
  70.4 6.1 %all-to-all-start.2 = ((bf16[8,4,128,128]{3,2,1,0:T(8,128)(2,1)}), bf16[8,4,128,128]{3,2,1,0:T(8,128)(2,1)S(1)}, u32[]{:S(2)}, u32[]{:S(2)}) async-start(bf16[8,4,128,128]{3,2,1,0:T(8,128)(2,1)} %get-tuple-element.17), calls=%async_computation.2 | async-start | bytes 2097152 | tf_op jit(solution)/shard_map/all_to_all | solution.py:511
  76.4 1.0 fusion.6
  77.4 2.1 %collective-permute-start.2 = (bf16[4,128,128]{2,1,0:T(8,128)(2,1)S(1)}, bf16[4,128,128]{2,1,0:T(8,128)(2,1)S(1)}, u32[]{:S(2)}, u32[]{:S(2)}) collective-permute-start(bf16[4,128,128]{2,1,0:T(8,128)(2,1)S(1)} %get-tuple-element.23), channel_id=1, source_target_pairs={{0,8},{8,16},{16,24},{24,32},{32,40},{40,48},{48,56},{56,64},{64,7... | collective-permute-start | bytes 393224 | tf_op jit(solution)/shard_map/ppermute | solution.py:509
  79.5 1.5 %collective-permute-start.3 = (bf16[4,128,128]{2,1,0:T(8,128)(2,1)S(1)}, bf16[4,128,128]{2,1,0:T(8,128)(2,1)S(1)}, u32[]{:S(2)}, u32[]{:S(2)}) collective-permute-start(bf16[4,128,128]{2,1,0:T(8,128)(2,1)S(1)} %get-tuple-element.22), channel_id=1, source_target_pairs={{8,0},{16,8},{24,16},{32,24},{40,32},{48,40},{56,48},{64,56},{72,6... | collective-permute-start | bytes 393224 | tf_op jit(solution)/shard_map/ppermute | solution.py:510
  81.1 7.7 %attend_inner.1 = (bf16[8,4,128,128]{3,2,1,0:T(8,128)(2,1)}, f32[4,2,1024]{2,1,0:T(2,128)}) custom-call(f32[2]{0:T(128)S(1)} %copy-done, bf16[4,1024,128]{2,1,0:T(8,128)(2,1)} %get-tuple-element.12.q_ref.q_low_ref.q_high_ref, bf16[4,1024,128]{2,1,0:T(8,128)(2,1)} %get-tuple-element.13.kv_ref.kv_low_ref.kv_high_ref), custom_call_target="tpu_custom_call" | custom-call | flops 1006632960 | bytes 3145728 | tf_op jit(solution)/shard_map/attend_inner/pallas_call | solution.py:253
  88.8 1.0 collective-permute-done.3.after_ref
  89.9 3.9 %attend_edge.1 = (bf16[8,4,128,128]{3,2,1,0:T(8,128)(2,1)}, f32[4,2,1024]{2,1,0:T(2,128)}) custom-call(s32[2]{0:T(128)S(1)} %pad_add_fusion.place_ref, f32[2]{0:T(128)S(1)} %copy-done, bf16[4,1024,128]{2,1,0:T(8,128)(2,1)} %get-tuple-element.12.q_ref.q_low_ref.q_high_ref, ...), custom_call_target="tpu_custom_call", output_to_operand_aliasing={{0}: (8, {}), {1}: (9, {})} | custom-call | flops 251658240 | bytes 1048576 | tf_op jit(solution)/shard_map/attend_edge/pallas_call | solution.py:337
  93.8 5.3 %all-to-all-done.2 = bf16[8,4,128,128]{3,2,1,0:T(8,128)(2,1)S(1)} async-done(((bf16[8,4,128,128]{3,2,1,0:T(8,128)(2,1)}), bf16[8,4,128,128]{3,2,1,0:T(8,128)(2,1)S(1)}, u32[]{:S(2)}, u32[]{:S(2)}) %all-to-all-start.2) | async-done | bytes 1048608 | tf_op jit(solution)/shard_map/all_to_all | solution.py:511
  99.2 5.6 %all-to-all-start.1 = ((bf16[8,4,128,128]{3,2,1,0:T(8,128)(2,1)}), bf16[8,4,128,128]{3,2,1,0:T(8,128)(2,1)S(1)}, u32[]{:S(2)}, u32[]{:S(2)}) async-start(bf16[8,4,128,128]{3,2,1,0:T(8,128)(2,1)} %get-tuple-element.16), calls=%async_computation.1 | async-start | bytes 2097152 | tf_op jit(solution)/shard_map/all_to_all | solution.py:516
  104.7 0.3 all-gather.2.cloned.1.call-done
  105.0 7.2 %mix_conv.1.part_ref = f32[512,2048]{1,0:T(8,128)} custom-call(bf16[8,512,128]{2,1,0:T(8,128)(2,1)S(1)} %bitcast.9, bf16[16,8,272,128]{3,2,1,0:T(8,128)(2,1)} %bitcast.11, bf16[16,8,272,128]{3,2,1,0:T(8,128)(2,1)} %bitcast.12), custom_call_target="tpu_custom_call" | custom-call | flops 2147483648 | bytes 4456448 | tf_op jit(solution)/shard_map/mix_conv/pallas_call | solution.py:407
  112.3 7.5 %all-to-all-done.1 = bf16[8,4,128,128]{3,2,1,0:T(8,128)(2,1)S(1)} async-done(((bf16[8,4,128,128]{3,2,1,0:T(8,128)(2,1)}), bf16[8,4,128,128]{3,2,1,0:T(8,128)(2,1)S(1)}, u32[]{:S(2)}, u32[]{:S(2)}) %all-to-all-start.1) | async-done | bytes 1048608 | tf_op jit(solution)/shard_map/all_to_all | solution.py:516
  119.7 5.7 %mix_attn.1 = bf16[512,2048]{1,0:T(8,128)(2,1)} custom-call(bf16[8,512,128]{2,1,0:T(8,128)(2,1)S(1)} %bitcast.10, f32[512,2048]{1,0:T(8,128)} %mix_conv.1.part_ref, bf16[16,8,272,128]{3,2,1,0:T(8,128)(2,1)} %bitcast.13), custom_call_target="tpu_custom_call" | custom-call | flops 2147483648 | bytes 4456448 | tf_op jit(solution)/shard_map/mix_attn/pallas_call | solution.py:407
  (11 shorter events, 0.2 us)
Async XLA Ops:
  7.2 97.9 %all-gather.2.cloned.1.call-start = ((), (), s32[]{:S(2)}) async-start(), calls=%async_computation.3 | async-start | bytes 8982528 | tf_op jit(solution)/shard_map/all_gather | solution.py:497
  9.6 42.5 %all-to-all-start = ((bf16[16,128,512]{2,1,0:T(8,128)(2,1)}), bf16[16,128,512]{2,1,0:T(8,128)(2,1)S(1)}, u32[]{:S(2)}, u32[]{:S(2)}) async-start(bf16[16,128,512]{2,1,0:T(8,128)(2,1)} %get-tuple-element.11), calls=%async_computation | async-start | bytes 4194304 | tf_op jit(solution)/shard_map/all_to_all | solution.py:499
  19.9 30.3 %collective-permute-start = (bf16[4,16,2048]{2,1,0:T(8,128)(2,1)}, bf16[4,16,2048]{2,1,0:T(8,128)(2,1)S(1)}, u32[]{:S(2)}, u32[]{:S(2)}) collective-permute-start(bf16[4,16,2048]{2,1,0:T(8,128)(2,1)} %get-tuple-element.21), channel_id=1, source_target_pairs={{0,8},{8,16},{16,24},{24,32},{32,40},{40,48},{48,56},{56,64},{64,7... | collective-permute-start | bytes 786440 | tf_op jit(solution)/shard_map/ppermute | solution.py:501
  23.2 28.9 %collective-permute-start.1 = (bf16[4,16,2048]{2,1,0:T(8,128)(2,1)}, bf16[4,16,2048]{2,1,0:T(8,128)(2,1)}, u32[]{:S(2)}, u32[]{:S(2)}) collective-permute-start(bf16[4,16,2048]{2,1,0:T(8,128)(2,1)} %get-tuple-element.20), channel_id=1, source_target_pairs={{8,0},{16,8},{24,16},{32,24},{40,32},{48,40},{56,48},{64,56},{72,6... | collective-permute-start | bytes 786440 | tf_op jit(solution)/shard_map/ppermute | solution.py:502
  25.2 26.9 %copy-start.1 = (bf16[31,128]{1,0:T(8,128)(2,1)S(1)}, bf16[31,128]{1,0:T(8,128)(2,1)}, u32[]{:S(2)}) copy-start(bf16[31,128]{1,0:T(8,128)(2,1)} %taps_ref.1) | copy-start | bytes 23812
  52.2 28.9 %copy-start = (f32[2]{0:T(128)S(1)}, f32[2]{0:T(128)}, u32[]{:S(2)}) copy-start(f32[2]{0:T(128)} %sink_ref.3) | copy-start | bytes 28
  70.4 28.8 %all-to-all-start.2 = ((bf16[8,4,128,128]{3,2,1,0:T(8,128)(2,1)}), bf16[8,4,128,128]{3,2,1,0:T(8,128)(2,1)S(1)}, u32[]{:S(2)}, u32[]{:S(2)}) async-start(bf16[8,4,128,128]{3,2,1,0:T(8,128)(2,1)} %get-tuple-element.17), calls=%async_computation.2 | async-start | bytes 2097152 | tf_op jit(solution)/shard_map/all_to_all | solution.py:511
  77.4 11.4 %collective-permute-start.2 = (bf16[4,128,128]{2,1,0:T(8,128)(2,1)S(1)}, bf16[4,128,128]{2,1,0:T(8,128)(2,1)S(1)}, u32[]{:S(2)}, u32[]{:S(2)}) collective-permute-start(bf16[4,128,128]{2,1,0:T(8,128)(2,1)S(1)} %get-tuple-element.23), channel_id=1, source_target_pairs={{0,8},{8,16},{16,24},{24,32},{32,40},{40,48},{48,56},{56,64},{64,7... | collective-permute-start | bytes 393224 | tf_op jit(solution)/shard_map/ppermute | solution.py:509
  79.5 10.3 %collective-permute-start.3 = (bf16[4,128,128]{2,1,0:T(8,128)(2,1)S(1)}, bf16[4,128,128]{2,1,0:T(8,128)(2,1)S(1)}, u32[]{:S(2)}, u32[]{:S(2)}) collective-permute-start(bf16[4,128,128]{2,1,0:T(8,128)(2,1)S(1)} %get-tuple-element.22), channel_id=1, source_target_pairs={{8,0},{16,8},{24,16},{32,24},{40,32},{48,40},{56,48},{64,56},{72,6... | collective-permute-start | bytes 393224 | tf_op jit(solution)/shard_map/ppermute | solution.py:510
  99.2 20.6 %all-to-all-start.1 = ((bf16[8,4,128,128]{3,2,1,0:T(8,128)(2,1)}), bf16[8,4,128,128]{3,2,1,0:T(8,128)(2,1)S(1)}, u32[]{:S(2)}, u32[]{:S(2)}) async-start(bf16[8,4,128,128]{3,2,1,0:T(8,128)(2,1)} %get-tuple-element.16), calls=%async_computation.1 | async-start | bytes 2097152 | tf_op jit(solution)/shard_map/all_to_all | solution.py:516
Sparse Core Ops, SparseCore 0:
  11.0 94.0 all-gather.1

commit v3 on v2

--- a/solution.py
+++ b/solution.py
@@ -63,7 +63,8 @@
 
 
 def project_kernel(
-    x_ref, before_ref, after_ref, gain_ref, w_ref, taps_ref, cos_ref, sin_ref, out_ref, q_ref, kv_ref, buf_ref, *, sub, chunk
+    x_ref, before_ref, after_ref, gain_ref, w_ref, taps_ref, cos_ref, sin_ref, out_ref, q_ref, kv_ref,
+    low_ref, high_ref, buf_ref, *, sub, chunk
 ):
     step = pl.program_id(0)
     dests, _, share, _ = out_ref.shape
@@ -113,7 +114,12 @@
                 turned = x * cosine + partner * sine
                 if scale is not None:
                     turned = turned * scale
-                ref[0, table, :] = turned.astype(BF16)
+                turned = turned.astype(BF16)
+                ref[0, table, :] = turned
+                if part == 3 and first == 0:
+                    low_ref[step] = turned[:WINDOW]
+                if part == 3 and first + sub == length:
+                    high_ref[step] = turned[sub - WINDOW :]
 
     @pl.when(step == seqs)
     def _():
@@ -139,10 +145,13 @@
             ),
             head_block,
             head_block,
+            inside,
+            inside,
         ],
         out_shape=[
             jax.ShapeDtypeStruct((dests, seqs, length // dests, LANES), BF16), heads, heads
-        ],
+        ]
+        + [jax.ShapeDtypeStruct((seqs, WINDOW, LANES), BF16)] * 2,
         scratch_shapes=[pltpu.VMEM((2, length + 2 * EDGE, LANES), F32)],
         compiler_params=params("arbitrary", mb=28),
         cost_estimate=pl.CostEstimate(
@@ -375,43 +384,57 @@
     return jnp.concatenate([ref[i] for i in range(ref.shape[0])], axis=-1)
 
 
+def by_core(ref, core):
+    count = ref.shape[0] // 2
+    own = [ref[2 * i + core] for i in range(count)]
+    other = [ref[2 * i + 1 - core] for i in range(count)]
+    return jnp.concatenate(own, axis=-1), jnp.concatenate(other, axis=-1)
+
+
 def columns(ref):
     return jnp.concatenate([ref[c].reshape(-1, LANES) for c in range(ref.shape[0])], axis=-1)
 
 
-def mix_conv_kernel(x_ref, gain_ref, w_ref, out_ref, act_ref):
+def mix_conv_kernel(core_ref, x_ref, own_gain_ref, other_gain_ref, own_ref, other_ref, out_ref, act_ref):
+    half = act_ref.shape[1] // 2
+
     @pl.when(pl.program_id(0) == 0)
     def _():
-        v = normalize(side_by_side(x_ref), side_by_side(gain_ref)[0:1])
+        x = jnp.concatenate(by_core(x_ref, core_ref[0]), axis=-1)
+        gain = jnp.concatenate([side_by_side(own_gain_ref), side_by_side(other_gain_ref)], axis=-1)
+        v = normalize(x, gain[0:1])
         act_ref[...] = (v / (1.0 + jnp.exp(-v))).astype(BF16)
 
-    out_ref[...] = jnp.dot(act_ref[...], columns(w_ref), preferred_element_type=F32)
-
-
-def mix_attn_kernel(x_ref, part_ref, w_ref, out_ref):
-    total = part_ref[...] + jnp.dot(
-        side_by_side(x_ref), columns(w_ref), preferred_element_type=F32
-    )
+    total = jnp.dot(act_ref[:, :half], columns(own_ref), preferred_element_type=F32)
+    total = total + jnp.dot(act_ref[:, half:], columns(other_ref), preferred_element_type=F32)
+    out_ref[...] = total
+
+
+def mix_attn_kernel(core_ref, x_ref, part_ref, own_ref, other_ref, out_ref):
+    own, other = by_core(x_ref, core_ref[0])
+    total = part_ref[...] + jnp.dot(own, columns(own_ref), preferred_element_type=F32)
+    total = total + jnp.dot(other, columns(other_ref), preferred_element_type=F32)
     out_ref[...] = total.astype(BF16)
 
 
-def mix(kernel, x, extra, weight, which, out_dtype, cols, name, scratch=()):
+def mix(kernel, core, x, extras, weights, which, out_dtype, cols, name, scratch=()):
     sources, rows, _ = x.shape
-    groups = weight.shape[0]
+    groups, half, height, _ = weights[0].shape
     block = pl.BlockSpec((rows, cols * LANES), lambda n: (0, n))
     if which == 0:
-        place = weight.shape[2] // EDGE - 1
-        extra_spec = pl.BlockSpec((None, sources, EDGE, LANES), lambda n: (0, 0, place, 0))
+        place = height // EDGE - 1
+        extra_spec = pl.BlockSpec((None, half, EDGE, LANES), lambda n: (0, 0, place, 0))
     else:
         extra_spec = block
     return pl.pallas_call(
         kernel,
         grid=(groups // cols,),
         in_specs=[
+            pl.BlockSpec(memory_space=pltpu.SMEM),
             pl.BlockSpec(x.shape, lambda n: (0, 0, 0)),
-            extra_spec,
-            pl.BlockSpec((cols, sources, LANES, LANES), lambda n: (n, 0, which, 0)),
-        ],
+        ]
+        + [extra_spec] * len(extras)
+        + [pl.BlockSpec((cols, half, LANES, LANES), lambda n: (n, 0, which, 0))] * 2,
         out_specs=block,
         out_shape=pltpu.HBM((rows, groups * LANES), out_dtype),
         scratch_shapes=list(scratch),
@@ -419,10 +442,10 @@
         cost_estimate=pl.CostEstimate(
             flops=2 * rows * sources * LANES * groups * LANES,
             transcendentals=0,
-            bytes_accessed=weight.size,
+            bytes_accessed=2 * weights[0].size,
         ),
         name=name,
-    )(x, extra, weight)
+    )(core, x, *extras, *weights)
 
 
 def pack_kernel(
@@ -494,20 +517,24 @@
         conv_value_weight, conv_gate_weight, query_weight, key_weight, value_weight,
         out_conv_weight, out_attn_weight, conv_gain, sp,
     )
-    out_weight = lax.all_gather(out_piece, ("sp", "tp"), axis=0, tiled=True)
-    out_weight = out_weight.reshape(sp, tp, out_piece.shape[0], LANES)
+    same_core = [
+        [row * tp + col for row in range(sp) for col in range(core, tp, 2)] for core in range(2)
+    ]
+    own_weight = lax.all_gather(
+        out_piece, ("sp", "tp"), axis=0, tiled=True, axis_index_groups=same_core
+    )
     in_weight = lax.all_to_all(in_piece, "sp", 0, 0, tiled=True)
 
     before = lax.ppermute(tokens[:, -EDGE:], "sp", up)
     after = lax.ppermute(tokens[:, :EDGE], "sp", down)
     normed = norm_tokens(tokens.reshape(seqs * length, width), norm_gain)
     cosine, sine = turn_tables(length)
-    filtered, query, kv = project(
+    filtered, query, kv, low, high = project(
         normed, before, after, norm_gain, in_weight, conv_taps, cosine, sine, tp
     )
 
-    before = lax.ppermute(kv[:, -WINDOW:], "sp", up)
-    after = lax.ppermute(kv[:, :WINDOW], "sp", down)
+    before = lax.ppermute(high, "sp", up)
+    after = lax.ppermute(low, "sp", down)
     conv_tok = lax.all_to_all(filtered, "tp", 0, 0, tiled=True)
     attn, log_total = attend_inner(sink_logit, query, kv, tp)
     attn, log_total = attend_edge(
@@ -516,13 +543,20 @@
     attn_tok = lax.all_to_all(attn, "tp", 0, 0, tiled=True)
 
     rows = seqs * length // tp
-    out_weight = in_hbm(out_weight)
+    own_weight, _ = lax.optimization_barrier((own_weight, log_total))
+    other_weight = lax.ppermute(own_weight, "tp", [(i, i ^ 1) for i in range(tp)])
+    weights = [
+        in_hbm(w.reshape(sp, tp // 2, out_piece.shape[0], LANES))
+        for w in (own_weight, other_weight)
+    ]
+    core = (lax.axis_index("tp") % 2).astype(jnp.int32).reshape(1)
     part = mix(
-        mix_conv_kernel, conv_tok.reshape(tp, rows, LANES), out_weight, out_weight, 0, F32, 4,
+        mix_conv_kernel, core, conv_tok.reshape(tp, rows, LANES), weights, weights, 0, F32, 4,
         "mix_conv", [pltpu.VMEM((rows, tp * LANES), BF16)],
     )
     mixed = mix(
-        mix_attn_kernel, attn_tok.reshape(tp, rows, LANES), in_hbm(part), out_weight, 1, BF16, 8, "mix_attn"
+        mix_attn_kernel, core, attn_tok.reshape(tp, rows, LANES), [in_hbm(part)], weights, 1, BF16,
+        4, "mix_attn",
     )
     return mixed.reshape(seqs, length // tp, width), log_total
 

time: 133 us -> 152 us (1.14)
  blocking collectives: 0 us -> 18.3 us
  starting transfers between devices: 28.2 us -> 23.8 us
  local copies, waits for them, and re-layouts: 3.58 us -> 6.15 us
  waiting for transfers between devices: 22 us -> 23.8 us
    all_to_all x0 -> x1, blocking collectives: none -> 18.3 us  [on_device(): conv_tok = lax.all_to_all(filtered, 'tp', 0, 0, tiled=True)]
    all_gather x1, waiting for transfers between devices: 0.3 us -> 6.97 us  [on_device(): lax.all_gather(out_piece, ('sp', 'tp'), axis=0, tiled=True, axis_index_gr...]
    all_to_all x1 -> x0, starting transfers between devices: 6.08 us -> none  [on_device(): conv_tok = lax.all_to_all(filtered, 'tp', 0, 0, tiled=True)]
    all_to_all x1 -> x0, waiting for transfers between devices: 5.34 us -> none  [on_device(): conv_tok = lax.all_to_all(filtered, 'tp', 0, 0, tiled=True)]
    unnamed x4 -> x16, local copies, waits for them, and re-layouts: 0.01 us -> 5.07 us
    ppermute x2 -> x3, starting transfers between devices: 3.57 us -> 6.22 us  [the longest x1 2.85 us: on_device(): before = lax.ppermute(high, 'sp', up)]
  transfers between devices with their start and end apart: 8 -> 8, of which waited for: 6 -> 5; matrix products, arithmetic and copies ran while one was open for 4% -> 3% of each run, Pallas kernels for 41% -> 36%
where the time goes in v3:
time: 152 us; the launch traced here: 151 us
  Pallas kernels  62.2 us (41%)
  starting transfers between devices  23.8 us (16%)
  waiting for transfers between devices  23.8 us (16%)
  blocking collectives  18.3 us (12%)
  between operations  14.1 us (9%)
  local copies, waits for them, and re-layouts  6.15 us (4%)
  other arithmetic  3.18 us (2%)
    all_to_all x1, blocking collectives, on_device(): conv_tok = lax.all_to_all(filtered, 'tp', 0, 0, tiled=True)  18.3 us
    pallas_call x1, Pallas kernels, project(): pl.pallas_call(functools.partial(project_kernel, sub=sub, chunk=chunk), g...  18.1 us
    pallas_call x1, Pallas kernels, norm_tokens(): pl.pallas_call(norm_kernel, grid=(rows // block,), in_specs=[pl.BlockSpec...  17.2 us
    pallas_call x2, Pallas kernels, mix(): pl.pallas_call(kernel, grid=(groups // cols,), in_specs=[pl.BlockSpec(mem...  13.7 us
    all_to_all x1, starting transfers between devices, on_device(): in_weight = lax.all_to_all(in_piece, 'sp', 0, 0, tiled=True)  8.43 us
    pallas_call x1, Pallas kernels, attend_inner(): pl.pallas_call(inner_kernel, grid=(seqs,), in_specs=[pl.BlockSpec(memory_...  7.74 us
    all_to_all x1, waiting for transfers between devices, on_device(): attn_tok = lax.all_to_all(attn, 'tp', 0, 0, tiled=True)  7.72 us
    all_gather x1, waiting for transfers between devices, on_device(): lax.all_gather(out_piece, ('sp', 'tp'), axis=0, tiled=True, axis_index_gr...  6.97 us
  transfers between devices with their start and end apart: 8, of which 5 were waited for; matrix products, arithmetic and copies ran while one was open for 3% of the time, Pallas kernels for 36%

profile of v3, /device:TPU:1, one launch (start us, length us, event | category | flops | bytes accessed | tf_op | source)
XLA Modules:
  0.0 151.5 jit_solution(14715691383711087717)
XLA Ops:
  7.2 1.6 %pack.1 = (bf16[272,128]{1,0:T(8,128)(2,1)}, bf16[16,128,512]{2,1,0:T(8,128)(2,1)S(1)}) custom-call(bf16[128,128]{1,0:T(8,128)(2,1)} %value_ref.1, bf16[128,128]{1,0:T(8,128)(2,1)} %gate_ref.1, bf16[128,128]{1,0:T(8,128)(2,1)} %query_ref.1, bf16[64,128]{1,0:T(8,128)(2,1)} %bitcast.18, bf16[64,128]{1,0:T(8,128)(2,1)} %bitcast.19, bf16[128,128]{1,0:T(8,128)(2,1)} %conv_ref.1, ...), custom_call_target="tpu_custom_call" | custom-call | tf_op jit(solution)/shard_map/pack/pallas_call | solution.py:468
  8.8 1.3 copy-done
  10.2 8.4 %all-to-all-start = ((bf16[16,128,512]{2,1,0:T(8,128)(2,1)}), bf16[16,128,512]{2,1,0:T(8,128)(2,1)S(1)}, u32[]{:S(2)}, u32[]{:S(2)}) async-start(bf16[16,128,512]{2,1,0:T(8,128)(2,1)} %copy-done), calls=%async_computation | async-start | bytes 4194304 | tf_op jit(solution)/shard_map/all_to_all | solution.py:526
  18.6 1.1 fusion.5
  19.7 3.3 %collective-permute-start = (bf16[4,16,2048]{2,1,0:T(8,128)(2,1)S(1)}, bf16[4,16,2048]{2,1,0:T(8,128)(2,1)S(1)}, u32[]{:S(2)}, u32[]{:S(2)}) collective-permute-start(bf16[4,16,2048]{2,1,0:T(8,128)(2,1)S(1)} %get-tuple-element.27), channel_id=1, source_target_pairs={{0,8},{8,16},{16,24},{24,32},{32,40},{40,48},{48,56},{56,64},{64,7... | collective-permute-start | bytes 786440 | tf_op jit(solution)/shard_map/ppermute | solution.py:528
  23.0 1.3 collective-permute-start.1
  24.3 17.2 %norm_tokens.1.x_ref = bf16[4096,2048]{1,0:T(8,128)(2,1)} custom-call(bf16[4096,2048]{1,0:T(8,128)(2,1)} %bitcast.16, bf16[1,2048]{1,0:T(2,128)(2,1)S(1)} %reshape.63.gain_ref), custom_call_target="tpu_custom_call" | custom-call | flops 335544320 | bytes 33554432 | tf_op jit(solution)/shard_map/norm_tokens/pallas_call | solution.py:48
  41.6 3.1 %fusion = (f32[1024,128]{1,0:T(8,128)}, f32[1024,128]{1,0:T(8,128)}) fusion(f32[128]{0:T(128)S(1)} %get-tuple-element.30, f32[128]{0:T(128)S(1)} %get-tuple-element.31, f32[1024]{0:T(1024)S(1)} %add_convert_fusion), kind=kLoop, calls=%fused_computation.2 | loop fusion | flops 262144 | bytes 1053696 | tf_op jit(solution)/shard_map/mul | solution.py:493
  44.6 6.1 %collective-permute-done.before_ref = bf16[4,16,2048]{2,1,0:T(8,128)(2,1)S(1)} collective-permute-done((bf16[4,16,2048]{2,1,0:T(8,128)(2,1)S(1)}, bf16[4,16,2048]{2,1,0:T(8,128)(2,1)S(1)}, u32[]{:S(2)}, u32[]{:S(2)}) %collective-permute-start) | collective-permute-done | bytes 262176 | tf_op jit(solution)/shard_map/ppermute | solution.py:528
  50.8 1.6 %collective-permute-done.1.after_ref = bf16[4,16,2048]{2,1,0:T(8,128)(2,1)S(1)} collective-permute-done((bf16[4,16,2048]{2,1,0:T(8,128)(2,1)S(1)}, bf16[4,16,2048]{2,1,0:T(8,128)(2,1)S(1)}, u32[]{:S(2)}, u32[]{:S(2)}) %collective-permute-start.1) | collective-permute-done | bytes 262176 | tf_op jit(solution)/shard_map/ppermute | solution.py:529
  53.1 1.0 copy-done.1
  56.2 18.1 %project.1 = (bf16[8,4,128,128]{3,2,1,0:T(8,128)(2,1)S(1)}, bf16[4,1024,128]{2,1,0:T(8,128)(2,1)}, bf16[4,1024,128]{2,1,0:T(8,128)(2,1)}, bf16[4,128,128]{2,1,0:T(8,128)(2,1)S(1)}, bf16[4,128,128]{2,1,0:T(8,128)(2,1)S(1)}) custom-call(bf16[4096,2048]{1,0:T(8,128)(2,1)} %norm_tokens.1.x_ref, bf16[4,16,2048]{2,1,0:T(8,128)(2,1)S(1)} %collective-permute-done.before_ref, ...), custom_call_target="tpu_custom_call" | custom-call | flops 8589934592 | bytes 16777216 | tf_op jit(solution)/shard_map/project/pallas_call | solution.py:137
  74.3 2.8 %collective-permute-start.2 = (bf16[4,128,128]{2,1,0:T(8,128)(2,1)S(1)}, bf16[4,128,128]{2,1,0:T(8,128)(2,1)S(1)}, u32[]{:S(2)}, u32[]{:S(2)}) collective-permute-start(bf16[4,128,128]{2,1,0:T(8,128)(2,1)S(1)} %get-tuple-element.16), channel_id=1, source_target_pairs={{0,8},{8,16},{16,24},{24,32},{32,40},{40,48},{48,56},{56,64},{64,7... | collective-permute-start | bytes 393224 | tf_op jit(solution)/shard_map/ppermute | solution.py:536
  77.1 1.3 collective-permute-start.3
  78.5 7.7 %attend_inner.1 = (bf16[8,4,128,128]{3,2,1,0:T(8,128)(2,1)}, f32[4,2,1024]{2,1,0:T(2,128)}) custom-call(f32[2]{0:T(128)S(1)} %copy-done.3, bf16[4,1024,128]{2,1,0:T(8,128)(2,1)} %get-tuple-element.15.q_ref.q_low_ref.q_high_ref, bf16[4,1024,128]{2,1,0:T(8,128)(2,1)} %get-tuple-element.17.kv_ref.kv_low_ref.kv_high_ref), custom_call_target="tpu_custom_call" | custom-call | flops 1006632960 | bytes 3145728 | tf_op jit(solution)/shard_map/attend_inner/pallas_call | solution.py:262
  86.3 1.3 collective-permute-done.3.after_ref
  87.5 3.9 %attend_edge.1 = (bf16[8,4,128,128]{3,2,1,0:T(8,128)(2,1)}, f32[4,2,1024]{2,1,0:T(2,128)}) custom-call(s32[2]{0:T(128)S(1)} %pad_add_fusion.place_ref, f32[2]{0:T(128)S(1)} %copy-done.3, bf16[4,1024,128]{2,1,0:T(8,128)(2,1)} %get-tuple-element.15.q_ref.q_low_ref.q_high_ref, ...), custom_call_target="tpu_custom_call", output_to_operand_aliasing={{0}: (8, {}), {1}: (9, {})} | custom-call | flops 251658240 | bytes 1048576 | tf_op jit(solution)/shard_map/attend_edge/pallas_call | solution.py:346
  91.4 7.0 %all-gather.2.cloned.1.call-done = bf16[17408,128]{1,0:T(8,128)(2,1)} async-done(((bf16[272,128]{1,0:T(8,128)(2,1)}), bf16[17408,128]{1,0:T(8,128)(2,1)}) %all-gather.2.cloned.1.call-update) | async-done | bytes 4456464 | tf_op jit(solution)/shard_map/all_gather | solution.py:523
  98.4 2.1 %collective-permute-start.4 = (bf16[17408,128]{1,0:T(8,128)(2,1)}, bf16[17408,128]{1,0:T(8,128)(2,1)}, u32[]{:S(2)}, u32[]{:S(2)}) collective-permute-start(bf16[17408,128]{1,0:T(8,128)(2,1)} %all-gather.2.cloned.1.call-done), channel_id=1, source_target_pairs={{0,1},{1,0},{2,3},{3,2},{4,5},{5,4},{6,7},{7,6},{8,9},{9,8},{10,11... | collective-permute-start | bytes 13369352 | tf_op jit(solution)/shard_map/ppermute | solution.py:547
  100.5 18.3 %all_to_all.15 = bf16[8,4,128,128]{3,2,1,0:T(8,128)(2,1)S(1)} all-to-all(bf16[8,4,128,128]{3,2,1,0:T(8,128)(2,1)S(1)} %get-tuple-element.22), channel_id=1, replica_groups=mesh['sp'=16,'tp'=8] {'tp'}, dimensions={0} | all-to-all | bytes 2097152 | tf_op jit(solution)/shard_map/all_to_all | solution.py:538
  118.7 4.5 %all-to-all-start.1 = ((bf16[8,4,128,128]{3,2,1,0:T(8,128)(2,1)}), bf16[8,4,128,128]{3,2,1,0:T(8,128)(2,1)S(1)}, u32[]{:S(2)}, u32[]{:S(2)}) async-start(bf16[8,4,128,128]{3,2,1,0:T(8,128)(2,1)} %get-tuple-element.21), calls=%async_computation.1 | async-start | bytes 2097152 | tf_op jit(solution)/shard_map/all_to_all | solution.py:543
  123.2 7.3 %mix_conv.1.part_ref = f32[512,2048]{1,0:T(8,128)} custom-call(s32[1]{0:T(128)} %bitcast.core_ref, bf16[8,512,128]{2,1,0:T(8,128)(2,1)S(1)} %bitcast.12, bf16[16,4,272,128]{3,2,1,0:T(8,128)(2,1)} %bitcast.13, bf16[16,4,272,128]{3,2,1,0:T(8,128)(2,1)} %bitcast.9.other_gain_ref.other_ref, bf16[16,4,272,128]{3,2,1,0:T(8,128)(2,1)} %bitcast.14, ...), custom_call_target="tpu_custom_call" | custom-call | flops 2147483648 | bytes 4456448 | tf_op jit(solution)/shard_map/mix_conv/pallas_call | solution.py:429
  130.5 7.7 %all-to-all-done.1 = bf16[8,4,128,128]{3,2,1,0:T(8,128)(2,1)S(1)} async-done(((bf16[8,4,128,128]{3,2,1,0:T(8,128)(2,1)}), bf16[8,4,128,128]{3,2,1,0:T(8,128)(2,1)S(1)}, u32[]{:S(2)}, u32[]{:S(2)}) %all-to-all-start.1) | async-done | bytes 1048608 | tf_op jit(solution)/shard_map/all_to_all | solution.py:543
  138.2 6.4 %mix_attn.1 = bf16[512,2048]{1,0:T(8,128)(2,1)} custom-call(s32[1]{0:T(128)} %bitcast.core_ref, bf16[8,512,128]{2,1,0:T(8,128)(2,1)S(1)} %bitcast.11, f32[512,2048]{1,0:T(8,128)} %mix_conv.1.part_ref, bf16[16,4,272,128]{3,2,1,0:T(8,128)(2,1)} %bitcast.15, bf16[16,4,272,128]{3,2,1,0:T(8,128)(2,1)} %bitcast.9.other_gain_ref.other_ref), custom_call_target="tpu_custom_call" | custom-call | flops 2147483648 | bytes 4456448 | tf_op jit(solution)/shard_map/mix_attn/pallas_call | solution.py:429
  (23 shorter events, 2.9 us)
Async XLA Ops:
  7.2 17.1 %copy-start.7 = (bf16[2048]{0:T(1024)(128)(2,1)S(1)}, bf16[2048]{0:T(1024)(128)(2,1)}, u32[]{:S(2)}) copy-start(bf16[2048]{0:T(1024)(128)(2,1)} %param.13) | copy-start | bytes 12292
  7.2 91.2 %all-gather.2.cloned.1.call-start = ((), (), s32[]{:S(2)}) async-start(), calls=%async_computation.3 | async-start | bytes 4526080 | tf_op jit(solution)/shard_map/all_gather | solution.py:523
  8.8 1.3 copy-start
  10.2 43.0 %all-to-all-start = ((bf16[16,128,512]{2,1,0:T(8,128)(2,1)}), bf16[16,128,512]{2,1,0:T(8,128)(2,1)S(1)}, u32[]{:S(2)}, u32[]{:S(2)}) async-start(bf16[16,128,512]{2,1,0:T(8,128)(2,1)} %copy-done), calls=%async_computation | async-start | bytes 4194304 | tf_op jit(solution)/shard_map/all_to_all | solution.py:526
  19.7 31.1 %collective-permute-start = (bf16[4,16,2048]{2,1,0:T(8,128)(2,1)S(1)}, bf16[4,16,2048]{2,1,0:T(8,128)(2,1)S(1)}, u32[]{:S(2)}, u32[]{:S(2)}) collective-permute-start(bf16[4,16,2048]{2,1,0:T(8,128)(2,1)S(1)} %get-tuple-element.27), channel_id=1, source_target_pairs={{0,8},{8,16},{16,24},{24,32},{32,40},{40,48},{48,56},{56,64},{64,7... | collective-permute-start | bytes 786440 | tf_op jit(solution)/shard_map/ppermute | solution.py:528
  23.0 29.5 %collective-permute-start.1 = (bf16[4,16,2048]{2,1,0:T(8,128)(2,1)S(1)}, bf16[4,16,2048]{2,1,0:T(8,128)(2,1)S(1)}, u32[]{:S(2)}, u32[]{:S(2)}) collective-permute-start(bf16[4,16,2048]{2,1,0:T(8,128)(2,1)S(1)} %get-tuple-element.26), channel_id=1, source_target_pairs={{8,0},{16,8},{24,16},{32,24},{40,32},{48,40},{56,48},{64,56},{72,6... | collective-permute-start | bytes 786440 | tf_op jit(solution)/shard_map/ppermute | solution.py:529
  24.3 28.8 %copy-start.6 = (bf16[31,128]{1,0:T(8,128)(2,1)S(1)}, bf16[31,128]{1,0:T(8,128)(2,1)}, u32[]{:S(2)}) copy-start(bf16[31,128]{1,0:T(8,128)(2,1)} %taps_ref.1) | copy-start | bytes 23812
  52.4 0.7 copy-start.4
  53.1 1.0 copy-start.1
  54.2 1.0 copy-start.2
  55.2 0.9 copy-start.5
  56.2 22.3 %copy-start.3 = (f32[2]{0:T(128)S(1)}, f32[2]{0:T(128)}, u32[]{:S(2)}) copy-start(f32[2]{0:T(128)} %sink_ref.3) | copy-start | bytes 28
  74.3 12.0 %collective-permute-start.2 = (bf16[4,128,128]{2,1,0:T(8,128)(2,1)S(1)}, bf16[4,128,128]{2,1,0:T(8,128)(2,1)S(1)}, u32[]{:S(2)}, u32[]{:S(2)}) collective-permute-start(bf16[4,128,128]{2,1,0:T(8,128)(2,1)S(1)} %get-tuple-element.16), channel_id=1, source_target_pairs={{0,8},{8,16},{16,24},{24,32},{32,40},{40,48},{48,56},{56,64},{64,7... | collective-permute-start | bytes 393224 | tf_op jit(solution)/shard_map/ppermute | solution.py:536
  77.1 10.4 %collective-permute-start.3 = (bf16[4,128,128]{2,1,0:T(8,128)(2,1)S(1)}, bf16[4,128,128]{2,1,0:T(8,128)(2,1)S(1)}, u32[]{:S(2)}, u32[]{:S(2)}) collective-permute-start(bf16[4,128,128]{2,1,0:T(8,128)(2,1)S(1)} %get-tuple-element.18), channel_id=1, source_target_pairs={{8,0},{16,8},{24,16},{32,24},{40,32},{48,40},{56,48},{64,56},{72,6... | collective-permute-start | bytes 393224 | tf_op jit(solution)/shard_map/ppermute | solution.py:537
  98.4 24.9 %collective-permute-start.4 = (bf16[17408,128]{1,0:T(8,128)(2,1)}, bf16[17408,128]{1,0:T(8,128)(2,1)}, u32[]{:S(2)}, u32[]{:S(2)}) collective-permute-start(bf16[17408,128]{1,0:T(8,128)(2,1)} %all-gather.2.cloned.1.call-done), channel_id=1, source_target_pairs={{0,1},{1,0},{2,3},{3,2},{4,5},{5,4},{6,7},{7,6},{8,9},{9,8},{10,11... | collective-permute-start | bytes 13369352 | tf_op jit(solution)/shard_map/ppermute | solution.py:547
  118.7 19.5 %all-to-all-start.1 = ((bf16[8,4,128,128]{3,2,1,0:T(8,128)(2,1)}), bf16[8,4,128,128]{3,2,1,0:T(8,128)(2,1)S(1)}, u32[]{:S(2)}, u32[]{:S(2)}) async-start(bf16[8,4,128,128]{3,2,1,0:T(8,128)(2,1)} %get-tuple-element.21), calls=%async_computation.1 | async-start | bytes 2097152 | tf_op jit(solution)/shard_map/all_to_all | solution.py:543
Sparse Core Ops, SparseCore 0:
  10.9 87.4 all-gather.1

commit v4 on v3

--- a/solution.py
+++ b/solution.py
@@ -417,7 +417,7 @@
     out_ref[...] = total.astype(BF16)
 
 
-def mix(kernel, core, x, extras, weights, which, out_dtype, cols, name, scratch=()):
+def mix(kernel, core, x, extras, weights, which, out_dtype, cols, scratch=()):
     sources, rows, _ = x.shape
     groups, half, height, _ = weights[0].shape
     block = pl.BlockSpec((rows, cols * LANES), lambda n: (0, n))
@@ -444,7 +444,6 @@
             transcendentals=0,
             bytes_accessed=2 * weights[0].size,
         ),
-        name=name,
     )(core, x, *extras, *weights)
 
 
@@ -543,7 +542,7 @@
     attn_tok = lax.all_to_all(attn, "tp", 0, 0, tiled=True)
 
     rows = seqs * length // tp
-    own_weight, _ = lax.optimization_barrier((own_weight, log_total))
+    own_weight, conv_tok, _ = lax.optimization_barrier((own_weight, conv_tok, log_total))
     other_weight = lax.ppermute(own_weight, "tp", [(i, i ^ 1) for i in range(tp)])
     weights = [
         in_hbm(w.reshape(sp, tp // 2, out_piece.shape[0], LANES))
@@ -552,11 +551,11 @@
     core = (lax.axis_index("tp") % 2).astype(jnp.int32).reshape(1)
     part = mix(
         mix_conv_kernel, core, conv_tok.reshape(tp, rows, LANES), weights, weights, 0, F32, 4,
-        "mix_conv", [pltpu.VMEM((rows, tp * LANES), BF16)],
+        [pltpu.VMEM((rows, tp * LANES), BF16)],
     )
     mixed = mix(
         mix_attn_kernel, core, attn_tok.reshape(tp, rows, LANES), [in_hbm(part)], weights, 1, BF16,
-        4, "mix_attn",
+        4,
     )
     return mixed.reshape(seqs, length // tp, width), log_total
 
@@ -576,6 +575,7 @@
         P("tp", "sp"),
         P("tp", "sp"),
     )
+
     return jax.shard_map(
         on_device,
         mesh=mesh,

time: 152 us -> 139 us (0.914)
  blocking collectives: 18.3 us -> 0 us
  waiting for transfers between devices: 23.8 us -> 28 us
  starting transfers between devices: 23.8 us -> 26.9 us
  local copies, waits for them, and re-layouts: 6.15 us -> 4.57 us
    all_to_all x1 -> x0, blocking collectives: 18.3 us -> none  [on_device(): conv_tok = lax.all_to_all(filtered, 'tp', 0, 0, tiled=True)]
    all_to_all x0 -> x1, waiting for transfers between devices: none -> 8.35 us  [on_device(): conv_tok = lax.all_to_all(filtered, 'tp', 0, 0, tiled=True)]
    all_to_all x0 -> x1, starting transfers between devices: none -> 6.22 us  [on_device(): conv_tok = lax.all_to_all(filtered, 'tp', 0, 0, tiled=True)]
    all_to_all x1, waiting for transfers between devices: 7.72 us -> 3.73 us  [on_device(): attn_tok = lax.all_to_all(attn, 'tp', 0, 0, tiled=True)]
    ppermute x1, waiting for transfers between devices: 0.01 us -> 3.98 us  [on_device(): lax.ppermute(own_weight, 'tp', [(i, i ^ 1) for i in range(tp)])]
    all_gather x1, waiting for transfers between devices: 6.97 us -> 3.03 us  [on_device(): lax.all_gather(out_piece, ('sp', 'tp'), axis=0, tiled=True, axis_index_gr...]
    unnamed x16 -> x10, local copies, waits for them, and re-layouts: 5.07 us -> 2.68 us
    ppermute x1, starting transfers between devices: 2.08 us -> 0.51 us  [on_device(): lax.ppermute(own_weight, 'tp', [(i, i ^ 1) for i in range(tp)])]
  transfers between devices with their start and end apart: 8 -> 9, of which waited for: 5 -> 7; matrix products, arithmetic and copies ran while one was open for 3% -> 3% of each run, Pallas kernels for 36% -> 39%
where the time goes in v4:
time: 139 us; the launch traced here: 138 us
  Pallas kernels  62.2 us (45%)
  waiting for transfers between devices  28 us (20%)
  starting transfers between devices  26.9 us (19%)
  between operations  14.2 us (10%)
  local copies, waits for them, and re-layouts  4.57 us (3%)
  other arithmetic  1.99 us (1%)
    pallas_call x1, Pallas kernels, project(): pl.pallas_call(functools.partial(project_kernel, sub=sub, chunk=chunk), g...  18.2 us
    pallas_call x1, Pallas kernels, norm_tokens(): pl.pallas_call(norm_kernel, grid=(rows // block,), in_specs=[pl.BlockSpec...  17.2 us
    pallas_call x2, Pallas kernels, mix(): pl.pallas_call(kernel, grid=(groups // cols,), in_specs=[pl.BlockSpec(mem...  13.6 us
    all_to_all x1, starting transfers between devices, on_device(): in_weight = lax.all_to_all(in_piece, 'sp', 0, 0, tiled=True)  8.43 us
    all_to_all x1, waiting for transfers between devices, on_device(): conv_tok = lax.all_to_all(filtered, 'tp', 0, 0, tiled=True)  8.35 us
    pallas_call x1, Pallas kernels, attend_inner(): pl.pallas_call(inner_kernel, grid=(seqs,), in_specs=[pl.BlockSpec(memory_...  7.71 us
    ppermute x1, waiting for transfers between devices, on_device(): before = lax.ppermute(tokens[:, -EDGE:], 'sp', up)  6.63 us
    all_to_all x1, starting transfers between devices, on_device(): conv_tok = lax.all_to_all(filtered, 'tp', 0, 0, tiled=True)  6.22 us
  transfers between devices with their start and end apart: 9, of which 7 were waited for; matrix products, arithmetic and copies ran while one was open for 3% of the time, Pallas kernels for 39%

profile of v4, /device:TPU:1, one launch (start us, length us, event | category | flops | bytes accessed | tf_op | source)
XLA Modules:
  0.0 137.8 jit_solution(6674596479698242611)
XLA Ops:
  7.2 1.6 %pack.1 = (bf16[272,128]{1,0:T(8,128)(2,1)}, bf16[16,128,512]{2,1,0:T(8,128)(2,1)S(1)}) custom-call(bf16[128,128]{1,0:T(8,128)(2,1)} %value_ref.1, bf16[128,128]{1,0:T(8,128)(2,1)} %gate_ref.1, bf16[128,128]{1,0:T(8,128)(2,1)} %query_ref.1, bf16[64,128]{1,0:T(8,128)(2,1)} %bitcast.18, bf16[64,128]{1,0:T(8,128)(2,1)} %bitcast.19, bf16[128,128]{1,0:T(8,128)(2,1)} %conv_ref.1, ...), custom_call_target="tpu_custom_call" | custom-call | tf_op jit(solution)/shard_map/pack/pallas_call | solution.py:467
  8.8 1.3 copy-done
  10.1 8.4 %all-to-all-start = ((bf16[16,128,512]{2,1,0:T(8,128)(2,1)}), bf16[16,128,512]{2,1,0:T(8,128)(2,1)S(1)}, u32[]{:S(2)}, u32[]{:S(2)}) async-start(bf16[16,128,512]{2,1,0:T(8,128)(2,1)} %copy-done), calls=%async_computation | async-start | bytes 4194304 | tf_op jit(solution)/shard_map/all_to_all | solution.py:525
  18.6 1.9 %fusion.5 = (bf16[4,16,2048]{2,1,0:T(8,128)(2,1)}, bf16[4,16,2048]{2,1,0:T(8,128)(2,1)}) fusion(bf16[4,1024,2048]{2,1,0:T(8,128)(2,1)} %param.12), kind=kLoop, calls=%fused_computation.12 | loop fusion | bytes 1048576 | tf_op jit(solution)/shard_map/slice | solution.py:528
  20.5 3.3 %collective-permute-start = (bf16[4,16,2048]{2,1,0:T(8,128)(2,1)}, bf16[4,16,2048]{2,1,0:T(8,128)(2,1)S(1)}, u32[]{:S(2)}, u32[]{:S(2)}) collective-permute-start(bf16[4,16,2048]{2,1,0:T(8,128)(2,1)} %get-tuple-element.29), channel_id=1, source_target_pairs={{0,8},{8,16},{16,24},{24,32},{32,40},{40,48},{48,56},{56,64},{64,7... | collective-permute-start | bytes 786440 | tf_op jit(solution)/shard_map/ppermute | solution.py:527
  23.7 1.3 collective-permute-start.1
  25.1 17.2 %norm_tokens.1.x_ref = bf16[4096,2048]{1,0:T(8,128)(2,1)} custom-call(bf16[4096,2048]{1,0:T(8,128)(2,1)} %bitcast.16, bf16[1,2048]{1,0:T(2,128)(2,1)S(1)} %reshape.63.gain_ref), custom_call_target="tpu_custom_call" | custom-call | flops 335544320 | bytes 33554432 | tf_op jit(solution)/shard_map/norm_tokens/pallas_call | solution.py:48
  42.3 1.9 %fusion = (f32[1024,128]{1,0:T(8,128)S(1)}, f32[1024,128]{1,0:T(8,128)S(1)}) fusion(f32[128]{0:T(128)S(1)} %get-tuple-element.32, f32[128]{0:T(128)S(1)} %get-tuple-element.33, f32[1024]{0:T(1024)S(1)} %add_convert_fusion), kind=kLoop, calls=%fused_computation.2 | loop fusion | flops 262144 | bytes 1053696 | tf_op jit(solution)/shard_map/mul | solution.py:492
  44.2 6.6 %collective-permute-done.before_ref = bf16[4,16,2048]{2,1,0:T(8,128)(2,1)S(1)} collective-permute-done((bf16[4,16,2048]{2,1,0:T(8,128)(2,1)}, bf16[4,16,2048]{2,1,0:T(8,128)(2,1)S(1)}, u32[]{:S(2)}, u32[]{:S(2)}) %collective-permute-start) | collective-permute-done | bytes 262176 | tf_op jit(solution)/shard_map/ppermute | solution.py:527
  50.9 1.6 %collective-permute-done.1.after_ref = bf16[4,16,2048]{2,1,0:T(8,128)(2,1)} collective-permute-done((bf16[4,16,2048]{2,1,0:T(8,128)(2,1)}, bf16[4,16,2048]{2,1,0:T(8,128)(2,1)}, u32[]{:S(2)}, u32[]{:S(2)}) %collective-permute-start.1) | collective-permute-done | bytes 262176 | tf_op jit(solution)/shard_map/ppermute | solution.py:528
  52.5 0.7 copy-done.3
  53.2 18.2 %project.1 = (bf16[8,4,128,128]{3,2,1,0:T(8,128)(2,1)}, bf16[4,1024,128]{2,1,0:T(8,128)(2,1)}, bf16[4,1024,128]{2,1,0:T(8,128)(2,1)}, bf16[4,128,128]{2,1,0:T(8,128)(2,1)S(1)}, bf16[4,128,128]{2,1,0:T(8,128)(2,1)S(1)}) custom-call(bf16[4096,2048]{1,0:T(8,128)(2,1)} %norm_tokens.1.x_ref, bf16[4,16,2048]{2,1,0:T(8,128)(2,1)S(1)} %collective-permute-done.before_ref, ...), custom_call_target="tpu_custom_call" | custom-call | flops 8589934592 | bytes 16777216 | tf_op jit(solution)/shard_map/project/pallas_call | solution.py:137
  72.1 6.2 %all-to-all-start.2 = ((bf16[8,4,128,128]{3,2,1,0:T(8,128)(2,1)}), bf16[8,4,128,128]{3,2,1,0:T(8,128)(2,1)S(1)}, u32[]{:S(2)}, u32[]{:S(2)}) async-start(bf16[8,4,128,128]{3,2,1,0:T(8,128)(2,1)} %get-tuple-element.24), calls=%async_computation.2 | async-start | bytes 2097152 | tf_op jit(solution)/shard_map/all_to_all | solution.py:537
  78.3 2.1 %collective-permute-start.2 = (bf16[4,128,128]{2,1,0:T(8,128)(2,1)}, bf16[4,128,128]{2,1,0:T(8,128)(2,1)S(1)}, u32[]{:S(2)}, u32[]{:S(2)}) collective-permute-start(bf16[4,128,128]{2,1,0:T(8,128)(2,1)} %copy-done.2), channel_id=1, source_target_pairs={{0,8},{8,16},{16,24},{24,32},{32,40},{40,48},{48,56},{56,64},{64,7... | collective-permute-start | bytes 393224 | tf_op jit(solution)/shard_map/ppermute | solution.py:535
  80.4 1.5 %collective-permute-start.3 = (bf16[4,128,128]{2,1,0:T(8,128)(2,1)S(1)}, bf16[4,128,128]{2,1,0:T(8,128)(2,1)S(1)}, u32[]{:S(2)}, u32[]{:S(2)}) collective-permute-start(bf16[4,128,128]{2,1,0:T(8,128)(2,1)S(1)} %get-tuple-element.19), channel_id=1, source_target_pairs={{8,0},{16,8},{24,16},{32,24},{40,32},{48,40},{56,48},{64,56},{72,6... | collective-permute-start | bytes 393224 | tf_op jit(solution)/shard_map/ppermute | solution.py:536
  82.0 7.7 %attend_inner.1 = (bf16[8,4,128,128]{3,2,1,0:T(8,128)(2,1)}, f32[4,2,1024]{2,1,0:T(2,128)}) custom-call(f32[2]{0:T(128)S(1)} %copy-done.1, bf16[4,1024,128]{2,1,0:T(8,128)(2,1)} %get-tuple-element.16.q_ref.q_low_ref.q_high_ref, bf16[4,1024,128]{2,1,0:T(8,128)(2,1)} %get-tuple-element.18.kv_ref.kv_low_ref.kv_high_ref), custom_call_target="tpu_custom_call" | custom-call | flops 1006632960 | bytes 3145728 | tf_op jit(solution)/shard_map/attend_inner/pallas_call | solution.py:262
  90.3 3.9 %attend_edge.1 = (bf16[8,4,128,128]{3,2,1,0:T(8,128)(2,1)}, f32[4,2,1024]{2,1,0:T(2,128)}) custom-call(s32[2]{0:T(128)S(1)} %pad_add_fusion.place_ref, f32[2]{0:T(128)S(1)} %copy-done.1, bf16[4,1024,128]{2,1,0:T(8,128)(2,1)} %get-tuple-element.16.q_ref.q_low_ref.q_high_ref, ...), custom_call_target="tpu_custom_call", output_to_operand_aliasing={{0}: (8, {}), {1}: (9, {})} | custom-call | flops 251658240 | bytes 1048576 | tf_op jit(solution)/shard_map/attend_edge/pallas_call | solution.py:346
  94.2 8.4 %all-to-all-done.2 = bf16[8,4,128,128]{3,2,1,0:T(8,128)(2,1)S(1)} async-done(((bf16[8,4,128,128]{3,2,1,0:T(8,128)(2,1)}), bf16[8,4,128,128]{3,2,1,0:T(8,128)(2,1)S(1)}, u32[]{:S(2)}, u32[]{:S(2)}) %all-to-all-start.2) | async-done | bytes 1048608 | tf_op jit(solution)/shard_map/all_to_all | solution.py:537
  102.6 3.0 %all-gather.2.cloned.1.call-done = bf16[17408,128]{1,0:T(8,128)(2,1)} async-done(((bf16[272,128]{1,0:T(8,128)(2,1)}), bf16[17408,128]{1,0:T(8,128)(2,1)}) %all-gather.2.cloned.1.call-update) | async-done | bytes 4456464 | tf_op jit(solution)/shard_map/all_gather | solution.py:522
  106.1 3.5 %all-to-all-start.1 = ((bf16[8,4,128,128]{3,2,1,0:T(8,128)(2,1)}), bf16[8,4,128,128]{3,2,1,0:T(8,128)(2,1)S(1)}, u32[]{:S(2)}, u32[]{:S(2)}) async-start(bf16[8,4,128,128]{3,2,1,0:T(8,128)(2,1)} %get-tuple-element.22), calls=%async_computation.1 | async-start | bytes 2097152 | tf_op jit(solution)/shard_map/all_to_all | solution.py:542
  109.6 4.0 %collective-permute-done.4 = bf16[17408,128]{1,0:T(8,128)(2,1)} collective-permute-done((bf16[17408,128]{1,0:T(8,128)(2,1)}, bf16[17408,128]{1,0:T(8,128)(2,1)}, u32[]{:S(2)}, u32[]{:S(2)}) %collective-permute-start.4) | collective-permute-done | bytes 4456480 | tf_op jit(solution)/shard_map/ppermute | solution.py:546
  113.6 7.2 %shard_map.131.part_ref = f32[512,2048]{1,0:T(8,128)} custom-call(s32[1]{0:T(128)} %bitcast.core_ref, bf16[8,512,128]{2,1,0:T(8,128)(2,1)S(1)} %bitcast.11, bf16[16,4,272,128]{3,2,1,0:T(8,128)(2,1)} %bitcast.13, bf16[16,4,272,128]{3,2,1,0:T(8,128)(2,1)} %bitcast.9.other_gain_ref.other_ref, bf16[16,4,272,128]{3,2,1,0:T(8,128)(2,1)} %bitcast.14, ...), custom_call_target="tpu_custom_call" | custom-call | flops 2147483648 | bytes 4456448 | tf_op jit(solution)/shard_map/pallas_call | solution.py:429
  120.8 3.7 %all-to-all-done.1 = bf16[8,4,128,128]{3,2,1,0:T(8,128)(2,1)S(1)} async-done(((bf16[8,4,128,128]{3,2,1,0:T(8,128)(2,1)}), bf16[8,4,128,128]{3,2,1,0:T(8,128)(2,1)S(1)}, u32[]{:S(2)}, u32[]{:S(2)}) %all-to-all-start.1) | async-done | bytes 1048608 | tf_op jit(solution)/shard_map/all_to_all | solution.py:542
  124.6 6.4 %shard_map.132 = bf16[512,2048]{1,0:T(8,128)(2,1)} custom-call(s32[1]{0:T(128)} %bitcast.core_ref, bf16[8,512,128]{2,1,0:T(8,128)(2,1)S(1)} %bitcast.12, f32[512,2048]{1,0:T(8,128)} %shard_map.131.part_ref, bf16[16,4,272,128]{3,2,1,0:T(8,128)(2,1)} %bitcast.15, bf16[16,4,272,128]{3,2,1,0:T(8,128)(2,1)} %bitcast.9.other_gain_ref.other_ref), custom_call_target="tpu_custom_call" | custom-call | flops 2147483648 | bytes 4456448 | tf_op jit(solution)/shard_map/pallas_call | solution.py:429
  (18 shorter events, 2.0 us)
Async XLA Ops:
  7.2 17.9 %copy-start.4 = (bf16[2048]{0:T(1024)(128)(2,1)S(1)}, bf16[2048]{0:T(1024)(128)(2,1)}, u32[]{:S(2)}) copy-start(bf16[2048]{0:T(1024)(128)(2,1)} %param.13) | copy-start | bytes 12292
  7.2 98.4 %all-gather.2.cloned.1.call-start = ((), (), s32[]{:S(2)}) async-start(), calls=%async_computation.3 | async-start | bytes 4526080 | tf_op jit(solution)/shard_map/all_gather | solution.py:522
  8.8 1.3 copy-start
  10.1 42.4 %all-to-all-start = ((bf16[16,128,512]{2,1,0:T(8,128)(2,1)}), bf16[16,128,512]{2,1,0:T(8,128)(2,1)S(1)}, u32[]{:S(2)}, u32[]{:S(2)}) async-start(bf16[16,128,512]{2,1,0:T(8,128)(2,1)} %copy-done), calls=%async_computation | async-start | bytes 4194304 | tf_op jit(solution)/shard_map/all_to_all | solution.py:525
  20.5 30.4 %collective-permute-start = (bf16[4,16,2048]{2,1,0:T(8,128)(2,1)}, bf16[4,16,2048]{2,1,0:T(8,128)(2,1)S(1)}, u32[]{:S(2)}, u32[]{:S(2)}) collective-permute-start(bf16[4,16,2048]{2,1,0:T(8,128)(2,1)} %get-tuple-element.29), channel_id=1, source_target_pairs={{0,8},{8,16},{16,24},{24,32},{32,40},{40,48},{48,56},{56,64},{64,7... | collective-permute-start | bytes 786440 | tf_op jit(solution)/shard_map/ppermute | solution.py:527
  23.7 28.8 %collective-permute-start.1 = (bf16[4,16,2048]{2,1,0:T(8,128)(2,1)}, bf16[4,16,2048]{2,1,0:T(8,128)(2,1)}, u32[]{:S(2)}, u32[]{:S(2)}) collective-permute-start(bf16[4,16,2048]{2,1,0:T(8,128)(2,1)} %get-tuple-element.28), channel_id=1, source_target_pairs={{8,0},{16,8},{24,16},{32,24},{40,32},{48,40},{56,48},{64,56},{72,6... | collective-permute-start | bytes 786440 | tf_op jit(solution)/shard_map/ppermute | solution.py:528
  52.5 0.7 copy-start.3
  53.2 28.8 %copy-start.1 = (f32[2]{0:T(128)S(1)}, f32[2]{0:T(128)}, u32[]{:S(2)}) copy-start(f32[2]{0:T(128)} %sink_ref.3) | copy-start | bytes 28
  71.4 0.7 copy-start.2
  72.1 30.5 %all-to-all-start.2 = ((bf16[8,4,128,128]{3,2,1,0:T(8,128)(2,1)}), bf16[8,4,128,128]{3,2,1,0:T(8,128)(2,1)S(1)}, u32[]{:S(2)}, u32[]{:S(2)}) async-start(bf16[8,4,128,128]{3,2,1,0:T(8,128)(2,1)} %get-tuple-element.24), calls=%async_computation.2 | async-start | bytes 2097152 | tf_op jit(solution)/shard_map/all_to_all | solution.py:537
  78.3 11.4 %collective-permute-start.2 = (bf16[4,128,128]{2,1,0:T(8,128)(2,1)}, bf16[4,128,128]{2,1,0:T(8,128)(2,1)S(1)}, u32[]{:S(2)}, u32[]{:S(2)}) collective-permute-start(bf16[4,128,128]{2,1,0:T(8,128)(2,1)} %copy-done.2), channel_id=1, source_target_pairs={{0,8},{8,16},{16,24},{24,32},{32,40},{40,48},{48,56},{56,64},{64,7... | collective-permute-start | bytes 393224 | tf_op jit(solution)/shard_map/ppermute | solution.py:535
  80.4 9.9 %collective-permute-start.3 = (bf16[4,128,128]{2,1,0:T(8,128)(2,1)S(1)}, bf16[4,128,128]{2,1,0:T(8,128)(2,1)S(1)}, u32[]{:S(2)}, u32[]{:S(2)}) collective-permute-start(bf16[4,128,128]{2,1,0:T(8,128)(2,1)S(1)} %get-tuple-element.19), channel_id=1, source_target_pairs={{8,0},{16,8},{24,16},{32,24},{40,32},{48,40},{56,48},{64,56},{72,6... | collective-permute-start | bytes 393224 | tf_op jit(solution)/shard_map/ppermute | solution.py:536
  105.6 8.0 %collective-permute-start.4 = (bf16[17408,128]{1,0:T(8,128)(2,1)}, bf16[17408,128]{1,0:T(8,128)(2,1)}, u32[]{:S(2)}, u32[]{:S(2)}) collective-permute-start(bf16[17408,128]{1,0:T(8,128)(2,1)} %all-gather.2.cloned.1.call-done), channel_id=1, source_target_pairs={{0,1},{1,0},{2,3},{3,2},{4,5},{5,4},{6,7},{7,6},{8,9},{9,8},{10,11... | collective-permute-start | bytes 13369352 | tf_op jit(solution)/shard_map/ppermute | solution.py:546
  106.1 18.5 %all-to-all-start.1 = ((bf16[8,4,128,128]{3,2,1,0:T(8,128)(2,1)}), bf16[8,4,128,128]{3,2,1,0:T(8,128)(2,1)S(1)}, u32[]{:S(2)}, u32[]{:S(2)}) async-start(bf16[8,4,128,128]{3,2,1,0:T(8,128)(2,1)} %get-tuple-element.22), calls=%async_computation.1 | async-start | bytes 2097152 | tf_op jit(solution)/shard_map/all_to_all | solution.py:542
Sparse Core Ops, SparseCore 0:
  10.9 94.6 all-gather.1

commit v5 on v4

--- a/solution.py
+++ b/solution.py
@@ -384,10 +384,12 @@
     return jnp.concatenate([ref[i] for i in range(ref.shape[0])], axis=-1)
 
 
-def by_core(ref, core):
+def by_core(ref, meta_ref):
+    core, y = meta_ref[0], meta_ref[1]
     count = ref.shape[0] // 2
-    own = [ref[2 * i + core] for i in range(count)]
-    other = [ref[2 * i + 1 - core] for i in range(count)]
+    places = [2 * ((y - step + count) % count) for step in range(count)]
+    own = [ref[place + core] for place in places]
+    other = [ref[place + 1 - core] for place in places]
     return jnp.concatenate(own, axis=-1), jnp.concatenate(other, axis=-1)
 
 
@@ -395,26 +397,27 @@
     return jnp.concatenate([ref[c].reshape(-1, LANES) for c in range(ref.shape[0])], axis=-1)
 
 
-def mix_conv_kernel(core_ref, x_ref, own_gain_ref, other_gain_ref, own_ref, other_ref, out_ref, act_ref):
-    half = act_ref.shape[1] // 2
-
+def product(rows, own_ref, other_ref):
+    both = jnp.concatenate([columns(own_ref), columns(other_ref)], axis=0)
+    return jnp.dot(rows, both, preferred_element_type=F32)
+
+
+def mix_conv_kernel(
+    meta_ref, x_ref, own_gain_ref, other_gain_ref, own_ref, other_ref, out_ref, act_ref
+):
     @pl.when(pl.program_id(0) == 0)
     def _():
-        x = jnp.concatenate(by_core(x_ref, core_ref[0]), axis=-1)
+        x = jnp.concatenate(by_core(x_ref, meta_ref), axis=-1)
         gain = jnp.concatenate([side_by_side(own_gain_ref), side_by_side(other_gain_ref)], axis=-1)
         v = normalize(x, gain[0:1])
         act_ref[...] = (v / (1.0 + jnp.exp(-v))).astype(BF16)
 
-    total = jnp.dot(act_ref[:, :half], columns(own_ref), preferred_element_type=F32)
-    total = total + jnp.dot(act_ref[:, half:], columns(other_ref), preferred_element_type=F32)
-    out_ref[...] = total
-
-
-def mix_attn_kernel(core_ref, x_ref, part_ref, own_ref, other_ref, out_ref):
-    own, other = by_core(x_ref, core_ref[0])
-    total = part_ref[...] + jnp.dot(own, columns(own_ref), preferred_element_type=F32)
-    total = total + jnp.dot(other, columns(other_ref), preferred_element_type=F32)
-    out_ref[...] = total.astype(BF16)
+    out_ref[...] = product(act_ref[...], own_ref, other_ref)
+
+
+def mix_attn_kernel(meta_ref, x_ref, part_ref, own_ref, other_ref, out_ref):
+    rows = jnp.concatenate(by_core(x_ref, meta_ref), axis=-1)
+    out_ref[...] = (part_ref[...] + product(rows, own_ref, other_ref)).astype(BF16)
 
 
 def mix(kernel, core, x, extras, weights, which, out_dtype, cols, scratch=()):
@@ -516,13 +519,12 @@
         conv_value_weight, conv_gate_weight, query_weight, key_weight, value_weight,
         out_conv_weight, out_attn_weight, conv_gain, sp,
     )
-    same_core = [
-        [row * tp + col for row in range(sp) for col in range(core, tp, 2)] for core in range(2)
-    ]
-    own_weight = lax.all_gather(
-        out_piece, ("sp", "tp"), axis=0, tiled=True, axis_index_groups=same_core
-    )
     in_weight = lax.all_to_all(in_piece, "sp", 0, 0, tiled=True)
+    pieces = [out_piece]
+    for d in range(1, tp // 2):
+        ring = [(i, (i + 2 * d) % tp) for i in range(tp)]
+        pieces.append(lax.ppermute(out_piece, "tp", ring))
+    own_weight = lax.all_gather(jnp.concatenate(pieces, axis=0), "sp", axis=0, tiled=True)
 
     before = lax.ppermute(tokens[:, -EDGE:], "sp", up)
     after = lax.ppermute(tokens[:, :EDGE], "sp", down)
@@ -548,7 +550,8 @@
         in_hbm(w.reshape(sp, tp // 2, out_piece.shape[0], LANES))
         for w in (own_weight, other_weight)
     ]
-    core = (lax.axis_index("tp") % 2).astype(jnp.int32).reshape(1)
+    col = lax.axis_index("tp")
+    core = jnp.stack([col % 2, col // 2]).astype(jnp.int32)
     part = mix(
         mix_conv_kernel, core, conv_tok.reshape(tp, rows, LANES), weights, weights, 0, F32, 4,
         [pltpu.VMEM((rows, tp * LANES), BF16)],

time: 139 us -> 140 us (level)
  the two profiles are of different devices: /device:TPU:1 before, /device:TPU:64 now
where the time goes in v5:
time: 140 us; the launch traced here: 139 us
  Pallas kernels  63.2 us (45%)
  starting transfers between devices  37.9 us (27%)
  waiting for transfers between devices  17.5 us (12%)
  between operations  14.2 us (10%)
  local copies, waits for them, and re-layouts  3.24 us (2%)
  other arithmetic  2.81 us (2%)
    pallas_call x1, Pallas kernels, project(): pl.pallas_call(functools.partial(project_kernel, sub=sub, chunk=chunk), g...  18.2 us
    pallas_call x1, Pallas kernels, norm_tokens(): pl.pallas_call(norm_kernel, grid=(rows // block,), in_specs=[pl.BlockSpec...  17.2 us
    pallas_call x2, Pallas kernels, mix(): pl.pallas_call(kernel, grid=(groups // cols,), in_specs=[pl.BlockSpec(mem...  13.8 us
    pallas_call x1, Pallas kernels, attend_inner(): pl.pallas_call(inner_kernel, grid=(seqs,), in_specs=[pl.BlockSpec(memory_...  7.72 us
    all_to_all x1, starting transfers between devices, on_device(): in_weight = lax.all_to_all(in_piece, 'sp', 0, 0, tiled=True)  7.45 us
    ppermute x1, waiting for transfers between devices, on_device(): before = lax.ppermute(tokens[:, -EDGE:], 'sp', up)  5.94 us
    ppermute x3, starting transfers between devices, on_device(): pieces.append(lax.ppermute(out_piece, 'tp', ring))  5.83 us
    all_to_all x1, waiting for transfers between devices, on_device(): attn_tok = lax.all_to_all(attn, 'tp', 0, 0, tiled=True)  5.59 us
  transfers between devices with their start and end apart: 12, of which 5 were waited for; matrix products, arithmetic and copies ran while one was open for 3% of the time, Pallas kernels for 39%

profile of v5, /device:TPU:64, one launch (start us, length us, event | category | flops | bytes accessed | tf_op | source)
XLA Modules:
  0.0 138.8 jit_solution(13818738283422578151)
XLA Ops:
  7.2 2.4 %pack.1 = (bf16[272,128]{1,0:T(8,128)(2,1)S(1)}, bf16[16,128,512]{2,1,0:T(8,128)(2,1)}) custom-call(bf16[128,128]{1,0:T(8,128)(2,1)} %value_ref.1, bf16[128,128]{1,0:T(8,128)(2,1)} %gate_ref.1, bf16[128,128]{1,0:T(8,128)(2,1)} %query_ref.1, bf16[64,128]{1,0:T(8,128)(2,1)} %bitcast.19, bf16[64,128]{1,0:T(8,128)(2,1)} %bitcast.20, bf16[128,128]{1,0:T(8,128)(2,1)} %conv_ref.1, ...), custom_call_target="tpu_custom_call" | custom-call | tf_op jit(solution)/shard_map/pack/pallas_call | solution.py:470
  9.6 1.6 %collective-permute-start.4 = (bf16[272,128]{1,0:T(8,128)(2,1)S(1)}, bf16[272,128]{1,0:T(8,128)(2,1)S(1)}, u32[]{:S(2)}, u32[]{:S(2)}) collective-permute-start(bf16[272,128]{1,0:T(8,128)(2,1)S(1)} %get-tuple-element.23), channel_id=1, source_target_pairs={{0,2},{1,3},{2,4},{3,5},{4,6},{5,7},{6,0},{7,1},{8,10},{9,11},{10,... | collective-permute-start | bytes 208904 | tf_op jit(solution)/shard_map/ppermute | solution.py:526
  11.2 2.9 %collective-permute-start.5 = (bf16[272,128]{1,0:T(8,128)(2,1)S(1)}, bf16[272,128]{1,0:T(8,128)(2,1)S(1)}, u32[]{:S(2)}, u32[]{:S(2)}) collective-permute-start(bf16[272,128]{1,0:T(8,128)(2,1)S(1)} %get-tuple-element.23), channel_id=1, source_target_pairs={{0,4},{1,5},{2,6},{3,7},{4,0},{5,1},{6,2},{7,3},{8,12},{9,13},{10,... | collective-permute-start | bytes 208904 | tf_op jit(solution)/shard_map/ppermute | solution.py:526
  14.1 1.3 collective-permute-start.6
  15.4 2.0 %collective-permute-done.5 = bf16[272,128]{1,0:T(8,128)(2,1)S(1)} collective-permute-done((bf16[272,128]{1,0:T(8,128)(2,1)S(1)}, bf16[272,128]{1,0:T(8,128)(2,1)S(1)}, u32[]{:S(2)}, u32[]{:S(2)}) %collective-permute-start.5) | collective-permute-done | bytes 69664 | tf_op jit(solution)/shard_map/ppermute | solution.py:526
  17.5 0.9 collective-permute-done.6
  19.2 7.5 %all-to-all-start = ((bf16[16,128,512]{2,1,0:T(8,128)(2,1)}), bf16[16,128,512]{2,1,0:T(8,128)(2,1)S(1)}, u32[]{:S(2)}, u32[]{:S(2)}) async-start(bf16[16,128,512]{2,1,0:T(8,128)(2,1)} %get-tuple-element.15), calls=%async_computation | async-start | bytes 4194304 | tf_op jit(solution)/shard_map/all_to_all | solution.py:522
  26.6 1.9 %fusion.5 = (bf16[4,16,2048]{2,1,0:T(8,128)(2,1)}, bf16[4,16,2048]{2,1,0:T(8,128)(2,1)}) fusion(bf16[4,1024,2048]{2,1,0:T(8,128)(2,1)} %param.12), kind=kLoop, calls=%fused_computation.14 | loop fusion | bytes 1048576 | tf_op jit(solution)/shard_map/slice | solution.py:530
  28.5 3.4 %collective-permute-start = (bf16[4,16,2048]{2,1,0:T(8,128)(2,1)}, bf16[4,16,2048]{2,1,0:T(8,128)(2,1)S(1)}, u32[]{:S(2)}, u32[]{:S(2)}) collective-permute-start(bf16[4,16,2048]{2,1,0:T(8,128)(2,1)} %get-tuple-element.29), channel_id=1, source_target_pairs={{0,8},{8,16},{16,24},{24,32},{32,40},{40,48},{48,56},{56,64},{64,7... | collective-permute-start | bytes 786440 | tf_op jit(solution)/shard_map/ppermute | solution.py:529
  31.9 4.6 %collective-permute-start.1 = (bf16[4,16,2048]{2,1,0:T(8,128)(2,1)}, bf16[4,16,2048]{2,1,0:T(8,128)(2,1)}, u32[]{:S(2)}, u32[]{:S(2)}) collective-permute-start(bf16[4,16,2048]{2,1,0:T(8,128)(2,1)} %get-tuple-element.28), channel_id=1, source_target_pairs={{8,0},{16,8},{24,16},{32,24},{40,32},{48,40},{56,48},{64,56},{72,6... | collective-permute-start | bytes 786440 | tf_op jit(solution)/shard_map/ppermute | solution.py:530
  36.5 17.2 %norm_tokens.1.x_ref = bf16[4096,2048]{1,0:T(8,128)(2,1)} custom-call(bf16[4096,2048]{1,0:T(8,128)(2,1)} %bitcast.17, bf16[1,2048]{1,0:T(2,128)(2,1)S(1)} %reshape.59.gain_ref), custom_call_target="tpu_custom_call" | custom-call | flops 335544320 | bytes 33554432 | tf_op jit(solution)/shard_map/norm_tokens/pallas_call | solution.py:48
  53.7 1.9 %fusion = (f32[1024,128]{1,0:T(8,128)S(1)}, f32[1024,128]{1,0:T(8,128)S(1)}) fusion(f32[128]{0:T(128)S(1)} %get-tuple-element.32, f32[128]{0:T(128)S(1)} %get-tuple-element.33, f32[1024]{0:T(1024)S(1)} %add_convert_fusion), kind=kLoop, calls=%fused_computation.2 | loop fusion | flops 262144 | bytes 1053696 | tf_op jit(solution)/shard_map/mul | solution.py:495
  55.7 5.9 %collective-permute-done.before_ref = bf16[4,16,2048]{2,1,0:T(8,128)(2,1)S(1)} collective-permute-done((bf16[4,16,2048]{2,1,0:T(8,128)(2,1)}, bf16[4,16,2048]{2,1,0:T(8,128)(2,1)S(1)}, u32[]{:S(2)}, u32[]{:S(2)}) %collective-permute-start) | collective-permute-done | bytes 262176 | tf_op jit(solution)/shard_map/ppermute | solution.py:529
  62.3 18.2 %project.1 = (bf16[8,4,128,128]{3,2,1,0:T(8,128)(2,1)}, bf16[4,1024,128]{2,1,0:T(8,128)(2,1)}, bf16[4,1024,128]{2,1,0:T(8,128)(2,1)}, bf16[4,128,128]{2,1,0:T(8,128)(2,1)S(1)}, bf16[4,128,128]{2,1,0:T(8,128)(2,1)S(1)}) custom-call(bf16[4096,2048]{1,0:T(8,128)(2,1)} %norm_tokens.1.x_ref, bf16[4,16,2048]{2,1,0:T(8,128)(2,1)S(1)} %collective-permute-done.before_ref, ...), custom_call_target="tpu_custom_call" | custom-call | flops 8589934592 | bytes 16777216 | tf_op jit(solution)/shard_map/project/pallas_call | solution.py:137
  81.2 3.6 %all-to-all-start.2 = ((bf16[8,4,128,128]{3,2,1,0:T(8,128)(2,1)}), bf16[8,4,128,128]{3,2,1,0:T(8,128)(2,1)S(1)}, u32[]{:S(2)}, u32[]{:S(2)}) async-start(bf16[8,4,128,128]{3,2,1,0:T(8,128)(2,1)} %get-tuple-element.24), calls=%async_computation.2 | async-start | bytes 2097152 | tf_op jit(solution)/shard_map/all_to_all | solution.py:539
  84.7 3.0 %collective-permute-start.2 = (bf16[4,128,128]{2,1,0:T(8,128)(2,1)}, bf16[4,128,128]{2,1,0:T(8,128)(2,1)S(1)}, u32[]{:S(2)}, u32[]{:S(2)}) collective-permute-start(bf16[4,128,128]{2,1,0:T(8,128)(2,1)} %copy-done.1), channel_id=1, source_target_pairs={{0,8},{8,16},{16,24},{24,32},{32,40},{40,48},{48,56},{56,64},{64,7... | collective-permute-start | bytes 393224 | tf_op jit(solution)/shard_map/ppermute | solution.py:537
  87.8 5.1 %collective-permute-start.3 = (bf16[4,128,128]{2,1,0:T(8,128)(2,1)S(1)}, bf16[4,128,128]{2,1,0:T(8,128)(2,1)S(1)}, u32[]{:S(2)}, u32[]{:S(2)}) collective-permute-start(bf16[4,128,128]{2,1,0:T(8,128)(2,1)S(1)} %get-tuple-element.19), channel_id=1, source_target_pairs={{8,0},{16,8},{24,16},{32,24},{40,32},{48,40},{56,48},{64,56},{72,6... | collective-permute-start | bytes 393224 | tf_op jit(solution)/shard_map/ppermute | solution.py:538
  93.0 7.7 %attend_inner.1 = (bf16[8,4,128,128]{3,2,1,0:T(8,128)(2,1)}, f32[4,2,1024]{2,1,0:T(2,128)}) custom-call(f32[2]{0:T(128)S(1)} %copy-done, bf16[4,1024,128]{2,1,0:T(8,128)(2,1)} %get-tuple-element.16.q_ref.q_low_ref.q_high_ref, bf16[4,1024,128]{2,1,0:T(8,128)(2,1)} %get-tuple-element.18.kv_ref.kv_low_ref.kv_high_ref), custom_call_target="tpu_custom_call" | custom-call | flops 1006632960 | bytes 3145728 | tf_op jit(solution)/shard_map/attend_inner/pallas_call | solution.py:262
  100.7 3.9 %attend_edge.1 = (bf16[8,4,128,128]{3,2,1,0:T(8,128)(2,1)}, f32[4,2,1024]{2,1,0:T(2,128)}) custom-call(s32[2]{0:T(128)S(1)} %pad_add_fusion.1.place_ref, f32[2]{0:T(128)S(1)} %copy-done, bf16[4,1024,128]{2,1,0:T(8,128)(2,1)} %get-tuple-element.16.q_ref.q_low_ref.q_high_ref, ...), custom_call_target="tpu_custom_call", output_to_operand_aliasing={{0}: (8, {}), {1}: (9, {})} | custom-call | flops 251658240 | bytes 1048576 | tf_op jit(solution)/shard_map/attend_edge/pallas_call | solution.py:346
  104.7 4.9 %all-to-all-start.1 = ((bf16[8,4,128,128]{3,2,1,0:T(8,128)(2,1)}), bf16[8,4,128,128]{3,2,1,0:T(8,128)(2,1)S(1)}, u32[]{:S(2)}, u32[]{:S(2)}) async-start(bf16[8,4,128,128]{3,2,1,0:T(8,128)(2,1)} %get-tuple-element.22), calls=%async_computation.1 | async-start | bytes 2097152 | tf_op jit(solution)/shard_map/all_to_all | solution.py:544
  109.6 2.9 %collective-permute-done.7 = bf16[17408,128]{1,0:T(8,128)(2,1)} collective-permute-done((bf16[17408,128]{1,0:T(8,128)(2,1)}, bf16[17408,128]{1,0:T(8,128)(2,1)}, u32[]{:S(2)}, u32[]{:S(2)}) %collective-permute-start.7) | collective-permute-done | bytes 4456480 | tf_op jit(solution)/shard_map/ppermute | solution.py:548
  112.6 7.3 %shard_map.131.part_ref = f32[512,2048]{1,0:T(8,128)} custom-call(s32[2]{0:T(128)S(1)} %pad_add_fusion.meta_ref, bf16[8,512,128]{2,1,0:T(8,128)(2,1)S(1)} %bitcast.12, bf16[16,4,272,128]{3,2,1,0:T(8,128)(2,1)} %bitcast.14, bf16[16,4,272,128]{3,2,1,0:T(8,128)(2,1)} %bitcast.10.other_gain_ref.other_ref, bf16[16,4,272,128]{3,2,1,0:T(8,128)(2,1)} %bitcast.15, ...), custom_call_target="tpu_custom_call" | custom-call | flops 2147483648 | bytes 4456448 | tf_op jit(solution)/shard_map/pallas_call | solution.py:432
  119.9 5.6 %all-to-all-done.1 = bf16[8,4,128,128]{3,2,1,0:T(8,128)(2,1)S(1)} async-done(((bf16[8,4,128,128]{3,2,1,0:T(8,128)(2,1)}), bf16[8,4,128,128]{3,2,1,0:T(8,128)(2,1)S(1)}, u32[]{:S(2)}, u32[]{:S(2)}) %all-to-all-start.1) | async-done | bytes 1048608 | tf_op jit(solution)/shard_map/all_to_all | solution.py:544
  125.5 6.4 %shard_map.132 = bf16[512,2048]{1,0:T(8,128)(2,1)} custom-call(s32[2]{0:T(128)S(1)} %pad_add_fusion.meta_ref, bf16[8,512,128]{2,1,0:T(8,128)(2,1)S(1)} %bitcast.13, f32[512,2048]{1,0:T(8,128)} %shard_map.131.part_ref, bf16[16,4,272,128]{3,2,1,0:T(8,128)(2,1)} %bitcast.16, bf16[16,4,272,128]{3,2,1,0:T(8,128)(2,1)} %bitcast.10.other_gain_ref.other_ref), custom_call_target="tpu_custom_call" | custom-call | flops 2147483648 | bytes 4456448 | tf_op jit(solution)/shard_map/pallas_call | solution.py:432
  (24 shorter events, 2.4 us)
Async XLA Ops:
  7.2 29.3 %copy-start.3 = (bf16[2048]{0:T(1024)(128)(2,1)S(1)}, bf16[2048]{0:T(1024)(128)(2,1)}, u32[]{:S(2)}) copy-start(bf16[2048]{0:T(1024)(128)(2,1)} %param.13) | copy-start | bytes 12292
  7.2 97.4 %all-gather.2.cloned.1.call-start = ((), (), s32[]{:S(2)}) async-start(), calls=%async_computation.3 | async-start | bytes 4734976 | tf_op jit(solution)/shard_map/all_gather | solution.py:527
  9.6 5.8 %collective-permute-start.4 = (bf16[272,128]{1,0:T(8,128)(2,1)S(1)}, bf16[272,128]{1,0:T(8,128)(2,1)S(1)}, u32[]{:S(2)}, u32[]{:S(2)}) collective-permute-start(bf16[272,128]{1,0:T(8,128)(2,1)S(1)} %get-tuple-element.23), channel_id=1, source_target_pairs={{0,2},{1,3},{2,4},{3,5},{4,6},{5,7},{6,0},{7,1},{8,10},{9,11},{10,... | collective-permute-start | bytes 208904 | tf_op jit(solution)/shard_map/ppermute | solution.py:526
  11.2 6.3 %collective-permute-start.5 = (bf16[272,128]{1,0:T(8,128)(2,1)S(1)}, bf16[272,128]{1,0:T(8,128)(2,1)S(1)}, u32[]{:S(2)}, u32[]{:S(2)}) collective-permute-start(bf16[272,128]{1,0:T(8,128)(2,1)S(1)} %get-tuple-element.23), channel_id=1, source_target_pairs={{0,4},{1,5},{2,6},{3,7},{4,0},{5,1},{6,2},{7,3},{8,12},{9,13},{10,... | collective-permute-start | bytes 208904 | tf_op jit(solution)/shard_map/ppermute | solution.py:526
  14.1 4.3 %collective-permute-start.6 = (bf16[272,128]{1,0:T(8,128)(2,1)S(1)}, bf16[272,128]{1,0:T(8,128)(2,1)S(1)}, u32[]{:S(2)}, u32[]{:S(2)}) collective-permute-start(bf16[272,128]{1,0:T(8,128)(2,1)S(1)} %get-tuple-element.23), channel_id=1, source_target_pairs={{0,6},{1,7},{2,0},{3,1},{4,2},{5,3},{6,4},{7,5},{8,14},{9,15},{10,... | collective-permute-start | bytes 208904 | tf_op jit(solution)/shard_map/ppermute | solution.py:526
  19.2 42.4 %all-to-all-start = ((bf16[16,128,512]{2,1,0:T(8,128)(2,1)}), bf16[16,128,512]{2,1,0:T(8,128)(2,1)S(1)}, u32[]{:S(2)}, u32[]{:S(2)}) async-start(bf16[16,128,512]{2,1,0:T(8,128)(2,1)} %get-tuple-element.15), calls=%async_computation | async-start | bytes 4194304 | tf_op jit(solution)/shard_map/all_to_all | solution.py:522
  28.5 33.1 %collective-permute-start = (bf16[4,16,2048]{2,1,0:T(8,128)(2,1)}, bf16[4,16,2048]{2,1,0:T(8,128)(2,1)S(1)}, u32[]{:S(2)}, u32[]{:S(2)}) collective-permute-start(bf16[4,16,2048]{2,1,0:T(8,128)(2,1)} %get-tuple-element.29), channel_id=1, source_target_pairs={{0,8},{8,16},{16,24},{24,32},{32,40},{40,48},{48,56},{56,64},{64,7... | collective-permute-start | bytes 786440 | tf_op jit(solution)/shard_map/ppermute | solution.py:529
  31.9 29.7 %collective-permute-start.1 = (bf16[4,16,2048]{2,1,0:T(8,128)(2,1)}, bf16[4,16,2048]{2,1,0:T(8,128)(2,1)}, u32[]{:S(2)}, u32[]{:S(2)}) collective-permute-start(bf16[4,16,2048]{2,1,0:T(8,128)(2,1)} %get-tuple-element.28), channel_id=1, source_target_pairs={{8,0},{16,8},{24,16},{32,24},{40,32},{48,40},{56,48},{64,56},{72,6... | collective-permute-start | bytes 786440 | tf_op jit(solution)/shard_map/ppermute | solution.py:530
  61.6 0.7 copy-start.2
  62.3 30.7 %copy-start = (f32[2]{0:T(128)S(1)}, f32[2]{0:T(128)}, u32[]{:S(2)}) copy-start(f32[2]{0:T(128)} %sink_ref.3) | copy-start | bytes 28
  80.5 0.7 copy-start.1
  81.2 23.4 %all-to-all-start.2 = ((bf16[8,4,128,128]{3,2,1,0:T(8,128)(2,1)}), bf16[8,4,128,128]{3,2,1,0:T(8,128)(2,1)S(1)}, u32[]{:S(2)}, u32[]{:S(2)}) async-start(bf16[8,4,128,128]{3,2,1,0:T(8,128)(2,1)} %get-tuple-element.24), calls=%async_computation.2 | async-start | bytes 2097152 | tf_op jit(solution)/shard_map/all_to_all | solution.py:539
  84.7 16.0 %collective-permute-start.2 = (bf16[4,128,128]{2,1,0:T(8,128)(2,1)}, bf16[4,128,128]{2,1,0:T(8,128)(2,1)S(1)}, u32[]{:S(2)}, u32[]{:S(2)}) collective-permute-start(bf16[4,128,128]{2,1,0:T(8,128)(2,1)} %copy-done.1), channel_id=1, source_target_pairs={{0,8},{8,16},{16,24},{24,32},{32,40},{40,48},{48,56},{56,64},{64,7... | collective-permute-start | bytes 393224 | tf_op jit(solution)/shard_map/ppermute | solution.py:537
  87.8 12.9 %collective-permute-start.3 = (bf16[4,128,128]{2,1,0:T(8,128)(2,1)S(1)}, bf16[4,128,128]{2,1,0:T(8,128)(2,1)S(1)}, u32[]{:S(2)}, u32[]{:S(2)}) collective-permute-start(bf16[4,128,128]{2,1,0:T(8,128)(2,1)S(1)} %get-tuple-element.19), channel_id=1, source_target_pairs={{8,0},{16,8},{24,16},{32,24},{40,32},{48,40},{56,48},{64,56},{72,6... | collective-permute-start | bytes 393224 | tf_op jit(solution)/shard_map/ppermute | solution.py:538
  104.6 8.0 %collective-permute-start.7 = (bf16[17408,128]{1,0:T(8,128)(2,1)}, bf16[17408,128]{1,0:T(8,128)(2,1)}, u32[]{:S(2)}, u32[]{:S(2)}) collective-permute-start(bf16[17408,128]{1,0:T(8,128)(2,1)} %all-gather.2.cloned.1.call-done), channel_id=1, source_target_pairs={{0,1},{1,0},{2,3},{3,2},{4,5},{5,4},{6,7},{7,6},{8,9},{9,8},{10,11... | collective-permute-start | bytes 13369352 | tf_op jit(solution)/shard_map/ppermute | solution.py:548
  104.7 20.8 %all-to-all-start.1 = ((bf16[8,4,128,128]{3,2,1,0:T(8,128)(2,1)}), bf16[8,4,128,128]{3,2,1,0:T(8,128)(2,1)S(1)}, u32[]{:S(2)}, u32[]{:S(2)}) async-start(bf16[8,4,128,128]{3,2,1,0:T(8,128)(2,1)} %get-tuple-element.22), calls=%async_computation.1 | async-start | bytes 2097152 | tf_op jit(solution)/shard_map/all_to_all | solution.py:544
Sparse Core Ops, SparseCore 0:
  19.3 71.4 all-gather.1

commit v6 on v5

--- a/solution.py
+++ b/solution.py
@@ -134,24 +134,26 @@
     inside = pl.BlockSpec(memory_space=pltpu.VMEM)
     heads = pltpu.HBM((seqs, length, LANES), BF16)
     head_block = pl.BlockSpec((1, length, LANES), lambda s: (jnp.minimum(s, seqs - 1), 0, 0))
+    edge_block = pl.BlockSpec((seqs, WINDOW, LANES), lambda s: (0, 0, 0))
     return pl.pallas_call(
         functools.partial(project_kernel, sub=sub, chunk=chunk),
         grid=(seqs + 1,),
         in_specs=[pl.BlockSpec((length, width), lambda s: (jnp.minimum(s, seqs - 1), 0))]
-        + [inside] * 7,
+        + [inside] * 4
+        + [pl.BlockSpec(taps.shape, lambda s: (0, 0)), inside, inside],
         out_specs=[
             pl.BlockSpec(
                 (dests, 1, length // dests, LANES), lambda s: (0, jnp.maximum(s - 1, 0), 0, 0)
             ),
             head_block,
             head_block,
-            inside,
-            inside,
+            edge_block,
+            edge_block,
         ],
         out_shape=[
             jax.ShapeDtypeStruct((dests, seqs, length // dests, LANES), BF16), heads, heads
         ]
-        + [jax.ShapeDtypeStruct((seqs, WINDOW, LANES), BF16)] * 2,
+        + [pltpu.HBM((seqs, WINDOW, LANES), BF16)] * 2,
         scratch_shapes=[pltpu.VMEM((2, length + 2 * EDGE, LANES), F32)],
         compiler_params=params("arbitrary", mb=28),
         cost_estimate=pl.CostEstimate(
@@ -160,7 +162,7 @@
             bytes_accessed=2 * rows * width,
         ),
         name="project",
-    )(in_hbm(normed), before, after, gain.reshape(1, width), weight, taps, cosine, sine)
+    )(in_hbm(normed), before, after, gain.reshape(1, width), weight, in_hbm(taps), cosine, sine)
 
 
 def band_bias(first, last):

time: 140 us -> 138 us (0.986)
  transfers between devices with their start and end apart: 12 -> 12, of which waited for: 5 -> 5; matrix products, arithmetic and copies ran while one was open for 3% -> 3% of each run, Pallas kernels for 39% -> 40%
where the time goes in v6:
time: 138 us
  Pallas kernels  63.3 us (46%)
  starting transfers between devices  37.9 us (27%)
  waiting for transfers between devices  17.5 us (13%)
  between operations  14.2 us (10%)
  other arithmetic  2.79 us (2%)
  local copies, waits for them, and re-layouts  1.9 us (1%)
    pallas_call x1, Pallas kernels, project(): pl.pallas_call(functools.partial(project_kernel, sub=sub, chunk=chunk), g...  18.4 us
    pallas_call x1, Pallas kernels, norm_tokens(): pl.pallas_call(norm_kernel, grid=(rows // block,), in_specs=[pl.BlockSpec...  17.2 us
    pallas_call x2, Pallas kernels, mix(): pl.pallas_call(kernel, grid=(groups // cols,), in_specs=[pl.BlockSpec(mem...  13.7 us
    pallas_call x1, Pallas kernels, attend_inner(): pl.pallas_call(inner_kernel, grid=(seqs,), in_specs=[pl.BlockSpec(memory_...  7.71 us
    all_to_all x1, starting transfers between devices, on_device(): in_weight = lax.all_to_all(in_piece, 'sp', 0, 0, tiled=True)  7.45 us
    ppermute x1, waiting for transfers between devices, on_device(): before = lax.ppermute(tokens[:, -EDGE:], 'sp', up)  5.95 us
    ppermute x3, starting transfers between devices, on_device(): pieces.append(lax.ppermute(out_piece, 'tp', ring))  5.83 us
    all_to_all x1, waiting for transfers between devices, on_device(): attn_tok = lax.all_to_all(attn, 'tp', 0, 0, tiled=True)  5.64 us
  transfers between devices with their start and end apart: 12, of which 5 were waited for; matrix products, arithmetic and copies ran while one was open for 3% of the time, Pallas kernels for 40%

profile of v6, /device:TPU:64, one launch (start us, length us, event | category | flops | bytes accessed | tf_op | source)
XLA Modules:
  0.0 137.6 jit_solution(9935961752440638115)
XLA Ops:
  7.2 2.4 %pack.1 = (bf16[272,128]{1,0:T(8,128)(2,1)S(1)}, bf16[16,128,512]{2,1,0:T(8,128)(2,1)}) custom-call(bf16[128,128]{1,0:T(8,128)(2,1)} %value_ref.1, bf16[128,128]{1,0:T(8,128)(2,1)} %gate_ref.1, bf16[128,128]{1,0:T(8,128)(2,1)} %query_ref.1, bf16[64,128]{1,0:T(8,128)(2,1)} %bitcast.19, bf16[64,128]{1,0:T(8,128)(2,1)} %bitcast.20, bf16[128,128]{1,0:T(8,128)(2,1)} %conv_ref.1, ...), custom_call_target="tpu_custom_call" | custom-call | tf_op jit(solution)/shard_map/pack/pallas_call | solution.py:472
  9.6 1.6 %collective-permute-start.4 = (bf16[272,128]{1,0:T(8,128)(2,1)S(1)}, bf16[272,128]{1,0:T(8,128)(2,1)S(1)}, u32[]{:S(2)}, u32[]{:S(2)}) collective-permute-start(bf16[272,128]{1,0:T(8,128)(2,1)S(1)} %get-tuple-element.23), channel_id=1, source_target_pairs={{0,2},{1,3},{2,4},{3,5},{4,6},{5,7},{6,0},{7,1},{8,10},{9,11},{10,... | collective-permute-start | bytes 208904 | tf_op jit(solution)/shard_map/ppermute | solution.py:528
  11.2 2.9 %collective-permute-start.5 = (bf16[272,128]{1,0:T(8,128)(2,1)S(1)}, bf16[272,128]{1,0:T(8,128)(2,1)S(1)}, u32[]{:S(2)}, u32[]{:S(2)}) collective-permute-start(bf16[272,128]{1,0:T(8,128)(2,1)S(1)} %get-tuple-element.23), channel_id=1, source_target_pairs={{0,4},{1,5},{2,6},{3,7},{4,0},{5,1},{6,2},{7,3},{8,12},{9,13},{10,... | collective-permute-start | bytes 208904 | tf_op jit(solution)/shard_map/ppermute | solution.py:528
  14.1 1.3 collective-permute-start.6
  15.4 2.0 %collective-permute-done.5 = bf16[272,128]{1,0:T(8,128)(2,1)S(1)} collective-permute-done((bf16[272,128]{1,0:T(8,128)(2,1)S(1)}, bf16[272,128]{1,0:T(8,128)(2,1)S(1)}, u32[]{:S(2)}, u32[]{:S(2)}) %collective-permute-start.5) | collective-permute-done | bytes 69664 | tf_op jit(solution)/shard_map/ppermute | solution.py:528
  17.5 0.9 collective-permute-done.6
  19.1 7.5 %all-to-all-start = ((bf16[16,128,512]{2,1,0:T(8,128)(2,1)}), bf16[16,128,512]{2,1,0:T(8,128)(2,1)S(1)}, u32[]{:S(2)}, u32[]{:S(2)}) async-start(bf16[16,128,512]{2,1,0:T(8,128)(2,1)} %get-tuple-element.15), calls=%async_computation | async-start | bytes 4194304 | tf_op jit(solution)/shard_map/all_to_all | solution.py:524
  26.6 1.9 %fusion.5 = (bf16[4,16,2048]{2,1,0:T(8,128)(2,1)}, bf16[4,16,2048]{2,1,0:T(8,128)(2,1)}) fusion(bf16[4,1024,2048]{2,1,0:T(8,128)(2,1)} %param.12), kind=kLoop, calls=%fused_computation.14 | loop fusion | bytes 1048576 | tf_op jit(solution)/shard_map/slice | solution.py:532
  28.5 3.4 %collective-permute-start = (bf16[4,16,2048]{2,1,0:T(8,128)(2,1)}, bf16[4,16,2048]{2,1,0:T(8,128)(2,1)S(1)}, u32[]{:S(2)}, u32[]{:S(2)}) collective-permute-start(bf16[4,16,2048]{2,1,0:T(8,128)(2,1)} %get-tuple-element.29), channel_id=1, source_target_pairs={{0,8},{8,16},{16,24},{24,32},{32,40},{40,48},{48,56},{56,64},{64,7... | collective-permute-start | bytes 786440 | tf_op jit(solution)/shard_map/ppermute | solution.py:531
  31.8 4.6 %collective-permute-start.1 = (bf16[4,16,2048]{2,1,0:T(8,128)(2,1)}, bf16[4,16,2048]{2,1,0:T(8,128)(2,1)}, u32[]{:S(2)}, u32[]{:S(2)}) collective-permute-start(bf16[4,16,2048]{2,1,0:T(8,128)(2,1)} %get-tuple-element.28), channel_id=1, source_target_pairs={{8,0},{16,8},{24,16},{32,24},{40,32},{48,40},{56,48},{64,56},{72,6... | collective-permute-start | bytes 786440 | tf_op jit(solution)/shard_map/ppermute | solution.py:532
  36.5 17.2 %norm_tokens.1.x_ref = bf16[4096,2048]{1,0:T(8,128)(2,1)} custom-call(bf16[4096,2048]{1,0:T(8,128)(2,1)} %bitcast.17, bf16[1,2048]{1,0:T(2,128)(2,1)S(1)} %reshape.59.gain_ref), custom_call_target="tpu_custom_call" | custom-call | flops 335544320 | bytes 33554432 | tf_op jit(solution)/shard_map/norm_tokens/pallas_call | solution.py:48
  53.7 1.9 %fusion = (f32[1024,128]{1,0:T(8,128)S(1)}, f32[1024,128]{1,0:T(8,128)S(1)}) fusion(f32[128]{0:T(128)S(1)} %get-tuple-element.32, f32[128]{0:T(128)S(1)} %get-tuple-element.33, f32[1024]{0:T(1024)S(1)} %add_convert_fusion), kind=kLoop, calls=%fused_computation.2 | loop fusion | flops 262144 | bytes 1053696 | tf_op jit(solution)/shard_map/mul | solution.py:497
  55.6 5.9 %collective-permute-done.before_ref = bf16[4,16,2048]{2,1,0:T(8,128)(2,1)S(1)} collective-permute-done((bf16[4,16,2048]{2,1,0:T(8,128)(2,1)}, bf16[4,16,2048]{2,1,0:T(8,128)(2,1)S(1)}, u32[]{:S(2)}, u32[]{:S(2)}) %collective-permute-start) | collective-permute-done | bytes 262176 | tf_op jit(solution)/shard_map/ppermute | solution.py:531
  61.6 18.4 %project.1 = (bf16[8,4,128,128]{3,2,1,0:T(8,128)(2,1)}, bf16[4,1024,128]{2,1,0:T(8,128)(2,1)}, bf16[4,1024,128]{2,1,0:T(8,128)(2,1)}, bf16[4,128,128]{2,1,0:T(8,128)(2,1)}, bf16[4,128,128]{2,1,0:T(8,128)(2,1)}) custom-call(bf16[4096,2048]{1,0:T(8,128)(2,1)} %norm_tokens.1.x_ref, bf16[4,16,2048]{2,1,0:T(8,128)(2,1)S(1)} %collective-permute-done.before_ref, ...), custom_call_target="tpu_custom_call" | custom-call | flops 8589934592 | bytes 16777216 | tf_op jit(solution)/shard_map/project/pallas_call | solution.py:138
  80.0 3.6 %all-to-all-start.2 = ((bf16[8,4,128,128]{3,2,1,0:T(8,128)(2,1)}), bf16[8,4,128,128]{3,2,1,0:T(8,128)(2,1)S(1)}, u32[]{:S(2)}, u32[]{:S(2)}) async-start(bf16[8,4,128,128]{3,2,1,0:T(8,128)(2,1)} %get-tuple-element.24), calls=%async_computation.2 | async-start | bytes 2097152 | tf_op jit(solution)/shard_map/all_to_all | solution.py:541
  83.6 3.0 %collective-permute-start.2 = (bf16[4,128,128]{2,1,0:T(8,128)(2,1)}, bf16[4,128,128]{2,1,0:T(8,128)(2,1)S(1)}, u32[]{:S(2)}, u32[]{:S(2)}) collective-permute-start(bf16[4,128,128]{2,1,0:T(8,128)(2,1)} %get-tuple-element.17), channel_id=1, source_target_pairs={{0,8},{8,16},{16,24},{24,32},{32,40},{40,48},{48,56},{56,64},{64,7... | collective-permute-start | bytes 393224 | tf_op jit(solution)/shard_map/ppermute | solution.py:539
  86.6 5.1 %collective-permute-start.3 = (bf16[4,128,128]{2,1,0:T(8,128)(2,1)}, bf16[4,128,128]{2,1,0:T(8,128)(2,1)S(1)}, u32[]{:S(2)}, u32[]{:S(2)}) collective-permute-start(bf16[4,128,128]{2,1,0:T(8,128)(2,1)} %get-tuple-element.19), channel_id=1, source_target_pairs={{8,0},{16,8},{24,16},{32,24},{40,32},{48,40},{56,48},{64,56},{72,6... | collective-permute-start | bytes 393224 | tf_op jit(solution)/shard_map/ppermute | solution.py:540
  91.8 7.7 %attend_inner.1 = (bf16[8,4,128,128]{3,2,1,0:T(8,128)(2,1)}, f32[4,2,1024]{2,1,0:T(2,128)}) custom-call(f32[2]{0:T(128)S(1)} %copy-done, bf16[4,1024,128]{2,1,0:T(8,128)(2,1)} %get-tuple-element.16.q_ref.q_low_ref.q_high_ref, bf16[4,1024,128]{2,1,0:T(8,128)(2,1)} %get-tuple-element.18.kv_ref.kv_low_ref.kv_high_ref), custom_call_target="tpu_custom_call" | custom-call | flops 1006632960 | bytes 3145728 | tf_op jit(solution)/shard_map/attend_inner/pallas_call | solution.py:264
  99.5 3.9 %attend_edge.1 = (bf16[8,4,128,128]{3,2,1,0:T(8,128)(2,1)}, f32[4,2,1024]{2,1,0:T(2,128)}) custom-call(s32[2]{0:T(128)S(1)} %pad_add_fusion.1.place_ref, f32[2]{0:T(128)S(1)} %copy-done, bf16[4,1024,128]{2,1,0:T(8,128)(2,1)} %get-tuple-element.16.q_ref.q_low_ref.q_high_ref, ...), custom_call_target="tpu_custom_call", output_to_operand_aliasing={{0}: (8, {}), {1}: (9, {})} | custom-call | flops 251658240 | bytes 1048576 | tf_op jit(solution)/shard_map/attend_edge/pallas_call | solution.py:348
  103.5 4.9 %all-to-all-start.1 = ((bf16[8,4,128,128]{3,2,1,0:T(8,128)(2,1)}), bf16[8,4,128,128]{3,2,1,0:T(8,128)(2,1)S(1)}, u32[]{:S(2)}, u32[]{:S(2)}) async-start(bf16[8,4,128,128]{3,2,1,0:T(8,128)(2,1)} %get-tuple-element.22), calls=%async_computation.1 | async-start | bytes 2097152 | tf_op jit(solution)/shard_map/all_to_all | solution.py:546
  108.4 2.9 %collective-permute-done.7 = bf16[17408,128]{1,0:T(8,128)(2,1)} collective-permute-done((bf16[17408,128]{1,0:T(8,128)(2,1)}, bf16[17408,128]{1,0:T(8,128)(2,1)}, u32[]{:S(2)}, u32[]{:S(2)}) %collective-permute-start.7) | collective-permute-done | bytes 4456480 | tf_op jit(solution)/shard_map/ppermute | solution.py:550
  111.4 7.3 %shard_map.131.part_ref = f32[512,2048]{1,0:T(8,128)} custom-call(s32[2]{0:T(128)S(1)} %pad_add_fusion.meta_ref, bf16[8,512,128]{2,1,0:T(8,128)(2,1)S(1)} %bitcast.12, bf16[16,4,272,128]{3,2,1,0:T(8,128)(2,1)} %bitcast.14, bf16[16,4,272,128]{3,2,1,0:T(8,128)(2,1)} %bitcast.10.other_gain_ref.other_ref, bf16[16,4,272,128]{3,2,1,0:T(8,128)(2,1)} %bitcast.15, ...), custom_call_target="tpu_custom_call" | custom-call | flops 2147483648 | bytes 4456448 | tf_op jit(solution)/shard_map/pallas_call | solution.py:434
  118.7 5.6 %all-to-all-done.1 = bf16[8,4,128,128]{3,2,1,0:T(8,128)(2,1)S(1)} async-done(((bf16[8,4,128,128]{3,2,1,0:T(8,128)(2,1)}), bf16[8,4,128,128]{3,2,1,0:T(8,128)(2,1)S(1)}, u32[]{:S(2)}, u32[]{:S(2)}) %all-to-all-start.1) | async-done | bytes 1048608 | tf_op jit(solution)/shard_map/all_to_all | solution.py:546
  124.3 6.4 %shard_map.132 = bf16[512,2048]{1,0:T(8,128)(2,1)} custom-call(s32[2]{0:T(128)S(1)} %pad_add_fusion.meta_ref, bf16[8,512,128]{2,1,0:T(8,128)(2,1)S(1)} %bitcast.13, f32[512,2048]{1,0:T(8,128)} %shard_map.131.part_ref, bf16[16,4,272,128]{3,2,1,0:T(8,128)(2,1)} %bitcast.16, bf16[16,4,272,128]{3,2,1,0:T(8,128)(2,1)} %bitcast.10.other_gain_ref.other_ref), custom_call_target="tpu_custom_call" | custom-call | flops 2147483648 | bytes 4456448 | tf_op jit(solution)/shard_map/pallas_call | solution.py:434
  (20 shorter events, 1.1 us)
Async XLA Ops:
  7.2 29.3 %copy-start.1 = (bf16[2048]{0:T(1024)(128)(2,1)S(1)}, bf16[2048]{0:T(1024)(128)(2,1)}, u32[]{:S(2)}) copy-start(bf16[2048]{0:T(1024)(128)(2,1)} %param.13) | copy-start | bytes 12292
  7.2 96.2 %all-gather.2.cloned.1.call-start = ((), (), s32[]{:S(2)}) async-start(), calls=%async_computation.3 | async-start | bytes 4734976 | tf_op jit(solution)/shard_map/all_gather | solution.py:529
  9.6 5.8 %collective-permute-start.4 = (bf16[272,128]{1,0:T(8,128)(2,1)S(1)}, bf16[272,128]{1,0:T(8,128)(2,1)S(1)}, u32[]{:S(2)}, u32[]{:S(2)}) collective-permute-start(bf16[272,128]{1,0:T(8,128)(2,1)S(1)} %get-tuple-element.23), channel_id=1, source_target_pairs={{0,2},{1,3},{2,4},{3,5},{4,6},{5,7},{6,0},{7,1},{8,10},{9,11},{10,... | collective-permute-start | bytes 208904 | tf_op jit(solution)/shard_map/ppermute | solution.py:528
  11.2 6.3 %collective-permute-start.5 = (bf16[272,128]{1,0:T(8,128)(2,1)S(1)}, bf16[272,128]{1,0:T(8,128)(2,1)S(1)}, u32[]{:S(2)}, u32[]{:S(2)}) collective-permute-start(bf16[272,128]{1,0:T(8,128)(2,1)S(1)} %get-tuple-element.23), channel_id=1, source_target_pairs={{0,4},{1,5},{2,6},{3,7},{4,0},{5,1},{6,2},{7,3},{8,12},{9,13},{10,... | collective-permute-start | bytes 208904 | tf_op jit(solution)/shard_map/ppermute | solution.py:528
  14.1 4.3 %collective-permute-start.6 = (bf16[272,128]{1,0:T(8,128)(2,1)S(1)}, bf16[272,128]{1,0:T(8,128)(2,1)S(1)}, u32[]{:S(2)}, u32[]{:S(2)}) collective-permute-start(bf16[272,128]{1,0:T(8,128)(2,1)S(1)} %get-tuple-element.23), channel_id=1, source_target_pairs={{0,6},{1,7},{2,0},{3,1},{4,2},{5,3},{6,4},{7,5},{8,14},{9,15},{10,... | collective-permute-start | bytes 208904 | tf_op jit(solution)/shard_map/ppermute | solution.py:528
  19.1 42.4 %all-to-all-start = ((bf16[16,128,512]{2,1,0:T(8,128)(2,1)}), bf16[16,128,512]{2,1,0:T(8,128)(2,1)S(1)}, u32[]{:S(2)}, u32[]{:S(2)}) async-start(bf16[16,128,512]{2,1,0:T(8,128)(2,1)} %get-tuple-element.15), calls=%async_computation | async-start | bytes 4194304 | tf_op jit(solution)/shard_map/all_to_all | solution.py:524
  28.5 33.1 %collective-permute-start = (bf16[4,16,2048]{2,1,0:T(8,128)(2,1)}, bf16[4,16,2048]{2,1,0:T(8,128)(2,1)S(1)}, u32[]{:S(2)}, u32[]{:S(2)}) collective-permute-start(bf16[4,16,2048]{2,1,0:T(8,128)(2,1)} %get-tuple-element.29), channel_id=1, source_target_pairs={{0,8},{8,16},{16,24},{24,32},{32,40},{40,48},{48,56},{56,64},{64,7... | collective-permute-start | bytes 786440 | tf_op jit(solution)/shard_map/ppermute | solution.py:531
  31.8 29.7 %collective-permute-start.1 = (bf16[4,16,2048]{2,1,0:T(8,128)(2,1)}, bf16[4,16,2048]{2,1,0:T(8,128)(2,1)}, u32[]{:S(2)}, u32[]{:S(2)}) collective-permute-start(bf16[4,16,2048]{2,1,0:T(8,128)(2,1)} %get-tuple-element.28), channel_id=1, source_target_pairs={{8,0},{16,8},{24,16},{32,24},{40,32},{48,40},{56,48},{64,56},{72,6... | collective-permute-start | bytes 786440 | tf_op jit(solution)/shard_map/ppermute | solution.py:532
  61.6 30.2 %copy-start = (f32[2]{0:T(128)S(1)}, f32[2]{0:T(128)}, u32[]{:S(2)}) copy-start(f32[2]{0:T(128)} %sink_ref.3) | copy-start | bytes 28
  80.0 23.4 %all-to-all-start.2 = ((bf16[8,4,128,128]{3,2,1,0:T(8,128)(2,1)}), bf16[8,4,128,128]{3,2,1,0:T(8,128)(2,1)S(1)}, u32[]{:S(2)}, u32[]{:S(2)}) async-start(bf16[8,4,128,128]{3,2,1,0:T(8,128)(2,1)} %get-tuple-element.24), calls=%async_computation.2 | async-start | bytes 2097152 | tf_op jit(solution)/shard_map/all_to_all | solution.py:541
  83.6 15.9 %collective-permute-start.2 = (bf16[4,128,128]{2,1,0:T(8,128)(2,1)}, bf16[4,128,128]{2,1,0:T(8,128)(2,1)S(1)}, u32[]{:S(2)}, u32[]{:S(2)}) collective-permute-start(bf16[4,128,128]{2,1,0:T(8,128)(2,1)} %get-tuple-element.17), channel_id=1, source_target_pairs={{0,8},{8,16},{16,24},{24,32},{32,40},{40,48},{48,56},{56,64},{64,7... | collective-permute-start | bytes 393224 | tf_op jit(solution)/shard_map/ppermute | solution.py:539
  86.6 12.9 %collective-permute-start.3 = (bf16[4,128,128]{2,1,0:T(8,128)(2,1)}, bf16[4,128,128]{2,1,0:T(8,128)(2,1)S(1)}, u32[]{:S(2)}, u32[]{:S(2)}) collective-permute-start(bf16[4,128,128]{2,1,0:T(8,128)(2,1)} %get-tuple-element.19), channel_id=1, source_target_pairs={{8,0},{16,8},{24,16},{32,24},{40,32},{48,40},{56,48},{64,56},{72,6... | collective-permute-start | bytes 393224 | tf_op jit(solution)/shard_map/ppermute | solution.py:540
  103.4 8.0 %collective-permute-start.7 = (bf16[17408,128]{1,0:T(8,128)(2,1)}, bf16[17408,128]{1,0:T(8,128)(2,1)}, u32[]{:S(2)}, u32[]{:S(2)}) collective-permute-start(bf16[17408,128]{1,0:T(8,128)(2,1)} %all-gather.2.cloned.1.call-done), channel_id=1, source_target_pairs={{0,1},{1,0},{2,3},{3,2},{4,5},{5,4},{6,7},{7,6},{8,9},{9,8},{10,11... | collective-permute-start | bytes 13369352 | tf_op jit(solution)/shard_map/ppermute | solution.py:550
  103.5 20.8 %all-to-all-start.1 = ((bf16[8,4,128,128]{3,2,1,0:T(8,128)(2,1)}), bf16[8,4,128,128]{3,2,1,0:T(8,128)(2,1)S(1)}, u32[]{:S(2)}, u32[]{:S(2)}) async-start(bf16[8,4,128,128]{3,2,1,0:T(8,128)(2,1)} %get-tuple-element.22), calls=%async_computation.1 | async-start | bytes 2097152 | tf_op jit(solution)/shard_map/all_to_all | solution.py:546
Sparse Core Ops, SparseCore 0:
  19.3 71.4 all-gather.1
